TPU v7x, 256 devices: a whole 4x4x8 slice. The times are simulated.
256 devices in a mesh: sp: 32 (over z, y), tp: 8 (over x, core).
Axes of the slice: x: 4, y: 4, z: 8, core: 2. Of those that a mesh axis runs over, the one named last changes fastest.
Arguments:
- head_value_rows: bfloat16 [24576, 2048], P('sp', 'tp'), may hold values from -6 to 6
- entry_map_rows: bfloat16 [24576, 1024], P('sp', 'tp'), may hold values from -6 to 6
- readout_map_rows: bfloat16 [24576, 1024], P('sp', 'tp'), may hold values from -6 to 6
- output_gate_rows: bfloat16 [24576, 2048], P('sp', 'tp'), may hold values from -6 to 6
- step_before_softplus: bfloat16 [24576, 32], P('sp', 'tp'), may hold values from -8 to 8
- sudden_log_decay: float32 [24576, 32], P('sp', 'tp'), may hold values from -1 to 0
- document_index: int32 [24576], replicated, may hold values from 0 to 7, never falling along the last dimension, each value on 1 to 6144 neighbouring positions
- head_rate_logarithm: float32 [2, 32], P(None, 'tp'), may hold values from -30 to 0
- head_step_bias: float32 [2, 32], P(None, 'tp'), may hold values from -3 to 3
- value_conv_taps: bfloat16 [5, 2048], P(None, 'tp'), may hold values from -2.5 to 2.5
- entry_conv_taps: bfloat16 [5, 1024], P(None, 'tp'), may hold values from -2.5 to 2.5
- readout_conv_taps: bfloat16 [5, 1024], P(None, 'tp'), may hold values from -2.5 to 2.5
- group_norm_gain: float32 [2048], P('tp'), may hold values from 0.1 to 1.9
- mixer_output_weight: bfloat16 [2048, 2048], P('tp'), may hold values from -0.125 to 0.125
- stream: bfloat16 [24576, 2048], P('sp', 'tp'), may hold values from -200 to 200
- mixer_norm_gain: float32 [2048], P('tp'), may hold values from 0.1 to 1.9
- channel_norm_gain: float32 [2048], P('tp'), may hold values from 0.1 to 1.9
- up_projection_weight: bfloat16 [2048, 8192], P('sp', 'tp'), may hold values from -0.125 to 0.125
- down_projection_weight: bfloat16 [2048, 8192], P('sp', 'tp'), may hold values from -0.0625 to 0.0625
Outputs:
- mixed: bfloat16 [24576, 2048], P('sp', 'tp')
All inputs are finite; a program needn't handle non-finite values.
Results may differ from a plain program's by a relative error of at most 0.018.
Values may be sent and summed in bfloat16 or wider, within the bound.
No kernel may reach another device: no remote copies, remote signals or barrier semaphores. Data moves between devices by JAX's collectives and lax.ppermute only.
A program may use at most 64 MiB of HBM per device.

v0:
```python
import jax
import jax.numpy as jnp
from jax import lax
from jax.sharding import Mesh
from jax.sharding import PartitionSpec as P

D = 2048
HEAD_DIM = 64
STATE = 128
BLOCK = 128
SP = ("sp_0", "sp_1")


norm_eps = 1e-05
resid_scale = 1.4142135623730951


def padded(block, sides, width):
    for axis, dim in sides:
        count = lax.axis_size(axis)
        forward = [(i, i + 1) for i in range(count - 1)]
        backward = [(target, source) for source, target in forward]
        low = lax.ppermute(
            lax.slice_in_dim(block, block.shape[dim] - width, None, axis=dim), axis, forward
        )
        high = lax.ppermute(lax.slice_in_dim(block, 0, width, axis=dim), axis, backward)
        block = jnp.concatenate([low, block, high], axis=dim)
    return block


def nothing_yet(array, identity):
    return jax.tree.map(
        lambda a, e: jnp.broadcast_to(jnp.asarray(e, a.dtype), a.shape), array, identity
    )


def carried_in(array, axes, combine, identity, reverse):
    before = start = nothing_yet(array, identity)
    subtotal = array
    for axis in reversed(axes):
        count, index = (lax.axis_size(axis), lax.axis_index(axis))
        pieces = jax.tree.map(
            lambda part, kind: lax.all_gather(part.astype(kind), axis),
            subtotal,
            (jnp.bfloat16, jnp.bfloat16),
        )
        inside, subtotal = (start, start)
        for k in reversed(range(count)) if reverse else range(count):
            passed = k > index if reverse else k < index
            subtotal = combine(
                subtotal, jax.tree.map(lambda part, own: part[k].astype(own.dtype), pieces, array)
            )
            inside = jax.tree.map(lambda new, old: jnp.where(passed, new, old), subtotal, inside)
        before = combine(inside, before)
    return before


def cut_along(array, dim, count):
    dims = array.shape
    blocks = array.reshape(*dims[:dim], count, dims[dim] // count, *dims[dim + 1 :])
    return jnp.moveaxis(blocks, dim, 0)


def sent_and_summed(array, axis, dim):
    blocks = cut_along(array, dim, lax.axis_size(axis))
    arrived = lax.all_to_all(blocks, axis, split_axis=0, concat_axis=0, tiled=True)
    return arrived.astype(jnp.float32).sum(axis=0)


def block_step(running, blocks):
    states, last_doc = running
    scaled, entries, readout, decay_logarithm, block_ids = blocks
    block_len = block_ids.shape[0]
    cum_decay = jnp.cumsum(decay_logarithm, axis=0)
    indices = lax.iota(jnp.int32, block_len)
    linked = (indices[:, None] >= indices[None, :]) & (block_ids[:, None] == block_ids[None, :])
    link_mask = linked[:, :, None, None]
    spread = cum_decay[:, None] - cum_decay[None, :]
    weights = jnp.where(link_mask, jnp.exp(jnp.where(link_mask, spread, 0.0)), 0.0)
    scores = jnp.einsum("tgn,sgn->tsg", readout, entries)
    within = jnp.einsum("tsg,tsgr,sgrp->tgrp", scores, weights, scaled)
    arrival = jnp.where((block_ids == last_doc)[:, None, None], jnp.exp(cum_decay), 0.0)
    carried = jnp.einsum("tgn,grpn->tgrp", readout, states) * arrival[..., None]
    end_doc = block_ids[-1]
    to_end = jnp.where(
        (block_ids == end_doc)[:, None, None], jnp.exp(cum_decay[-1] - cum_decay), 0.0
    )
    passing = jnp.where(end_doc == last_doc, jnp.exp(cum_decay[-1]), 0.0)
    fresh = jnp.einsum("sgn,sgr,sgrp->grpn", entries, to_end, scaled)
    return ((states * passing[..., None, None] + fresh, end_doc), within + carried)


def sweep_blocks(
    scaled, entries, readout, decay_logarithm, document_index, states, last_doc, block_len
):
    row_count = document_index.shape[0]
    block_count = row_count // block_len

    def in_blocks(array):
        return array.reshape((block_count, block_len) + array.shape[1:])

    inputs = tuple(
        (in_blocks(array) for array in (scaled, entries, readout, decay_logarithm, document_index))
    )
    (states, last_doc), output = lax.scan(block_step, (states, last_doc), inputs)
    return (output.reshape((row_count,) + output.shape[2:]), states)


def chain(earlier, later):
    return (earlier[0] * later[0], earlier[1] * later[0][..., None, None] + later[1])


def norm_rows(residual, gain, width):
    sums = lax.psum((jnp.sum(residual, axis=1), jnp.sum(residual * residual, axis=1)), "tp")
    row_mean = sums[0] / width
    row_var = sums[1] / width - row_mean * row_mean
    return ((residual - row_mean[:, None]) * lax.rsqrt(row_var + norm_eps)[:, None] * gain).astype(
        jnp.bfloat16
    )


def per_device(
    head_value_rows,
    entry_map_rows,
    readout_map_rows,
    output_gate_rows,
    step_before_softplus,
    sudden_log_decay,
    document_index,
    head_rate_logarithm,
    head_step_bias,
    value_conv_taps,
    entry_conv_taps,
    readout_conv_taps,
    group_norm_gain,
    mixer_output_weight,
    stream,
    mixer_norm_gain,
    channel_norm_gain,
    up_projection_weight,
    down_projection_weight,
):
    row_count = head_value_rows.shape[0]
    head_count = step_before_softplus.shape[1]
    groups = entry_map_rows.shape[1] // STATE
    per_group = head_count // groups
    value_width = head_value_rows.shape[1]
    state_width = entry_map_rows.shape[1]
    joined = jnp.concatenate([head_value_rows, entry_map_rows, readout_map_rows], axis=1)
    conv_all = jnp.concatenate(
        [value_conv_taps, entry_conv_taps, readout_conv_taps], axis=1
    ).astype(jnp.float32)
    taps = conv_all.shape[0]
    half_width = taps // 2
    extended = padded(joined, ((SP, 0),), half_width).astype(jnp.float32)
    position = lax.axis_index(SP) * row_count
    doc_pad = jnp.pad(document_index, half_width + 1, constant_values=-1)
    window_ids = lax.dynamic_slice_in_dim(doc_pad, position + 1, row_count + 2 * half_width)
    own_ids = window_ids[half_width : half_width + row_count]
    prev_id = lax.dynamic_index_in_dim(doc_pad, position + half_width, 0, keepdims=False)
    next_id = lax.dynamic_index_in_dim(
        doc_pad, position + row_count + half_width + 1, 0, keepdims=False
    )
    summed = jnp.zeros((row_count, conv_all.shape[1]), jnp.float32)
    for offset in range(taps):
        same_doc = (window_ids[offset : offset + row_count] == own_ids)[:, None]
        summed = summed + conv_all[offset] * jnp.where(
            same_doc, extended[offset : offset + row_count], 0.0
        )
    activ = jax.nn.silu(summed)
    values = activ[:, :value_width].reshape(row_count, groups, per_group, HEAD_DIM)
    entries = activ[:, value_width : value_width + state_width].reshape(row_count, groups, STATE)
    readout = activ[:, value_width + state_width :].reshape(row_count, groups, STATE)
    local_parts = []
    for sweep_direction in range(2):
        head_step_length = jax.nn.softplus(
            step_before_softplus.astype(jnp.float32) + head_step_bias[sweep_direction]
        )
        decay_logarithm = (
            -jnp.exp(head_rate_logarithm[sweep_direction]) * head_step_length + sudden_log_decay
        ).reshape(row_count, groups, per_group)
        scaled = values * head_step_length.reshape(row_count, groups, per_group)[..., None]
        arrays = (scaled, entries, readout, decay_logarithm, own_ids)
        edge_id = prev_id
        if sweep_direction == 1:
            arrays = tuple((jnp.flip(array, 0) for array in arrays))
            edge_id = next_id
        start_state = jnp.zeros((groups, per_group, HEAD_DIM, STATE), jnp.float32)
        output, end_state = sweep_blocks(*arrays, start_state, jnp.int32(-1), BLOCK)
        total_decay = jnp.sum(arrays[3], axis=0)
        passing = jnp.where(edge_id == arrays[4][-1], jnp.exp(total_decay), 0.0)
        local_parts.append((arrays, edge_id, output, end_state, passing))
    identity = (
        jnp.ones((groups, per_group), jnp.float32),
        jnp.zeros((groups, per_group, HEAD_DIM, STATE), jnp.float32),
    )
    forward_in = carried_in((local_parts[0][4], local_parts[0][3]), SP, chain, identity, False)[1]
    backward_in = carried_in((local_parts[1][4], local_parts[1][3]), SP, chain, identity, True)[1]
    summed_heads = jnp.zeros((row_count, groups, per_group, HEAD_DIM), jnp.float32)
    for sweep_direction, incoming in ((0, forward_in), (1, backward_in)):
        arrays, edge_id, output, end_state, passing = local_parts[sweep_direction]
        arrival = jnp.where(
            (arrays[4] == edge_id)[:, None, None], jnp.exp(jnp.cumsum(arrays[3], axis=0)), 0.0
        )
        carried = jnp.einsum("tgn,grpn->tgrp", arrays[2], incoming) * arrival[..., None]
        output = output + carried
        if sweep_direction == 1:
            output = jnp.flip(output, 0)
        summed_heads = summed_heads + output
    gated = summed_heads.reshape(row_count, groups, per_group * HEAD_DIM)
    gated = gated * jax.nn.silu(output_gate_rows.astype(jnp.float32)).reshape(
        row_count, groups, per_group * HEAD_DIM
    )
    gated = gated * lax.rsqrt(jnp.mean(gated * gated, axis=2, keepdims=True) + norm_eps)
    normed = (gated.reshape(row_count, value_width) * group_norm_gain).astype(jnp.bfloat16)
    partial_value = jnp.dot(normed, mixer_output_weight, preferred_element_type=jnp.float32)
    mixer_sum = sent_and_summed(partial_value.astype(jnp.bfloat16), "tp", 1)
    first_sum = resid_scale * stream.astype(jnp.float32) + mixer_sum
    normed_one = norm_rows(first_sum, mixer_norm_gain, D)
    up_full, down_full = (
        lax.all_gather(up_projection_weight, SP, axis=0, tiled=True),
        lax.all_gather(down_projection_weight, SP, axis=0, tiled=True),
    )
    hidden = jnp.dot(
        lax.all_gather(normed_one, "tp", axis=1, tiled=True),
        up_full,
        preferred_element_type=jnp.float32,
    )
    squared = jnp.square(jax.nn.relu(hidden)).astype(jnp.bfloat16)
    down_part = lax.dot_general(
        squared, down_full, (((1,), (1,)), ((), ())), preferred_element_type=jnp.float32
    )
    down_sum = lax.psum_scatter(
        down_part.astype(jnp.bfloat16), "tp", scatter_dimension=1, tiled=True
    ).astype(jnp.float32)
    second_sum = resid_scale * normed_one.astype(jnp.float32) + down_sum
    return norm_rows(second_sum, channel_norm_gain, D)


def solution(mesh):
    torus = Mesh(mesh.devices.reshape(8, 4, mesh.shape["tp"]), ("sp_0", "sp_1", "tp"))
    return jax.shard_map(
        per_device,
        mesh=torus,
        in_specs=(
            P(SP, "tp"),
            P(SP, "tp"),
            P(SP, "tp"),
            P(SP, "tp"),
            P(SP, "tp"),
            P(SP, "tp"),
            P(),
            P(None, "tp"),
            P(None, "tp"),
            P(None, "tp"),
            P(None, "tp"),
            P(None, "tp"),
            P("tp"),
            P("tp", None),
            P(SP, "tp"),
            P("tp"),
            P("tp"),
            P(SP, "tp"),
            P(SP, "tp"),
        ),
        out_specs=P(SP, "tp"),
        check_vma=False,
    )
```

profile of v0, /device:TPU:1, one launch (start us, length us, event | category | flops | bytes accessed | tf_op | source)
XLA Modules:
  0.0 508.4 jit_solution(5436518853810099621)
XLA Ops:
  10.4 4.0 collective-permute-start
  24.4 9.6 %all-reduce.5 = (bf16[16]{0:T(256)(128)(2,1)S(1)}, bf16[16]{0:T(256)(128)(2,1)S(1)}) all-reduce(bf16[16]{0:T(256)(128)(2,1)S(1)} %dynamic-update-slice.1, bf16[16]{0:T(256)(128)(2,1)S(1)} %dynamic-update-slice), channel_id=4, replica_groups=mesh['sp_0'=8,'sp_1'=4,'tp'=8] {'sp_1'}, use_global_device_ids=true, to_apply=%add.2 | all-reduce | flops 32 | bytes 128
  36.8 15.4 %all_gather.51 = bf16[8,1,4]{2,1,0:T(2,128)(2,1)S(1)} all-gather(bf16[1,1,4]{2,1,0:T(2,128)(2,1)S(1)} %get-tuple-element.271), channel_id=1, replica_groups=mesh['sp_0'=8,'sp_1'=4,'tp'=8] {'sp_0'}, dimensions={0}, use_global_device_ids=true | all-gather | bytes 72 | tf_op jit(solution)/shard_map/all_gather | solution.py:43
  54.6 10.3 %all_gather.46 = bf16[8,1,4]{2,1,0:T(2,128)(2,1)S(1)} all-gather(bf16[1,1,4]{2,1,0:T(2,128)(2,1)S(1)} %get-tuple-element.269), channel_id=1, replica_groups=mesh['sp_0'=8,'sp_1'=4,'tp'=8] {'sp_0'}, dimensions={0}, use_global_device_ids=true | all-gather | bytes 72 | tf_op jit(solution)/shard_map/all_gather | solution.py:43
  76.4 3.6 reverse.11
  80.0 3.6 reverse.12
  84.7 92.6 %while.30 = (s32[]{:T(128)}, f32[1,4,64,128]{3,2,1,0:T(8,128)S(1)}, s32[]{:T(128)}, f32[6,128,1,4,64]{1,0,4,3,2:T(8,128)S(1)}, s32[6,128]{1,0:T(8,128)}, /*index...) while((s32[]{:T(128)}, f32[1,4,64,128]{3,2,1,0:T(8,128)S(1)}, ...), condition=%wide.region_2.3_spmd.clone, body=%wide.region_0.2_spmd.clone.sunk | while | flops 29967624 | bytes 2036490 | solution.py:105
  94.4 3.3 dynamic_update_slice.11
  109.9 3.3 dynamic_update_slice.11
  125.3 3.3 dynamic_update_slice.11
  140.8 3.3 dynamic_update_slice.11
  156.2 3.3 dynamic_update_slice.11
  171.6 3.3 dynamic_update_slice.11
  183.4 64.5 %while.31 = (s32[]{:T(128)}, f32[1,4,64,128]{3,2,1,0:T(8,128)S(1)}, s32[]{:T(128)}, f32[6,128,1,4,64]{1,0,4,3,2:T(8,128)S(1)}, s32[6,128]{1,0:T(8,128)}, /*index...) while((s32[]{:T(128)}, f32[1,4,64,128]{3,2,1,0:T(8,128)S(1)}, ...), condition=%wide.region_8.9_spmd.clone, body=%wide.region_6.8_spmd.clone.sunk | while | flops 29967624 | bytes 2035982 | solution.py:105
  250.5 9.4 %all-gather.3 = bf16[4,4,64,128]{3,2,1,0:T(8,128)(2,1)S(1)} all-gather(bf16[1,4,64,128]{3,2,1,0:T(8,128)(2,1)S(1)} %convert_element_type.693), channel_id=5, replica_groups=mesh['sp_0'=8,'sp_1'=4,'tp'=8] {'sp_1'}, dimensions={0}, use_global_device_ids=true | all-gather | bytes 327680 | tf_op jit(solution)/shard_map/all_gather | solution.py:43
  260.0 19.5 %all_gather.54 = bf16[8,1,4,64,128]{4,3,2,1,0:T(8,128)(2,1)S(1)} all-gather(bf16[1,1,4,64,128]{4,3,2,1,0:T(8,128)(2,1)S(1)} %fusion.137), channel_id=1, replica_groups=mesh['sp_0'=8,'sp_1'=4,'tp'=8] {'sp_0'}, dimensions={0}, use_global_device_ids=true | all-gather | bytes 589824 | tf_op jit(solution)/shard_map/all_gather | solution.py:43
  285.4 9.4 %all-gather.1 = bf16[4,4,64,128]{3,2,1,0:T(8,128)(2,1)S(1)} all-gather(bf16[1,4,64,128]{3,2,1,0:T(8,128)(2,1)S(1)} %convert_element_type.649), channel_id=3, replica_groups=mesh['sp_0'=8,'sp_1'=4,'tp'=8] {'sp_1'}, dimensions={0}, use_global_device_ids=true | all-gather | bytes 327680 | tf_op jit(solution)/shard_map/all_gather | solution.py:43
  295.0 19.2 %all_gather.49 = bf16[8,1,4,64,128]{4,3,2,1,0:T(8,128)(2,1)S(1)} all-gather(bf16[1,1,4,64,128]{4,3,2,1,0:T(8,128)(2,1)S(1)} %fusion.170), channel_id=1, replica_groups=mesh['sp_0'=8,'sp_1'=4,'tp'=8] {'sp_0'}, dimensions={0}, use_global_device_ids=true | all-gather | bytes 589824 | tf_op jit(solution)/shard_map/all_gather | solution.py:43
  319.9 69.1 %all_to_all.5 = bf16[8,768,256]{2,1,0:T(8,128)(2,1)S(1)} all-to-all(bf16[8,768,256]{2,1,0:T(8,128)(2,1)S(1)} %bitcast.468), channel_id=1, replica_groups=mesh['sp_0'=8,'sp_1'=4,'tp'=8] {'tp'}, dimensions={0} | all-to-all | bytes 6291456 | tf_op jit(solution)/shard_map/all_to_all | solution.py:66
  390.2 13.0 %all-reduce.4 = (f32[768]{0:T(1024)S(1)}, f32[768]{0:T(1024)S(1)}) all-reduce(f32[768]{0:T(1024)S(1)} %get-tuple-element.220, f32[768]{0:T(1024)S(1)} %get-tuple-element.219), channel_id=1, replica_groups=mesh['sp_0'=8,'sp_1'=4,'tp'=8] {'tp'}, use_global_device_ids=true, to_apply=%region_17.18 | all-reduce | flops 1536 | bytes 12288 | tf_op jit(solution)/shard_map/psum | solution.py:114
  404.4 30.3 %all-gather.8.cloned.1.call-done = bf16[768,2048]{1,0:T(8,128)(2,1)} async-done(((bf16[768,256]{1,0:T(8,128)(2,1)}), bf16[768,2048]{1,0:T(8,128)(2,1)}) %all-gather.8.cloned.1.call-update) | async-done | bytes 3145744 | tf_op jit(solution)/shard_map/all_gather | solution.py:225
  434.7 11.9 %convolution_convert_fusion = bf16[768,2048]{1,0:T(8,128)(2,1)} fusion(bf16[2048,1024]{1,0:T(8,128)(2,1)} %all-gather.12.cloned.1.call-done, bf16[768,2048]{1,0:T(8,128)(2,1)} %all-gather.8.cloned.1.call-done, bf16[2048,1024]{1,0:T(8,128)(2,1)} %all-gather.10.cloned.1.call-done), kind=kOutput, calls=%fused_computation.95 | convolution fusion | flops 6446383104 | bytes 14680064 | tf_op jit(solution)/shard_map/dot_general | solution.py:230
  446.7 36.7 %reduce-scatter.2.cloned.1.call-done = bf16[768,256]{1,0:T(8,128)(2,1)} async-done(((bf16[768,2048]{1,0:T(8,128)(2,1)}), bf16[768,256]{1,0:T(8,128)(2,1)}) %reduce-scatter.2.cloned.1.call-update) | async-done | bytes 393232 | tf_op jit(solution)/shard_map/reduce_scatter | solution.py:233
  484.6 15.2 %all-reduce.3 = (f32[768]{0:T(1024)S(1)}, f32[768]{0:T(1024)S(1)}) all-reduce(f32[768]{0:T(1024)S(1)} %get-tuple-element.222, f32[768]{0:T(1024)S(1)} %get-tuple-element.221), channel_id=1, replica_groups=mesh['sp_0'=8,'sp_1'=4,'tp'=8] {'tp'}, use_global_device_ids=true, to_apply=%region_22.23 | all-reduce | flops 1536 | bytes 12288 | tf_op jit(solution)/shard_map/psum | solution.py:114
  (420 shorter events, 175.0 us)
Async XLA Ops:
  6.5 312.0 %copy-start = (bf16[256,2048]{1,0:T(8,128)(2,1)S(1)}, bf16[256,2048]{1,0:T(8,128)(2,1)}, u32[]{:S(2)}) copy-start(bf16[256,2048]{1,0:T(8,128)(2,1)} %param.36) | copy-start | bytes 3145732
  6.6 63.4 %copy-start.17 = (bf16[5,256]{1,0:T(8,128)(2,1)S(1)}, bf16[5,256]{1,0:T(8,128)(2,1)}, u32[]{:S(2)}) copy-start(bf16[5,256]{1,0:T(8,128)(2,1)} %param.32) | copy-start | bytes 7684
  6.6 63.4 %copy-start.31 = (bf16[5,128]{1,0:T(8,128)(2,1)S(1)}, bf16[5,128]{1,0:T(8,128)(2,1)}, u32[]{:S(2)}) copy-start(bf16[5,128]{1,0:T(8,128)(2,1)} %param.33) | copy-start | bytes 3844
  6.6 63.4 %copy-start.30 = (bf16[5,128]{1,0:T(8,128)(2,1)S(1)}, bf16[5,128]{1,0:T(8,128)(2,1)}, u32[]{:S(2)}) copy-start(bf16[5,128]{1,0:T(8,128)(2,1)} %param.34) | copy-start | bytes 3844
  6.6 397.8 %all-gather.10.cloned.1.call-start = ((), (), s32[]{:S(2)}) async-start(), calls=%async_computation.3 | async-start | bytes 4325376 | tf_op jit(solution)/shard_map/all_gather | solution.py:221
  7.3 397.1 %all-gather.12.cloned.1.call-start = ((), (), s32[]{:S(2)}) async-start(), calls=%async_computation.4 | async-start | bytes 4325376 | tf_op jit(solution)/shard_map/all_gather | solution.py:222
  10.4 61.5 %collective-permute-start = (bf16[2,512]{1,0:T(2,128)(2,1)S(1)}, bf16[2,512]{1,0:T(2,128)(2,1)S(1)}, u32[]{:S(2)}, u32[]{:S(2)}) collective-permute-start(bf16[2,512]{1,0:T(2,128)(2,1)S(1)} %get-tuple-element.284), channel_id=1, source_target_pairs={{0,8},{8,16},{16,24},{24,32},{32,40},{40,48},{48,56},{56,64},{64,7... | collective-permute-start | bytes 6152 | tf_op jit(solution)/shard_map/ppermute | solution.py:23
  14.4 57.5 %collective-permute-start.1 = (bf16[2,512]{1,0:T(2,128)(2,1)S(1)}, bf16[2,512]{1,0:T(2,128)(2,1)S(1)}, u32[]{:S(2)}, u32[]{:S(2)}) collective-permute-start(bf16[2,512]{1,0:T(2,128)(2,1)S(1)} %get-tuple-element.285), channel_id=1, source_target_pairs={{8,0},{16,8},{24,16},{32,24},{40,32},{48,40},{56,48},{64,56},{72,6... | collective-permute-start | bytes 6152 | tf_op jit(solution)/shard_map/ppermute | solution.py:26
  15.7 419.0 %all-gather.8.cloned.1.call-start = ((), (), s32[]{:S(2)}) async-start(), calls=%async_computation.2 | async-start | bytes 3538944 | tf_op jit(solution)/shard_map/all_gather | solution.py:225
  249.4 30.1 %copy-start.10 = (f32[768,4]{0,1:T(4,128)S(1)}, f32[768,4]{0,1:T(4,128)}, u32[]{:S(2)}) copy-start(f32[768,4]{0,1:T(4,128)} %select_bitcast_fusion) | copy-start | bytes 36868
  249.4 30.1 %copy-start.37 = (f32[4]{0:T(128)S(1)}, f32[4]{0:T(128)}, u32[]{:S(2)}) copy-start(f32[4]{0:T(128)} %get-tuple-element.313) | copy-start | bytes 52
  282.2 32.0 %copy-start.8 = (f32[768,4]{0,1:T(4,128)S(1)}, f32[768,4]{0,1:T(4,128)}, u32[]{:S(2)}) copy-start(f32[768,4]{0,1:T(4,128)} %select_bitcast_fusion.1) | copy-start | bytes 36868
  282.2 32.0 %copy-start.18 = (f32[4]{0:T(128)S(1)}, f32[4]{0:T(128)}, u32[]{:S(2)}) copy-start(f32[4]{0:T(128)} %get-tuple-element.299) | copy-start | bytes 52
  282.2 32.0 %copy-start.19 = (f32[4]{0:T(128)S(1)}, f32[4]{0:T(128)}, u32[]{:S(2)}) copy-start(f32[4]{0:T(128)} %get-tuple-element.300) | copy-start | bytes 52
  282.2 32.0 %copy-start.20 = (f32[4]{0:T(128)S(1)}, f32[4]{0:T(128)}, u32[]{:S(2)}) copy-start(f32[4]{0:T(128)} %get-tuple-element.301) | copy-start | bytes 52
  282.2 32.0 %copy-start.21 = (f32[4]{0:T(128)S(1)}, f32[4]{0:T(128)}, u32[]{:S(2)}) copy-start(f32[4]{0:T(128)} %get-tuple-element.302) | copy-start | bytes 52
  282.2 32.0 %copy-start.22 = (f32[4]{0:T(128)S(1)}, f32[4]{0:T(128)}, u32[]{:S(2)}) copy-start(f32[4]{0:T(128)} %get-tuple-element.303) | copy-start | bytes 52
  282.2 32.0 %copy-start.23 = (f32[4]{0:T(128)S(1)}, f32[4]{0:T(128)}, u32[]{:S(2)}) copy-start(f32[4]{0:T(128)} %get-tuple-element.304) | copy-start | bytes 52
  282.2 32.0 %copy-start.24 = (f32[4]{0:T(128)S(1)}, f32[4]{0:T(128)}, u32[]{:S(2)}) copy-start(f32[4]{0:T(128)} %get-tuple-element.305) | copy-start | bytes 52
  282.3 32.0 %copy-start.25 = (f32[4]{0:T(128)S(1)}, f32[4]{0:T(128)}, u32[]{:S(2)}) copy-start(f32[4]{0:T(128)} %get-tuple-element.326) | copy-start | bytes 52
  282.3 32.0 %copy-start.36 = (f32[4]{0:T(128)S(1)}, f32[4]{0:T(128)}, u32[]{:S(2)}) copy-start(f32[4]{0:T(128)} %fusion.271) | copy-start | bytes 52
  404.3 79.0 %reduce-scatter.2.cloned.1.call-start = ((), (), s32[]{:S(2)}) async-start(), calls=%async_computation.5 | async-start | bytes 3538944 | tf_op jit(solution)/shard_map/reduce_scatter | solution.py:233
  446.6 36.7 %copy-start.1 = (bf16[768,256]{1,0:T(8,128)(2,1)S(1)}, bf16[768,256]{1,0:T(8,128)(2,1)}, u32[]{:S(2)}) copy-start(bf16[768,256]{1,0:T(8,128)(2,1)} %multiply_convert_fusion.2) | copy-start | bytes 1179652
  446.6 53.3 %copy-start.35 = (f32[256]{0:T(256)S(1)}, f32[256]{0:T(256)}, u32[]{:S(2)}) copy-start(f32[256]{0:T(256)} %param.39) | copy-start | bytes 3076
  (30 other events, 452.1 us)
Sparse Core Ops, SparseCore 0:
  10.0 81.9 all-gather.9
  94.6 78.7 all-gather.11
  404.5 30.2 all-gather.7
  446.8 36.4 reduce-scatter.1
where the time goes:
time: 515 us; the launch traced here: 508 us
  blocking collectives  190 us (37%)
  local copies, waits for them, and re-layouts  111 us (22%)
  waiting for transfers between devices  67.7 us (13%)
  matrix products  58.9 us (11%)
  other arithmetic  41.6 us (8%)
  between operations  17.2 us (3%)
  loops' own time  16.1 us (3%)
  starting transfers between devices  5.47 us (1%)
    all_gather x6, blocking collectives, carried_in(): lax.all_gather(part.astype(kind), axis)  83.1 us
    all_to_all x1, blocking collectives, sent_and_summed(): lax.all_to_all(blocks, axis, split_axis=0, concat_axis=0, tiled=True)  69.1 us
    reduce_scatter x1, waiting for transfers between devices, per_device(): lax.psum_scatter(down_part.astype(jnp.bfloat16), 'tp', scatter_dimension=...  36.7 us
    dynamic_update_slice x12, local copies, waits for them, and re-layouts, sweep_blocks(): lax.scan(block_step, (states, last_doc), inputs)  35.4 us
    all_gather x1, waiting for transfers between devices, per_device(): lax.all_gather(normed_one, 'tp', axis=1, tiled=True)  30.3 us
    psum x2, blocking collectives, norm_rows(): lax.psum((jnp.sum(residual, axis=1), jnp.sum(residual * residual, axis=1)...  28.3 us
    dynamic_slice x24, local copies, waits for them, and re-layouts, sweep_blocks(): lax.scan(block_step, (states, last_doc), inputs)  26.6 us
    another operation x2, loops' own time, sweep_blocks(): lax.scan(block_step, (states, last_doc), inputs)  16.1 us
  transfers between devices with their start and end apart: 6, of which 2 were waited for; matrix products, arithmetic and copies ran while one was open for 38% of the time, Pallas kernels for 0%

commit v1 on v0

v1 whole, which is shorter than its diff:
```python
import jax
import jax.numpy as jnp
from jax import lax
from jax.experimental import pallas as pl
from jax.experimental.pallas import tpu as pltpu
from jax.sharding import Mesh
from jax.sharding import PartitionSpec as P

EPS = 1e-05
RES = 1.4142135623730951
SP = ("z", "y")
TP = ("x", "c")
ROWS = 768
HALF = 384
TILE = 256
TILES = ROWS // TILE
HI = lax.Precision.HIGHEST
F32 = jnp.float32
BF = jnp.bfloat16


def vm():
    return pl.BlockSpec(memory_space=pltpu.VMEM)


def sm():
    return pl.BlockSpec(memory_space=pltpu.SMEM)


def call(body, ins, outs, scratch=(), scalars=0, name=None, flops=0):
    return pl.pallas_call(
        body,
        in_specs=[sm()] * scalars + [vm()] * (ins - scalars),
        out_specs=[vm()] * len(outs),
        out_shape=[jax.ShapeDtypeStruct(s, d) for s, d in outs],
        scratch_shapes=list(scratch),
        name=name,
        cost_estimate=pl.CostEstimate(flops=flops, bytes_accessed=1000000, transcendentals=0),
    )


def iota(shape, dim):
    return lax.broadcasted_iota(jnp.int32, shape, dim)


def dot(a, b, ca, cb, precision=None):
    return lax.dot_general(
        a, b, (((ca,), (cb,)), ((), ())), precision=precision, preferred_element_type=F32
    )


def head_spread():
    return (iota((8, 512), 1) // 64 == iota((8, 512), 0)).astype(F32)


def conv_body(
    sp, rate, bias, v, e, r, lo, hi, tv, te, tr, step, sudden, doc,
    x_out, b_out, c_out, cum_out, dt_out, ct_out, dev_out, doc_out, si_out, pay_out, ext,
):
    base = sp[0] * 6
    rows = [doc[pl.ds(jnp.maximum(base - 1, 0), 1), :]]
    rows += [doc[pl.ds(base + k, 1), :] for k in range(6)]
    rows += [doc[pl.ds(jnp.minimum(base + 6, 191), 1), :]]
    lane = iota((1, 128), 1)
    first = jnp.where(sp[0] == 0, -1, rows[0])
    last = jnp.where(sp[0] == 31, -1, rows[7])
    window = jnp.concatenate([first] + rows[1:7] + [last], axis=1)
    own = window[:, 128:896]
    masks = []
    for d in range(-2, 3):
        moved = window if d == 0 else pltpu.roll(window, (-d) % 1024, 1)
        masks.append((moved[:, 128:896] == own).astype(F32))
    zero = jnp.zeros((1, ROWS), F32)
    mask_cols = jnp.transpose(jnp.concatenate(masks + [zero] * 3, axis=0))
    ext[8:776, 0:256] = v[...].astype(F32)
    ext[8:776, 256:384] = e[...].astype(F32)
    ext[8:776, 384:512] = r[...].astype(F32)
    ext[6:8, :] = lo[...].astype(F32)
    ext[776:778, :] = hi[...].astype(F32)
    taps = jnp.concatenate([tv[...], te[...], tr[...]], axis=1).astype(F32)
    acc = jnp.zeros((ROWS, 512), F32)
    for d in range(5):
        acc = acc + taps[d : d + 1, :] * (mask_cols[:, d : d + 1] * ext[6 + d : 6 + d + ROWS, :])
    act = acc * jax.nn.sigmoid(acc)
    x = act[:, 0:256]
    b = act[:, 256:384].astype(BF)
    x_out[...] = x.astype(BF)
    b_out[...] = b
    c_out[...] = act[:, 384:512].astype(BF)

    row = iota((8, 1), 0)
    fwd = row < 4
    rate_col = jnp.zeros((8, 1), F32)
    bias_col = jnp.zeros((8, 1), F32)
    for k in range(8):
        rate_col = jnp.where(row == k, rate[k // 4, k % 4], rate_col)
        bias_col = jnp.where(row == k, bias[k // 4, k % 4], bias_col)
    pick = (iota((8, 4), 0) % 4 == iota((8, 4), 1)).astype(F32)
    raw = dot(pick, step[...].astype(F32), 1, 1, HI) + bias_col
    dt = jnp.maximum(raw, 0.0) + jnp.log1p(jnp.exp(-jnp.abs(raw)))
    ld = -jnp.exp(rate_col) * dt + dot(pick, sudden[...], 1, 1, HI)
    dt_out[...] = dt
    dev = own.astype(F32)
    doc_out[...] = jnp.broadcast_to(dev, (8, ROWS))
    prev_id = window[:, 127:128].astype(F32)
    next_id = window[:, 896:897].astype(F32)
    upper = (iota((TILE, TILE), 0) <= iota((TILE, TILE), 1)).astype(F32)
    spread = head_spread()
    inc, exc, tot, dl, df = [], [], [], [], []
    for i in range(TILES):
        part = ld[:, i * TILE : (i + 1) * TILE]
        c = dot(part, upper, 1, 0, HI)
        inc.append(c)
        exc.append(c - part)
        tot.append(c[:, TILE - 1 : TILE])
        dl.append(dev[:, (i + 1) * TILE - 1 : (i + 1) * TILE])
        df.append(dev[:, i * TILE : i * TILE + 1])
    before = [prev_id, dl[0], dl[1]]
    after = [df[1], df[2], next_id]
    states, passing = [], []
    for i in range(TILES):
        ids = dev[:, i * TILE : (i + 1) * TILE]
        cols = slice(i * TILE, (i + 1) * TILE)
        cum_out[:, cols] = jnp.where(fwd, inc[i], exc[i])
        keep = ids == jnp.where(fwd, dl[i], df[i])
        weight = jnp.where(keep, dt[:, cols] * jnp.exp(jnp.where(fwd, tot[i] - inc[i], exc[i])), 0.0)
        wide = dot(weight, spread, 0, 0, HI)
        xi = x[i * TILE : (i + 1) * TILE, :]
        scaled = (jnp.concatenate([xi, xi], axis=1) * wide).astype(BF)
        states.append(dot(b[i * TILE : (i + 1) * TILE, :], scaled, 0, 0))
        reach = jnp.where(fwd, inc[i], tot[i] - exc[i])
        edge = jnp.where(fwd, before[i], after[i])
        ct_out[:, cols] = jnp.where(ids == edge, jnp.exp(reach), 0.0)
        far = jnp.where(fwd, sum(tot[:i], jnp.zeros((8, 1), F32)), sum(tot[i + 1 :], jnp.zeros((8, 1), F32)))
        dev_out[:, cols] = jnp.where(ids == jnp.where(fwd, prev_id, next_id), jnp.exp(reach + far), 0.0)
        through = jnp.where(jnp.where(fwd, dl[i], df[i]) == edge, jnp.exp(tot[i]), 0.0)
        passing.append(jnp.sum(through * spread, axis=0, keepdims=True))
    f = [s[:, 0:256] for s in states]
    g = [s[:, 256:512] for s in states]
    pf = [q[:, 0:256] for q in passing]
    pg = [q[:, 256:512] for q in passing]
    f2 = f[1] + pf[1] * f[0]
    g0 = g[1] + pg[1] * g[2]
    si_out[0] = f[0].astype(BF)
    si_out[1] = f2.astype(BF)
    si_out[2] = g0.astype(BF)
    si_out[3] = g[2].astype(BF)
    pay_out[0:128, 0:256] = (f[2] + pf[2] * f2).astype(BF)
    pay_out[0:128, 256:512] = (g[0] + pg[0] * g0).astype(BF)
    whole = passing[0] * passing[1] * passing[2]
    pay_out[128:144, :] = jnp.broadcast_to(whole, (16, 512)).astype(BF)


def local_body(x, b, c, cum, dt, ct, doc, si, y_out):
    spread = head_spread()
    lower = iota((TILE, TILE), 0) > iota((TILE, TILE), 1)
    upper = iota((TILE, TILE), 0) < iota((TILE, TILE), 1)
    side = iota((TILE, 128), 1) < 64
    for i in range(TILES):
        cols = slice(i * TILE, (i + 1) * TILE)
        cc = c[cols, :]
        score = dot(cc, b[cols, :], 1, 1)
        cum_row = cum[:, cols]
        cum_col = jnp.transpose(cum_row)
        ids = doc[:, cols]
        same = ids[0:1, :] == jnp.transpose(ids)[:, 0:1]
        score = jnp.where(same, score, 0.0)
        steps = dt[:, cols]
        carried = dot(ct[:, cols], spread, 0, 0, HI)
        for pair in range(2):
            xp = x[cols, pair * 128 : pair * 128 + 128]
            got = []
            for h in (2 * pair, 2 * pair + 1):
                spread_f = cum_col[:, h : h + 1] - cum_row[h : h + 1, :]
                spread_b = cum_row[h + 4 : h + 5, :] - cum_col[:, h + 4 : h + 5]
                reach = jnp.exp(jnp.where(upper, spread_b, spread_f))
                d0 = steps[h : h + 1, :]
                d1 = steps[h + 4 : h + 5, :]
                amount = jnp.where(lower, d0, jnp.where(upper, d1, d0 + d1))
                got.append(dot((score * (reach * amount)).astype(BF), xp, 1, 0))
            part = jnp.where(side, got[0], got[1])
            lanes = slice(pair * 128, pair * 128 + 128)
            wide = slice(256 + pair * 128, 384 + pair * 128)
            if i > 0:
                part = part + dot(cc, si[i - 1][:, lanes], 1, 0) * carried[:, lanes]
            if i < TILES - 1:
                part = part + dot(cc, si[i + 2][:, lanes], 1, 0) * carried[:, wide]
            y_out[cols, lanes] = part


def chain_body(where_y, pay, send_f, send_b, pre_out):
    y = where_y[0]
    for lanes, order, out in ((slice(0, 256), range(4), send_f), (slice(256, 512), range(3, -1, -1), send_b)):
        state = jnp.zeros((128, 256), F32)
        through = jnp.ones((1, 256), F32)
        pre, pre_through = state, through
        for k in order:
            pre = jnp.where(y == k, state, pre)
            pre_through = jnp.where(y == k, through, pre_through)
            hop = pay[k, 128:144, lanes].astype(F32)[0:1, :]
            state = state * hop + pay[k, 0:128, lanes].astype(F32)
            through = through * hop
        out[0:128, :] = state.astype(BF)
        out[128:144, :] = jnp.broadcast_to(through, (16, 256)).astype(BF)
        pre_out[0:128, lanes] = pre
        pre_out[128:136, lanes] = jnp.broadcast_to(pre_through, (8, 256))


def gate_body(core, yl, c, dev, pre, f1, f2, b1, b2, gate, gain, keep, send, normed):
    spread = head_spread()
    states = []
    for lanes, near, far in ((slice(0, 256), f1, f2), (slice(256, 512), b1, b2)):
        more = near[128:144, :].astype(F32)[0:1, :] * far[0:128, :].astype(F32)
        come = near[0:128, :].astype(F32) + more
        states.append((pre[0:128, lanes] + pre[128:129, lanes] * come).astype(BF))
    for i in range(TILES):
        cols = slice(i * TILE, (i + 1) * TILE)
        wide = dot(dev[:, cols], spread, 0, 0, HI)
        y = yl[cols, :]
        y = y + dot(c[cols, :], states[0], 1, 0) * wide[:, 0:256]
        y = y + dot(c[cols, :], states[1], 1, 0) * wide[:, 256:512]
        z = gate[cols, :].astype(F32)
        y = y * (z * jax.nn.sigmoid(z))
        y = y * lax.rsqrt(jnp.mean(y * y, axis=1, keepdims=True) + EPS)
        normed[cols, :] = (y * gain[...]).astype(BF)
    mine = pl.multiple_of(core[0] * HALF, HALF)
    other = pl.multiple_of(HALF - core[0] * HALF, HALF)
    keep[...] = normed[pl.ds(mine, HALF), :]
    send[...] = normed[pl.ds(other, HALF), :]


def mix_body(where_x, a, b, wa, wb, o0, o1, o2, o3):
    for k, out in ((2, o2), (1, o1), (3, o3), (0, o0)):
        block = pl.multiple_of(((where_x[0] + k) % 4) * 512, 512)
        got = dot(a[...], wa[:, pl.ds(block, 512)], 1, 0)
        got = got + dot(b[...], wb[:, pl.ds(block, 512)], 1, 0)
        out[...] = got.astype(BF)


def first_body(core, own, stream_a, stream_b, r1, r2, r3, gain_a, gain_b, out, total, gain):
    lane_a = pl.multiple_of(core[0] * 256, 256)
    lane_b = pl.multiple_of(256 - core[0] * 256, 256)
    total[:, pl.ds(lane_a, 256)] = stream_a[...].astype(F32)
    total[:, pl.ds(lane_b, 256)] = stream_b[...].astype(F32)
    gain[0:1, pl.ds(lane_a, 256)] = gain_a[0:1, :]
    gain[0:1, pl.ds(lane_b, 256)] = gain_b[0:1, :]
    mix = own[...].astype(F32) + r1[...].astype(F32) + r2[...].astype(F32) + r3[...].astype(F32)
    first = RES * total[...] + mix
    mean = jnp.mean(first, axis=1, keepdims=True).astype(BF).astype(F32)
    out[0:HALF, :] = (first - mean).astype(BF)
    means = jnp.transpose(jnp.broadcast_to(mean, (HALF, 128)))[0:1, :]
    means = jnp.concatenate([means, jnp.zeros((1, 128), F32)], axis=1)
    g = gain[0:1, :]
    g0 = g.astype(BF).astype(F32)
    g1 = (g - g0).astype(BF).astype(F32)
    g2 = g - g0 - g1
    row = iota((16, 512), 0)
    tail = jnp.where(row == 0, means, jnp.where(row == 1, g0, jnp.where(row == 2, g1, jnp.where(row == 3, g2, 0.0))))
    out[HALF : HALF + 16, :] = tail.astype(BF)


def up_body(where_x, p0, p1, p2, p3, w, hidden, resid, xn):
    @pl.when(pl.program_id(0) == 0)
    def _():
        blocks = (p0, p1, p2, p3)
        tails = [p[HALF : HALF + 16, :].astype(F32) for p in blocks]
        means = jnp.concatenate([t[0:1, 0:HALF] for t in tails] + [jnp.zeros((4, HALF), F32)], axis=0)
        mean_cols = jnp.transpose(means)
        full = [p[0:HALF, :].astype(F32) + mean_cols[:, k : k + 1] for k, p in enumerate(blocks)]
        m = sum(jnp.sum(q, axis=1, keepdims=True) for q in full) / 2048.0
        full = [q - m for q in full]
        v = sum(jnp.sum(q * q, axis=1, keepdims=True) for q in full) / 2048.0
        scale = lax.rsqrt(v + EPS)
        for k, q in enumerate(full):
            gain = tails[k][1:2, :] + tails[k][2:3, :] + tails[k][3:4, :]
            done = (q * scale * gain).astype(BF)
            block = pl.multiple_of(((where_x[0] + (4 - k)) % 4) * 512, 512)
            xn[:, pl.ds(block, 512)] = done
            if k == 0:
                resid[...] = done

    got = dot(xn[...], w[...].reshape(2048, 512), 1, 0)
    got = jnp.maximum(got, 0.0)
    hidden[...] = (got * got).astype(BF)


def down_body(where_x, h, w, out, acc):
    got = dot(h[...], w[...].reshape(512, 1024), 1, 1)

    @pl.when(pl.program_id(0) == 0)
    def _():
        acc[...] = got

    @pl.when(pl.program_id(0) == 1)
    def _():
        out[...] = (acc[...] + got).astype(BF)


def second_body(resid, own, r1, r2, r3, second, stats):
    total = own[...].astype(F32) + r1[...].astype(F32) + r2[...].astype(F32) + r3[...].astype(F32)
    total = RES * resid[...].astype(F32) + total
    second[...] = total
    s1 = jnp.transpose(jnp.broadcast_to(jnp.sum(total, axis=1, keepdims=True), (HALF, 128)))[0:8, :]
    s2 = jnp.transpose(jnp.broadcast_to(jnp.sum(total * total, axis=1, keepdims=True), (HALF, 128)))[0:8, :]
    stats[...] = jnp.where(iota((8, HALF), 0) == 0, s1, s2)


def last_body(core, second, s0, s1, s2, s3, gain_a, gain_b, keep, send):
    stats = s0[...] + s1[...] + s2[...] + s3[...]
    cols = jnp.transpose(stats)
    m = cols[:, 0:1] / 2048.0
    v = cols[:, 1:2] / 2048.0 - m * m
    scale = lax.rsqrt(v + EPS)
    for off, gain, out in ((core[0], gain_a, keep), (1 - core[0], gain_b, send)):
        lanes = pl.multiple_of(off * 256, 256)
        out[...] = ((second[:, pl.ds(lanes, 256)] - m) * scale * gain[1:2, :]).astype(BF)


def per_device(
    head_value_rows,
    entry_map_rows,
    readout_map_rows,
    output_gate_rows,
    step_before_softplus,
    sudden_log_decay,
    document_index,
    head_rate_logarithm,
    head_step_bias,
    value_conv_taps,
    entry_conv_taps,
    readout_conv_taps,
    group_norm_gain,
    mixer_output_weight,
    stream,
    mixer_norm_gain,
    channel_norm_gain,
    up_projection_weight,
    down_projection_weight,
):
    core = lax.axis_index("c")
    at_x = jnp.reshape(lax.axis_index("x"), (1,))
    at_c = jnp.reshape(core, (1,))
    at_y = jnp.reshape(lax.axis_index("y"), (1,))
    at_sp = jnp.reshape(lax.axis_index(SP), (1,))
    swap = [(0, 1), (1, 0)]

    def shift(a, axis, by, count):
        return lax.ppermute(a, axis, [(i, i + by) for i in range(count) if 0 <= i + by < count])

    def around(a, by):
        return lax.ppermute(a, "x", [(i, (i + by) % 4) for i in range(4)])

    tail = jnp.concatenate([a[ROWS - 2 :] for a in (head_value_rows, entry_map_rows, readout_map_rows)], axis=1)
    head = jnp.concatenate([a[:2] for a in (head_value_rows, entry_map_rows, readout_map_rows)], axis=1)
    low = shift(tail, SP, 1, 32)
    high = shift(head, SP, -1, 32)

    weights = jnp.concatenate([up_projection_weight, down_projection_weight], axis=1)
    weights = lax.all_gather(weights, ("z", "y", "c"), axis=0, tiled=True).reshape(32, 2, 64, 2048)

    weight_other = lax.ppermute(mixer_output_weight, "c", swap)
    stream_mine = lax.dynamic_slice_in_dim(stream, core * HALF, HALF)
    stream_other = lax.ppermute(lax.dynamic_slice_in_dim(stream, (1 - core) * HALF, HALF), "c", swap)
    gains = jnp.stack([mixer_norm_gain, channel_norm_gain])
    gains_other = lax.ppermute(gains, "c", swap)

    x, b, c, cum, dt, ct, dev, doc, si, pay = call(
        conv_body,
        14,
        [((ROWS, 256), BF), ((ROWS, 128), BF), ((ROWS, 128), BF)]
        + [((8, ROWS), F32)] * 5
        + [((4, 128, 256), BF), ((144, 512), BF)],
        scratch=[pltpu.VMEM((784, 512), F32)],
        scalars=3,
        name="conv_states",
        flops=10**9,
    )(
        at_sp, head_rate_logarithm, head_step_bias, head_value_rows, entry_map_rows, readout_map_rows,
        low, high, value_conv_taps, entry_conv_taps, readout_conv_taps, step_before_softplus,
        sudden_log_decay, document_index.reshape(192, 128),
    )
    rows = lax.all_gather(pay, "y")
    send_f, send_b, pre = call(
        chain_body, 2, [((144, 256), BF), ((144, 256), BF), ((136, 512), F32)], scalars=1, name="chain", flops=10**8
    )(at_y, rows)
    f1, f2 = shift(send_f, "z", 1, 8), shift(send_f, "z", 2, 8)
    b1, b2 = shift(send_b, "z", -1, 8), shift(send_b, "z", -2, 8)
    yl = call(local_body, 8, [((ROWS, 256), F32)], name="local", flops=2 * 10**9)(x, b, c, cum, dt, ct, doc, si)[0]
    keep, send = call(
        gate_body, 11, [((HALF, 256), BF)] * 2, scratch=[pltpu.VMEM((ROWS, 256), BF)], scalars=1, name="gate", flops=10**9
    )(at_c, yl, c, dev, pre, f1, f2, b1, b2, output_gate_rows, group_norm_gain.reshape(1, 256))
    other = lax.ppermute(send, "c", swap)
    o0, o1, o2, o3 = call(mix_body, 5, [((HALF, 512), BF)] * 4, scalars=1, name="mix", flops=10**9)(
        at_x, keep, other, mixer_output_weight, weight_other
    )
    r2, r1, r3 = around(o2, 2), around(o1, 1), around(o3, 3)
    p0 = call(
        first_body,
        9,
        [((HALF + 16, 512), BF)],
        scratch=[pltpu.VMEM((HALF, 512), F32), pltpu.VMEM((8, 512), F32)],
        scalars=1,
        name="first",
        flops=10**8,
    )(at_c, o0, stream_mine, stream_other, r1, r2, r3, gains, gains_other)[0]
    p2, p1, p3 = around(p0, 2), around(p0, 1), around(p0, 3)
    fixed = pl.BlockSpec((HALF + 16, 512), lambda s, _: (0, 0))
    hidden, resid = pl.pallas_call(
        up_body,
        grid_spec=pltpu.PrefetchScalarGridSpec(
            num_scalar_prefetch=1,
            grid=(4,),
            in_specs=[fixed] * 4 + [pl.BlockSpec((32, 1, 64, 512), lambda s, _: (0, s // 2, 0, s % 2))],
            out_specs=[
                pl.BlockSpec((HALF, 512), lambda s, _: (0, s)),
                pl.BlockSpec((HALF, 512), lambda s, _: (0, 0)),
            ],
            scratch_shapes=[pltpu.VMEM((HALF, 2048), BF)],
        ),
        out_shape=[jax.ShapeDtypeStruct((HALF, 2048), BF), jax.ShapeDtypeStruct((HALF, 512), BF)],
        name="up",
        cost_estimate=pl.CostEstimate(flops=3 * 10**9, bytes_accessed=10**7, transcendentals=0),
    )(at_x, p0, p1, p2, p3, weights)

    def down(k):
        return pl.pallas_call(
            down_body,
            grid_spec=pltpu.PrefetchScalarGridSpec(
                num_scalar_prefetch=1,
                grid=(2,),
                in_specs=[
                    pl.BlockSpec((HALF, 1024), lambda s, _: (0, s)),
                    pl.BlockSpec((8, 1, 64, 1024), lambda s, at: ((at[0] + k) % 4, s, 0, 1)),
                ],
                out_specs=pl.BlockSpec((HALF, 512), lambda s, _: (0, 0)),
                scratch_shapes=[pltpu.VMEM((HALF, 512), F32)],
            ),
            out_shape=jax.ShapeDtypeStruct((HALF, 512), BF),
            name="down",
            cost_estimate=pl.CostEstimate(flops=8 * 10**8, bytes_accessed=3 * 10**6, transcendentals=0),
        )(at_x, hidden, weights)

    d2, d1, d3, d0 = down(2), down(1), down(3), down(0)
    q2, q1, q3 = around(d2, 2), around(d1, 1), around(d3, 3)
    second, stats = call(second_body, 5, [((HALF, 512), F32), ((8, HALF), F32)], name="second", flops=10**8)(
        resid, d0, q1, q2, q3
    )
    s1, s2, s3 = around(stats, 1), around(stats, 2), around(stats, 3)
    keep, send = call(last_body, 8, [((HALF, 256), BF)] * 2, scalars=1, name="last", flops=10**8)(
        at_c, second, stats, s1, s2, s3, gains, gains_other
    )
    got = lax.ppermute(send, "c", swap)
    lower = core == 0
    return jnp.concatenate([jnp.where(lower, keep, got), jnp.where(lower, got, keep)], axis=0)


def solution(mesh):
    torus = Mesh(mesh.devices.reshape(8, 4, 4, 2), ("z", "y", "x", "c"))
    return jax.shard_map(
        per_device,
        mesh=torus,
        in_specs=(
            P(SP, TP),
            P(SP, TP),
            P(SP, TP),
            P(SP, TP),
            P(SP, TP),
            P(SP, TP),
            P(),
            P(None, TP),
            P(None, TP),
            P(None, TP),
            P(None, TP),
            P(None, TP),
            P(TP),
            P(TP, None),
            P(SP, TP),
            P(TP),
            P(TP),
            P(SP, TP),
            P(SP, TP),
        ),
        out_specs=P(SP, TP),
        check_vma=False,
    )
```

time: 515 us -> 193 us (0.37)
  blocking collectives: 190 us -> 16.2 us
  local copies, waits for them, and re-layouts: 111 us -> 10.7 us
  matrix products: 58.9 us -> 0 us
  Pallas kernels: 0 us -> 51.1 us
  starting transfers between devices: 5.47 us -> 44.6 us
  other arithmetic: 41.6 us -> 3.48 us
  loops' own time: 16.1 us -> 0 us
  waiting for transfers between devices: 67.7 us -> 51.6 us
    all_to_all x1 -> x0, blocking collectives: 69.1 us -> none  [sent_and_summed(): lax.all_to_all(blocks, axis, split_axis=0, concat_axis=0, tiled=True)]
    all_gather x6 -> x1, blocking collectives: 83.1 us -> 16.2 us  [per_device(): rows = lax.all_gather(pay, 'y')]
    dot_general x52 -> x0, matrix products: 58.9 us -> none  [the longest x12 12.3 us: block_step(): within = jnp.einsum('tsg,tsgr,sgrp->tgrp', scores, weights, scaled)]
    ppermute x2 -> x23, waiting for transfers between devices: 0.01 us -> 51.6 us  [the longest x12 47.3 us: around(): return lax.ppermute(a, 'x', [(i, (i + by) % 4) for i in range(4)])]
    pallas_call x0 -> x13, Pallas kernels: none -> 51.1 us  [the longest x4 14.3 us: down(): pl.pallas_call(down_body, grid_spec=pltpu.PrefetchScalarGridSpec(num_scal...]
    ppermute x2 -> x23, starting transfers between devices: 5.31 us -> 44.6 us  [the longest x12 16.8 us: around(): return lax.ppermute(a, 'x', [(i, (i + by) % 4) for i in range(4)])]
    reduce_scatter x1 -> x0, waiting for transfers between devices: 36.7 us -> none  [per_device(): lax.psum_scatter(down_part.astype(jnp.bfloat16), 'tp', scatter_dimension=...]
    dynamic_update_slice x12 -> x0, local copies, waits for them, and re-layouts: 35.4 us -> none  [sweep_blocks(): lax.scan(block_step, (states, last_doc), inputs)]
  transfers between devices with their start and end apart: 6 -> 24, of which waited for: 2 -> 13; matrix products, arithmetic and copies ran while one was open for 38% -> 3% of each run, Pallas kernels for 0% -> 14%
where the time goes in v1:
time: 193 us; the launch traced here: 191 us
  waiting for transfers between devices  51.6 us (27%)
  Pallas kernels  51.1 us (26%)
  starting transfers between devices  44.6 us (23%)
  blocking collectives  16.2 us (8%)
  between operations  13.6 us (7%)
  local copies, waits for them, and re-layouts  10.7 us (6%)
  other arithmetic  3.48 us (2%)
    ppermute x12, waiting for transfers between devices, around(): return lax.ppermute(a, 'x', [(i, (i + by) % 4) for i in range(4)])  47.3 us
    ppermute x12, starting transfers between devices, around(): return lax.ppermute(a, 'x', [(i, (i + by) % 4) for i in range(4)])  16.8 us
    all_gather x1, blocking collectives, per_device(): rows = lax.all_gather(pay, 'y')  16.2 us
    ppermute x6, starting transfers between devices, shift(): lax.ppermute(a, axis, [(i, i + by) for i in range(count) if 0 <= i + by <...  16.1 us
    pallas_call x4, Pallas kernels, down(): pl.pallas_call(down_body, grid_spec=pltpu.PrefetchScalarGridSpec(num_scal...  14.3 us
    pallas_call x1, Pallas kernels, per_device(): pl.pallas_call(up_body, grid_spec=pltpu.PrefetchScalarGridSpec(num_scalar...  9.09 us
    unnamed x58, local copies, waits for them, and re-layouts  8.57 us
    pallas_call x1, Pallas kernels, per_device(): call(conv_body, 14, [((ROWS, 256), BF), ((ROWS, 128), BF), ((ROWS, 128),...  5.99 us
  transfers between devices with their start and end apart: 24, of which 13 were waited for; matrix products, arithmetic and copies ran while one was open for 3% of the time, Pallas kernels for 14%

profile of v1, /device:TPU:1, one launch (start us, length us, event | category | flops | bytes accessed | tf_op | source)
XLA Modules:
  0.0 191.3 jit_solution(6752031849518770994)
XLA Ops:
  8.3 3.3 %collective-permute-start.7 = (bf16[256,2048]{1,0:T(8,128)(2,1)}, bf16[256,2048]{1,0:T(8,128)(2,1)S(1)}, u32[]{:S(2)}, u32[]{:S(2)}) collective-permute-start(bf16[256,2048]{1,0:T(8,128)(2,1)} %wa.1), channel_id=1, source_target_pairs={{0,1},{1,0},{2,3},{3,2},{4,5},{5,4},{6,7},{7,6},{8,9},{9,8},{10,11... | collective-permute-start | bytes 3145736 | tf_op jit(solution)/shard_map/ppermute | solution.py:361
  19.6 6.0 %conv_states.1 = (bf16[768,256]{1,0:T(8,128)(2,1)}, bf16[768,128]{1,0:T(8,128)(2,1)}, bf16[768,128]{1,0:T(8,128)(2,1)}, f32[8,768]{1,0:T(8,128)}, f32[8,768]{1,0...) custom-call(s32[1]{0:T(128)} %bitcast.2.sp, ...), custom_call_target="tpu_custom_call" | custom-call | flops 1000000000 | bytes 1000000 | tf_op jit(solution)/shard_map/conv_states/pallas_call | solution.py:367
  25.6 16.2 %all-gather = bf16[576,512]{1,0:T(8,128)(2,1)} all-gather(bf16[144,512]{1,0:T(8,128)(2,1)} %get-tuple-element.39), channel_id=2, replica_groups=mesh['z'=8,'y'=4,'x'=4,'c'=2] {'y'}, dimensions={0}, use_global_device_ids=true | all-gather | bytes 737280 | tf_op jit(solution)/shard_map/all_gather | solution.py:382
  43.8 3.1 %collective-permute-start.2 = (bf16[144,256]{1,0:T(8,128)(2,1)}, bf16[144,256]{1,0:T(8,128)(2,1)S(1)}, u32[]{:S(2)}, u32[]{:S(2)}) collective-permute-start(bf16[144,256]{1,0:T(8,128)(2,1)} %get-tuple-element.41), channel_id=1, source_target_pairs={{0,32},{32,64},{64,96},{96,128},{128,160},{160,192},{192,224},{1,3... | collective-permute-start | bytes 221192 | tf_op jit(solution)/shard_map/ppermute | solution.py:348
  46.9 7.6 %collective-permute-start.3 = (bf16[144,256]{1,0:T(8,128)(2,1)}, bf16[144,256]{1,0:T(8,128)(2,1)S(1)}, u32[]{:S(2)}, u32[]{:S(2)}) collective-permute-start(bf16[144,256]{1,0:T(8,128)(2,1)} %get-tuple-element.41), channel_id=1, source_target_pairs={{0,64},{32,96},{64,128},{96,160},{128,192},{160,224},{1,65},{33,97... | collective-permute-start | bytes 221192 | tf_op jit(solution)/shard_map/ppermute | solution.py:348
  57.1 4.3 %local.1.yl = f32[768,256]{1,0:T(8,128)} custom-call(bf16[768,256]{1,0:T(8,128)(2,1)} %get-tuple-element.30.x, bf16[768,128]{1,0:T(8,128)(2,1)} %get-tuple-element.31.b, bf16[768,128]{1,0:T(8,128)(2,1)} %get-tuple-element.32.c, f32[8,768]{1,0:T(8,128)} %get-tuple-element.33.cum, f32[8,768]{1,0:T(8,128)} %get-tuple-element.34.dt, ...), custom_call_target="tpu_custom_call" | custom-call | flops 2000000000 | bytes 1000000 | tf_op jit(solution)/shard_map/local/pallas_call | solution.py:388
  62.6 4.1 %gate.2 = (bf16[384,256]{1,0:T(8,128)(2,1)}, bf16[384,256]{1,0:T(8,128)(2,1)}) custom-call(s32[1]{0:T(128)} %bitcast.core, f32[768,256]{1,0:T(8,128)} %local.1.yl, bf16[768,128]{1,0:T(8,128)(2,1)} %get-tuple-element.32.c, f32[8,768]{1,0:T(8,128)} %get-tuple-element.38.dev, f32[136,512]{1,0:T(8,128)} %get-tuple-element.40.pre, bf16[144,256]{1,0:T(8,128)(2,1)} %copy-done.22, ...), custom_call_target="tpu_custom_call" | custom-call | flops 1000000000 | bytes 1000000 | tf_op jit(solution)/shard_map/gate/pallas_call | solution.py:389
  66.7 5.2 %collective-permute-start.6 = (bf16[384,256]{1,0:T(8,128)(2,1)}, bf16[384,256]{1,0:T(8,128)(2,1)S(1)}, u32[]{:S(2)}, u32[]{:S(2)}) collective-permute-start(bf16[384,256]{1,0:T(8,128)(2,1)} %get-tuple-element.44), channel_id=1, source_target_pairs={{0,1},{1,0},{2,3},{3,2},{4,5},{5,4},{6,7},{7,6},{8,9},{9,8},{10,11... | collective-permute-start | bytes 589832 | tf_op jit(solution)/shard_map/ppermute | solution.py:392
  74.3 3.6 %mix.1 = (bf16[384,512]{1,0:T(8,128)(2,1)}, bf16[384,512]{1,0:T(8,128)(2,1)}, bf16[384,512]{1,0:T(8,128)(2,1)}, bf16[384,512]{1,0:T(8,128)(2,1)}) custom-call(s32[1]{0:T(128)} %bitcast.1.where_x, bf16[384,256]{1,0:T(8,128)(2,1)} %get-tuple-element.43.a, bf16[384,256]{1,0:T(8,128)(2,1)} %copy-done.21, bf16[256,2048]{1,0:T(8,128)(2,1)} %wa.1, ...), custom_call_target="tpu_custom_call" | custom-call | flops 1000000000 | bytes 1000000 | tf_op jit(solution)/shard_map/mix/pallas_call | solution.py:393
  77.9 2.6 %collective-permute-start.10 = (bf16[384,512]{1,0:T(8,128)(2,1)}, bf16[384,512]{1,0:T(8,128)(2,1)S(1)}, u32[]{:S(2)}, u32[]{:S(2)}) collective-permute-start(bf16[384,512]{1,0:T(8,128)(2,1)} %get-tuple-element.47), channel_id=1, source_target_pairs={{0,4},{2,6},{4,0},{6,2},{1,5},{3,7},{5,1},{7,3},{8,12},{10,14},{12... | collective-permute-start | bytes 1179656 | tf_op jit(solution)/shard_map/ppermute | solution.py:351
  85.3 4.6 %collective-permute-done.10.r2 = bf16[384,512]{1,0:T(8,128)(2,1)S(1)} collective-permute-done((bf16[384,512]{1,0:T(8,128)(2,1)}, bf16[384,512]{1,0:T(8,128)(2,1)S(1)}, u32[]{:S(2)}, u32[]{:S(2)}) %collective-permute-start.10) | collective-permute-done | bytes 393248 | tf_op jit(solution)/shard_map/ppermute | solution.py:351
  89.8 8.5 %collective-permute-done.11.r3 = bf16[384,512]{1,0:T(8,128)(2,1)S(1)} collective-permute-done((bf16[384,512]{1,0:T(8,128)(2,1)}, bf16[384,512]{1,0:T(8,128)(2,1)S(1)}, u32[]{:S(2)}, u32[]{:S(2)}) %collective-permute-start.11) | collective-permute-done | bytes 393248 | tf_op jit(solution)/shard_map/ppermute | solution.py:351
  99.9 2.8 %first.1.p0 = bf16[400,512]{1,0:T(8,128)(2,1)} custom-call(s32[1]{0:T(128)} %bitcast.core, bf16[384,512]{1,0:T(8,128)(2,1)} %get-tuple-element.45.own, bf16[384,256]{1,0:T(8,128)(2,1)} %get-tuple-element.58.stream_a, bf16[384,256]{1,0:T(8,128)(2,1)} %copy-done.12, bf16[384,512]{1,0:T(8,128)(2,1)} %copy-done.6, bf16[384,512]{1,0:T(8,128)(2,1)} %copy-done.4, ...), custom_call_target="tpu_custom_call" | custom-call | flops 100000000 | bytes 1000000 | tf_op jit(solution)/shard_map/first/pallas_call | solution.py:397
  107.4 7.2 %collective-permute-done.13.p1 = bf16[400,512]{1,0:T(8,128)(2,1)S(1)} collective-permute-done((bf16[400,512]{1,0:T(8,128)(2,1)}, bf16[400,512]{1,0:T(8,128)(2,1)S(1)}, u32[]{:S(2)}, u32[]{:S(2)}) %collective-permute-start.13) | collective-permute-done | bytes 409632 | tf_op jit(solution)/shard_map/ppermute | solution.py:351
  114.6 9.9 %collective-permute-done.14.p2 = bf16[400,512]{1,0:T(8,128)(2,1)S(1)} collective-permute-done((bf16[400,512]{1,0:T(8,128)(2,1)}, bf16[400,512]{1,0:T(8,128)(2,1)S(1)}, u32[]{:S(2)}, u32[]{:S(2)}) %collective-permute-start.14) | collective-permute-done | bytes 409632 | tf_op jit(solution)/shard_map/ppermute | solution.py:351
  125.4 9.1 %up.1 = (bf16[384,2048]{1,0:T(8,128)(2,1)}, bf16[384,512]{1,0:T(8,128)(2,1)}) custom-call(s32[1]{0:T(128)} %bitcast.1.where_x, bf16[400,512]{1,0:T(8,128)(2,1)} %first.1.p0, bf16[400,512]{1,0:T(8,128)(2,1)} %copy-done, bf16[400,512]{1,0:T(8,128)(2,1)} %copy-done.1, bf16[400,512]{1,0:T(8,128)(2,1)} %copy-done.2, bf16[32,2,64,2048]{3,2,1,0:T(8,128)(2,1)} %bitcast.10), custom_call_target="tpu_custom_call" | custom-call | flops 3000000000 | bytes 10000000 | tf_op jit(solution)/shard_map/up/pallas_call | solution.py:408
  134.5 3.6 %down.5 = bf16[384,512]{1,0:T(8,128)(2,1)} custom-call(s32[1]{0:T(128)} %bitcast.1.where_x, bf16[384,2048]{1,0:T(8,128)(2,1)} %get-tuple-element.50.h, bf16[32,2,64,2048]{3,2,1,0:T(8,128)(2,1)} %bitcast.11), custom_call_target="tpu_custom_call" | custom-call | flops 800000000 | bytes 3000000 | tf_op jit(solution)/shard_map/down/pallas_call | solution.py:426
  138.0 3.6 %down.6 = bf16[384,512]{1,0:T(8,128)(2,1)} custom-call(s32[1]{0:T(128)} %bitcast.1.where_x, bf16[384,2048]{1,0:T(8,128)(2,1)} %get-tuple-element.50.h, bf16[32,2,64,2048]{3,2,1,0:T(8,128)(2,1)} %bitcast.12), custom_call_target="tpu_custom_call" | custom-call | flops 800000000 | bytes 3000000 | tf_op jit(solution)/shard_map/down/pallas_call | solution.py:426
  141.6 3.6 %down.7 = bf16[384,512]{1,0:T(8,128)(2,1)} custom-call(s32[1]{0:T(128)} %bitcast.1.where_x, bf16[384,2048]{1,0:T(8,128)(2,1)} %get-tuple-element.50.h, bf16[32,2,64,2048]{3,2,1,0:T(8,128)(2,1)} %bitcast.13), custom_call_target="tpu_custom_call" | custom-call | flops 800000000 | bytes 3000000 | tf_op jit(solution)/shard_map/down/pallas_call | solution.py:426
  146.3 2.7 %collective-permute-start.17 = (bf16[384,512]{1,0:T(8,128)(2,1)S(1)}, bf16[384,512]{1,0:T(8,128)(2,1)S(1)}, u32[]{:S(2)}, u32[]{:S(2)}) collective-permute-start(bf16[384,512]{1,0:T(8,128)(2,1)S(1)} %copy-done.10), channel_id=1, source_target_pairs={{0,4},{2,6},{4,0},{6,2},{1,5},{3,7},{5,1},{7,3},{8,12},{10,14},{12... | collective-permute-start | bytes 1179656 | tf_op jit(solution)/shard_map/ppermute | solution.py:351
  149.3 3.5 %down.4.own = bf16[384,512]{1,0:T(8,128)(2,1)} custom-call(s32[1]{0:T(128)} %bitcast.1.where_x, bf16[384,2048]{1,0:T(8,128)(2,1)} %get-tuple-element.50.h, bf16[32,2,64,2048]{3,2,1,0:T(8,128)(2,1)} %bitcast.14), custom_call_target="tpu_custom_call" | custom-call | flops 800000000 | bytes 3000000 | tf_op jit(solution)/shard_map/down/pallas_call | solution.py:426
  152.8 3.1 %collective-permute-done.16.r1 = bf16[384,512]{1,0:T(8,128)(2,1)S(1)} collective-permute-done((bf16[384,512]{1,0:T(8,128)(2,1)S(1)}, bf16[384,512]{1,0:T(8,128)(2,1)S(1)}, u32[]{:S(2)}, u32[]{:S(2)}) %collective-permute-start.16) | collective-permute-done | bytes 393248 | tf_op jit(solution)/shard_map/ppermute | solution.py:351
  155.9 10.2 %collective-permute-done.17.r2 = bf16[384,512]{1,0:T(8,128)(2,1)S(1)} collective-permute-done((bf16[384,512]{1,0:T(8,128)(2,1)S(1)}, bf16[384,512]{1,0:T(8,128)(2,1)S(1)}, u32[]{:S(2)}, u32[]{:S(2)}) %collective-permute-start.17) | collective-permute-done | bytes 393248 | tf_op jit(solution)/shard_map/ppermute | solution.py:351
  167.0 2.7 %second.1 = (f32[384,512]{1,0:T(8,128)}, f32[8,384]{1,0:T(8,128)}) custom-call(bf16[384,512]{1,0:T(8,128)(2,1)} %get-tuple-element.49.resid, bf16[384,512]{1,0:T(8,128)(2,1)} %down.4.own, bf16[384,512]{1,0:T(8,128)(2,1)} %copy-done.7, bf16[384,512]{1,0:T(8,128)(2,1)} %copy-done.8, bf16[384,512]{1,0:T(8,128)(2,1)} %copy-done.9), custom_call_target="tpu_custom_call" | custom-call | flops 100000000 | bytes 1000000 | tf_op jit(solution)/shard_map/second/pallas_call | solution.py:445
  (106 shorter events, 46.6 us)
Async XLA Ops:
  6.5 118.0 %all-gather.3.cloned.1.call-start = ((), (), s32[]{:S(2)}) async-start(), calls=%async_computation | async-start | bytes 17039360 | tf_op jit(solution)/shard_map/all_gather | solution.py:359
  8.3 64.9 %collective-permute-start.7 = (bf16[256,2048]{1,0:T(8,128)(2,1)}, bf16[256,2048]{1,0:T(8,128)(2,1)S(1)}, u32[]{:S(2)}, u32[]{:S(2)}) collective-permute-start(bf16[256,2048]{1,0:T(8,128)(2,1)} %wa.1), channel_id=1, source_target_pairs={{0,1},{1,0},{2,3},{3,2},{4,5},{5,4},{6,7},{7,6},{8,9},{9,8},{10,11... | collective-permute-start | bytes 3145736 | tf_op jit(solution)/shard_map/ppermute | solution.py:361
  13.0 6.0 %collective-permute-start = (bf16[2,512]{1,0:T(2,128)(2,1)S(1)}, bf16[2,512]{1,0:T(2,128)(2,1)S(1)}, u32[]{:S(2)}, u32[]{:S(2)}) collective-permute-start(bf16[2,512]{1,0:T(2,128)(2,1)S(1)} %pad_maximum_fusion.2), channel_id=1, source_target_pairs={{0,8},{8,16},{16,24},{24,32},{32,40},{40,48},{48,56},{56,64},{64,7... | collective-permute-start | bytes 6152 | tf_op jit(solution)/shard_map/ppermute | solution.py:348
  14.6 4.5 %collective-permute-start.1 = (bf16[2,512]{1,0:T(2,128)(2,1)S(1)}, bf16[2,512]{1,0:T(2,128)(2,1)S(1)}, u32[]{:S(2)}, u32[]{:S(2)}) collective-permute-start(bf16[2,512]{1,0:T(2,128)(2,1)S(1)} %pad_maximum_fusion.3), channel_id=1, source_target_pairs={{8,0},{16,8},{24,16},{32,24},{40,32},{48,40},{56,48},{64,56},{72,6... | collective-permute-start | bytes 6152 | tf_op jit(solution)/shard_map/ppermute | solution.py:348
  43.8 17.7 %collective-permute-start.2 = (bf16[144,256]{1,0:T(8,128)(2,1)}, bf16[144,256]{1,0:T(8,128)(2,1)S(1)}, u32[]{:S(2)}, u32[]{:S(2)}) collective-permute-start(bf16[144,256]{1,0:T(8,128)(2,1)} %get-tuple-element.41), channel_id=1, source_target_pairs={{0,32},{32,64},{64,96},{96,128},{128,160},{160,192},{192,224},{1,3... | collective-permute-start | bytes 221192 | tf_op jit(solution)/shard_map/ppermute | solution.py:348
  46.9 14.5 %collective-permute-start.3 = (bf16[144,256]{1,0:T(8,128)(2,1)}, bf16[144,256]{1,0:T(8,128)(2,1)S(1)}, u32[]{:S(2)}, u32[]{:S(2)}) collective-permute-start(bf16[144,256]{1,0:T(8,128)(2,1)} %get-tuple-element.41), channel_id=1, source_target_pairs={{0,64},{32,96},{64,128},{96,160},{128,192},{160,224},{1,65},{33,97... | collective-permute-start | bytes 221192 | tf_op jit(solution)/shard_map/ppermute | solution.py:348
  54.5 6.9 %collective-permute-start.4 = (bf16[144,256]{1,0:T(8,128)(2,1)}, bf16[144,256]{1,0:T(8,128)(2,1)S(1)}, u32[]{:S(2)}, u32[]{:S(2)}) collective-permute-start(bf16[144,256]{1,0:T(8,128)(2,1)} %get-tuple-element.42), channel_id=1, source_target_pairs={{32,0},{64,32},{96,64},{128,96},{160,128},{192,160},{224,192},{33,... | collective-permute-start | bytes 221192 | tf_op jit(solution)/shard_map/ppermute | solution.py:348
  55.8 6.2 %collective-permute-start.5 = (bf16[144,256]{1,0:T(8,128)(2,1)}, bf16[144,256]{1,0:T(8,128)(2,1)S(1)}, u32[]{:S(2)}, u32[]{:S(2)}) collective-permute-start(bf16[144,256]{1,0:T(8,128)(2,1)} %get-tuple-element.42), channel_id=1, source_target_pairs={{64,0},{96,32},{128,64},{160,96},{192,128},{224,160},{65,1},{97,33... | collective-permute-start | bytes 221192 | tf_op jit(solution)/shard_map/ppermute | solution.py:348
  66.7 6.5 %collective-permute-start.6 = (bf16[384,256]{1,0:T(8,128)(2,1)}, bf16[384,256]{1,0:T(8,128)(2,1)S(1)}, u32[]{:S(2)}, u32[]{:S(2)}) collective-permute-start(bf16[384,256]{1,0:T(8,128)(2,1)} %get-tuple-element.44), channel_id=1, source_target_pairs={{0,1},{1,0},{2,3},{3,2},{4,5},{5,4},{6,7},{7,6},{8,9},{9,8},{10,11... | collective-permute-start | bytes 589832 | tf_op jit(solution)/shard_map/ppermute | solution.py:392
  77.9 12.0 %collective-permute-start.10 = (bf16[384,512]{1,0:T(8,128)(2,1)}, bf16[384,512]{1,0:T(8,128)(2,1)S(1)}, u32[]{:S(2)}, u32[]{:S(2)}) collective-permute-start(bf16[384,512]{1,0:T(8,128)(2,1)} %get-tuple-element.47), channel_id=1, source_target_pairs={{0,4},{2,6},{4,0},{6,2},{1,5},{3,7},{5,1},{7,3},{8,12},{10,14},{12... | collective-permute-start | bytes 1179656 | tf_op jit(solution)/shard_map/ppermute | solution.py:351
  80.5 17.8 %collective-permute-start.11 = (bf16[384,512]{1,0:T(8,128)(2,1)}, bf16[384,512]{1,0:T(8,128)(2,1)S(1)}, u32[]{:S(2)}, u32[]{:S(2)}) collective-permute-start(bf16[384,512]{1,0:T(8,128)(2,1)} %get-tuple-element.48), channel_id=1, source_target_pairs={{0,6},{2,0},{4,2},{6,4},{1,7},{3,1},{5,3},{7,5},{8,14},{10,8},{12,... | collective-permute-start | bytes 1179656 | tf_op jit(solution)/shard_map/ppermute | solution.py:351
  81.4 17.8 %collective-permute-start.9 = (bf16[384,512]{1,0:T(8,128)(2,1)}, bf16[384,512]{1,0:T(8,128)(2,1)S(1)}, u32[]{:S(2)}, u32[]{:S(2)}) collective-permute-start(bf16[384,512]{1,0:T(8,128)(2,1)} %get-tuple-element.46), channel_id=1, source_target_pairs={{0,2},{2,4},{4,6},{6,0},{1,3},{3,5},{5,7},{7,1},{8,10},{10,12},{12... | collective-permute-start | bytes 1179656 | tf_op jit(solution)/shard_map/ppermute | solution.py:351
  82.7 2.6 %collective-permute-start.8 = (bf16[384,256]{1,0:T(8,128)(2,1)S(1)}, bf16[384,256]{1,0:T(8,128)(2,1)S(1)}, u32[]{:S(2)}, u32[]{:S(2)}) collective-permute-start(bf16[384,256]{1,0:T(8,128)(2,1)S(1)} %get-tuple-element.57), channel_id=1, source_target_pairs={{0,1},{1,0},{2,3},{3,2},{4,5},{5,4},{6,7},{7,6},{8,9},{9,8},{10,11... | collective-permute-start | bytes 589832 | tf_op jit(solution)/shard_map/ppermute | solution.py:363
  84.0 1.3 collective-permute-start.12
  102.6 11.9 %collective-permute-start.13 = (bf16[400,512]{1,0:T(8,128)(2,1)}, bf16[400,512]{1,0:T(8,128)(2,1)S(1)}, u32[]{:S(2)}, u32[]{:S(2)}) collective-permute-start(bf16[400,512]{1,0:T(8,128)(2,1)} %first.1.p0), channel_id=1, source_target_pairs={{0,2},{2,4},{4,6},{6,0},{1,3},{3,5},{5,7},{7,1},{8,10},{10,12},{12... | collective-permute-start | bytes 1228808 | tf_op jit(solution)/shard_map/ppermute | solution.py:351
  103.9 20.6 %collective-permute-start.14 = (bf16[400,512]{1,0:T(8,128)(2,1)}, bf16[400,512]{1,0:T(8,128)(2,1)S(1)}, u32[]{:S(2)}, u32[]{:S(2)}) collective-permute-start(bf16[400,512]{1,0:T(8,128)(2,1)} %first.1.p0), channel_id=1, source_target_pairs={{0,4},{2,6},{4,0},{6,2},{1,5},{3,7},{5,1},{7,3},{8,12},{10,14},{12... | collective-permute-start | bytes 1228808 | tf_op jit(solution)/shard_map/ppermute | solution.py:351
  106.3 18.2 %collective-permute-start.15 = (bf16[400,512]{1,0:T(8,128)(2,1)}, bf16[400,512]{1,0:T(8,128)(2,1)S(1)}, u32[]{:S(2)}, u32[]{:S(2)}) collective-permute-start(bf16[400,512]{1,0:T(8,128)(2,1)} %first.1.p0), channel_id=1, source_target_pairs={{0,6},{2,0},{4,2},{6,4},{1,7},{3,1},{5,3},{7,5},{8,14},{10,8},{12,... | collective-permute-start | bytes 1228808 | tf_op jit(solution)/shard_map/ppermute | solution.py:351
  145.3 10.7 %collective-permute-start.16 = (bf16[384,512]{1,0:T(8,128)(2,1)S(1)}, bf16[384,512]{1,0:T(8,128)(2,1)S(1)}, u32[]{:S(2)}, u32[]{:S(2)}) collective-permute-start(bf16[384,512]{1,0:T(8,128)(2,1)S(1)} %copy-done.11), channel_id=1, source_target_pairs={{0,2},{2,4},{4,6},{6,0},{1,3},{3,5},{5,7},{7,1},{8,10},{10,12},{12... | collective-permute-start | bytes 1179656 | tf_op jit(solution)/shard_map/ppermute | solution.py:351
  146.3 19.8 %collective-permute-start.17 = (bf16[384,512]{1,0:T(8,128)(2,1)S(1)}, bf16[384,512]{1,0:T(8,128)(2,1)S(1)}, u32[]{:S(2)}, u32[]{:S(2)}) collective-permute-start(bf16[384,512]{1,0:T(8,128)(2,1)S(1)} %copy-done.10), channel_id=1, source_target_pairs={{0,4},{2,6},{4,0},{6,2},{1,5},{3,7},{5,1},{7,3},{8,12},{10,14},{12... | collective-permute-start | bytes 1179656 | tf_op jit(solution)/shard_map/ppermute | solution.py:351
  149.0 17.1 %collective-permute-start.18 = (bf16[384,512]{1,0:T(8,128)(2,1)}, bf16[384,512]{1,0:T(8,128)(2,1)S(1)}, u32[]{:S(2)}, u32[]{:S(2)}) collective-permute-start(bf16[384,512]{1,0:T(8,128)(2,1)} %down.7), channel_id=1, source_target_pairs={{0,6},{2,0},{4,2},{6,4},{1,7},{3,1},{5,3},{7,5},{8,14},{10,8},{12,... | collective-permute-start | bytes 1179656 | tf_op jit(solution)/shard_map/ppermute | solution.py:351
  169.7 4.0 %collective-permute-start.19 = (f32[8,384]{1,0:T(8,128)}, f32[8,384]{1,0:T(8,128)S(1)}, u32[]{:S(2)}, u32[]{:S(2)}) collective-permute-start(f32[8,384]{1,0:T(8,128)} %get-tuple-element.52.s0), channel_id=1, source_target_pairs={{0,2},{2,4},{4,6},{6,0},{1,3},{3,5},{5,7},{7,1},{8,10},{10,12},{12... | collective-permute-start | bytes 36872 | tf_op jit(solution)/shard_map/ppermute | solution.py:351
  171.3 4.3 %collective-permute-start.20 = (f32[8,384]{1,0:T(8,128)}, f32[8,384]{1,0:T(8,128)S(1)}, u32[]{:S(2)}, u32[]{:S(2)}) collective-permute-start(f32[8,384]{1,0:T(8,128)} %get-tuple-element.52.s0), channel_id=1, source_target_pairs={{0,4},{2,6},{4,0},{6,2},{1,5},{3,7},{5,1},{7,3},{8,12},{10,14},{12... | collective-permute-start | bytes 36872 | tf_op jit(solution)/shard_map/ppermute | solution.py:351
  173.5 3.1 %collective-permute-start.21 = (f32[8,384]{1,0:T(8,128)}, f32[8,384]{1,0:T(8,128)S(1)}, u32[]{:S(2)}, u32[]{:S(2)}) collective-permute-start(f32[8,384]{1,0:T(8,128)} %get-tuple-element.52.s0), channel_id=1, source_target_pairs={{0,6},{2,0},{4,2},{6,4},{1,7},{3,1},{5,3},{7,5},{8,14},{10,8},{12,... | collective-permute-start | bytes 36872 | tf_op jit(solution)/shard_map/ppermute | solution.py:351
  179.6 3.1 %collective-permute-start.22 = (bf16[384,256]{1,0:T(8,128)(2,1)}, bf16[384,256]{1,0:T(8,128)(2,1)S(1)}, u32[]{:S(2)}, u32[]{:S(2)}) collective-permute-start(bf16[384,256]{1,0:T(8,128)(2,1)} %get-tuple-element.54), channel_id=1, source_target_pairs={{0,1},{1,0},{2,3},{3,2},{4,5},{5,4},{6,7},{7,6},{8,9},{9,8},{10,11... | collective-permute-start | bytes 589832 | tf_op jit(solution)/shard_map/ppermute | solution.py:452
  (28 other events, 329.7 us)
Sparse Core Ops, SparseCore 0:
  10.1 104.1 all-gather.2

commit v2 on v1

--- a/solution.py
+++ b/solution.py
@@ -1,3 +1,5 @@
+from functools import partial
+
 import jax
 import jax.numpy as jnp
 from jax import lax
@@ -27,16 +29,24 @@
     return pl.BlockSpec(memory_space=pltpu.SMEM)
 
 
-def call(body, ins, outs, scratch=(), scalars=0, name=None, flops=0):
-    return pl.pallas_call(
+def near(a):
+    return pltpu.with_memory_space_constraint(a, pltpu.VMEM)
+
+
+def off(a):
+    return pltpu.with_memory_space_constraint(a, pltpu.HBM)
+
+
+def call(body, ins, outs, scratch=(), scalars=0, far=(), plain=()):
+    run = pl.pallas_call(
         body,
         in_specs=[sm()] * scalars + [vm()] * (ins - scalars),
         out_specs=[vm()] * len(outs),
-        out_shape=[jax.ShapeDtypeStruct(s, d) for s, d in outs],
+        out_shape=[(jax.ShapeDtypeStruct if k in plain else pltpu.VMEM)(*o) for k, o in enumerate(outs)],
         scratch_shapes=list(scratch),
-        name=name,
-        cost_estimate=pl.CostEstimate(flops=flops, bytes_accessed=1000000, transcendentals=0),
-    )
+        compiler_params=pltpu.CompilerParams(vmem_limit_bytes=24 * 2**20),
+    )
+    return lambda *a: run(*[off(b) if k in far else b if k < scalars else near(b) for k, b in enumerate(a)])
 
 
 def iota(shape, dim):
@@ -259,41 +269,46 @@
     out[HALF : HALF + 16, :] = tail.astype(BF)
 
 
-def up_body(where_x, p0, p1, p2, p3, w, hidden, resid, xn):
-    @pl.when(pl.program_id(0) == 0)
-    def _():
-        blocks = (p0, p1, p2, p3)
-        tails = [p[HALF : HALF + 16, :].astype(F32) for p in blocks]
-        means = jnp.concatenate([t[0:1, 0:HALF] for t in tails] + [jnp.zeros((4, HALF), F32)], axis=0)
-        mean_cols = jnp.transpose(means)
-        full = [p[0:HALF, :].astype(F32) + mean_cols[:, k : k + 1] for k, p in enumerate(blocks)]
-        m = sum(jnp.sum(q, axis=1, keepdims=True) for q in full) / 2048.0
-        full = [q - m for q in full]
-        v = sum(jnp.sum(q * q, axis=1, keepdims=True) for q in full) / 2048.0
-        scale = lax.rsqrt(v + EPS)
-        for k, q in enumerate(full):
-            gain = tails[k][1:2, :] + tails[k][2:3, :] + tails[k][3:4, :]
-            done = (q * scale * gain).astype(BF)
-            block = pl.multiple_of(((where_x[0] + (4 - k)) % 4) * 512, 512)
-            xn[:, pl.ds(block, 512)] = done
-            if k == 0:
-                resid[...] = done
-
-    got = dot(xn[...], w[...].reshape(2048, 512), 1, 0)
-    got = jnp.maximum(got, 0.0)
-    hidden[...] = (got * got).astype(BF)
-
-
-def down_body(where_x, h, w, out, acc):
-    got = dot(h[...], w[...].reshape(512, 1024), 1, 1)
-
-    @pl.when(pl.program_id(0) == 0)
-    def _():
-        acc[...] = got
-
-    @pl.when(pl.program_id(0) == 1)
-    def _():
-        out[...] = (acc[...] + got).astype(BF)
+def up_body(where_x, p0, p1, p2, p3, w, hidden, resid, down, xn, up, sems):
+    loads = []
+    for core in range(2):
+        for part in range(2):
+            lanes = slice(part * 512, part * 512 + 512)
+            loads.append((w.at[:, core, :, lanes], up.at[2 * core + part]))
+    for block in range(4):
+        rows = slice(block * 8, block * 8 + 8)
+        loads.append((w.at[rows, :, :, 1024:2048], down.at[rows]))
+    loads = [pltpu.make_async_copy(src, dst, sems.at[k]) for k, (src, dst) in enumerate(loads)]
+    for load in loads:
+        load.start()
+    blocks = (p0, p1, p2, p3)
+    tails = [p[HALF : HALF + 16, :].astype(F32) for p in blocks]
+    means = jnp.concatenate([t[0:1, 0:HALF] for t in tails] + [jnp.zeros((4, HALF), F32)], axis=0)
+    mean_cols = jnp.transpose(means)
+    full = [p[0:HALF, :].astype(F32) + mean_cols[:, k : k + 1] for k, p in enumerate(blocks)]
+    m = sum(jnp.sum(q, axis=1, keepdims=True) for q in full) / 2048.0
+    full = [q - m for q in full]
+    v = sum(jnp.sum(q * q, axis=1, keepdims=True) for q in full) / 2048.0
+    scale = lax.rsqrt(v + EPS)
+    for k, q in enumerate(full):
+        gain = tails[k][1:2, :] + tails[k][2:3, :] + tails[k][3:4, :]
+        done = (q * scale * gain).astype(BF)
+        block = pl.multiple_of(((where_x[0] + (4 - k)) % 4) * 512, 512)
+        xn[:, pl.ds(block, 512)] = done
+        if k == 0:
+            resid[...] = done
+    for k in range(4):
+        loads[k].wait()
+        got = jnp.maximum(dot(xn[...], up[k].reshape(2048, 512), 1, 0), 0.0)
+        hidden[:, k * 512 : k * 512 + 512] = (got * got).astype(BF)
+    for k in range(4, 8):
+        loads[k].wait()
+
+
+def down_body(block, where_x, h, w, out):
+    rows = pl.ds(((where_x[0] + block) % 4) * 8, 8)
+    got = dot(h[:, 0:1024], w[rows, 0].reshape(512, 1024), 1, 1)
+    out[...] = (got + dot(h[:, 1024:2048], w[rows, 1].reshape(512, 1024), 1, 1)).astype(BF)
 
 
 def second_body(resid, own, r1, r2, r3, second, stats):
@@ -305,18 +320,20 @@
     stats[...] = jnp.where(iota((8, HALF), 0) == 0, s1, s2)
 
 
-def last_body(core, second, s0, s1, s2, s3, gain_a, gain_b, keep, send):
+def last_body(core, second, s0, s1, s2, s3, gain_a, gain_b, full, send):
     stats = s0[...] + s1[...] + s2[...] + s3[...]
     cols = jnp.transpose(stats)
     m = cols[:, 0:1] / 2048.0
     v = cols[:, 1:2] / 2048.0 - m * m
     scale = lax.rsqrt(v + EPS)
-    for off, gain, out in ((core[0], gain_a, keep), (1 - core[0], gain_b, send)):
-        lanes = pl.multiple_of(off * 256, 256)
-        out[...] = ((second[:, pl.ds(lanes, 256)] - m) * scale * gain[1:2, :]).astype(BF)
-
-
-def per_device(
+    mine = pl.multiple_of(core[0] * 256, 256)
+    other = pl.multiple_of(256 - core[0] * 256, 256)
+    send[...] = ((second[:, pl.ds(other, 256)] - m) * scale * gain_b[1:2, :]).astype(BF)
+    rows = pl.ds(pl.multiple_of(core[0] * HALF, HALF), HALF)
+    full[rows, :] = ((second[:, pl.ds(mine, 256)] - m) * scale * gain_a[1:2, :]).astype(BF)
+
+
+def layer(
     head_value_rows,
     entry_map_rows,
     readout_map_rows,
@@ -372,8 +389,7 @@
         + [((4, 128, 256), BF), ((144, 512), BF)],
         scratch=[pltpu.VMEM((784, 512), F32)],
         scalars=3,
-        name="conv_states",
-        flops=10**9,
+        far=(1, 2, 3, 4, 5, 8, 9, 10, 13),
     )(
         at_sp, head_rate_logarithm, head_step_bias, head_value_rows, entry_map_rows, readout_map_rows,
         low, high, value_conv_taps, entry_conv_taps, readout_conv_taps, step_before_softplus,
@@ -381,16 +397,16 @@
     )
     rows = lax.all_gather(pay, "y")
     send_f, send_b, pre = call(
-        chain_body, 2, [((144, 256), BF), ((144, 256), BF), ((136, 512), F32)], scalars=1, name="chain", flops=10**8
+        chain_body, 2, [((144, 256), BF), ((144, 256), BF), ((136, 512), F32)], scalars=1
     )(at_y, rows)
     f1, f2 = shift(send_f, "z", 1, 8), shift(send_f, "z", 2, 8)
     b1, b2 = shift(send_b, "z", -1, 8), shift(send_b, "z", -2, 8)
-    yl = call(local_body, 8, [((ROWS, 256), F32)], name="local", flops=2 * 10**9)(x, b, c, cum, dt, ct, doc, si)[0]
+    yl = call(local_body, 8, [((ROWS, 256), F32)])(x, b, c, cum, dt, ct, doc, si)[0]
     keep, send = call(
-        gate_body, 11, [((HALF, 256), BF)] * 2, scratch=[pltpu.VMEM((ROWS, 256), BF)], scalars=1, name="gate", flops=10**9
+        gate_body, 11, [((HALF, 256), BF)] * 2, scratch=[pltpu.VMEM((ROWS, 256), BF)], scalars=1, far=(9, 10)
     )(at_c, yl, c, dev, pre, f1, f2, b1, b2, output_gate_rows, group_norm_gain.reshape(1, 256))
     other = lax.ppermute(send, "c", swap)
-    o0, o1, o2, o3 = call(mix_body, 5, [((HALF, 512), BF)] * 4, scalars=1, name="mix", flops=10**9)(
+    o0, o1, o2, o3 = call(mix_body, 5, [((HALF, 512), BF)] * 4, scalars=1, far=(3,))(
         at_x, keep, other, mixer_output_weight, weight_other
     )
     r2, r1, r3 = around(o2, 2), around(o1, 1), around(o3, 3)
@@ -400,64 +416,46 @@
         [((HALF + 16, 512), BF)],
         scratch=[pltpu.VMEM((HALF, 512), F32), pltpu.VMEM((8, 512), F32)],
         scalars=1,
-        name="first",
-        flops=10**8,
     )(at_c, o0, stream_mine, stream_other, r1, r2, r3, gains, gains_other)[0]
     p2, p1, p3 = around(p0, 2), around(p0, 1), around(p0, 3)
-    fixed = pl.BlockSpec((HALF + 16, 512), lambda s, _: (0, 0))
-    hidden, resid = pl.pallas_call(
+    hidden, resid, down_weights = pl.pallas_call(
         up_body,
-        grid_spec=pltpu.PrefetchScalarGridSpec(
-            num_scalar_prefetch=1,
-            grid=(4,),
-            in_specs=[fixed] * 4 + [pl.BlockSpec((32, 1, 64, 512), lambda s, _: (0, s // 2, 0, s % 2))],
-            out_specs=[
-                pl.BlockSpec((HALF, 512), lambda s, _: (0, s)),
-                pl.BlockSpec((HALF, 512), lambda s, _: (0, 0)),
-            ],
-            scratch_shapes=[pltpu.VMEM((HALF, 2048), BF)],
-        ),
-        out_shape=[jax.ShapeDtypeStruct((HALF, 2048), BF), jax.ShapeDtypeStruct((HALF, 512), BF)],
+        in_specs=[sm()] + [vm()] * 4 + [pl.BlockSpec(memory_space=pltpu.HBM)],
+        out_specs=[vm()] * 3,
+        out_shape=[
+            pltpu.VMEM((HALF, 2048), BF),
+            pltpu.VMEM((HALF, 512), BF),
+            pltpu.VMEM((32, 2, 64, 1024), BF),
+        ],
+        scratch_shapes=[
+            pltpu.VMEM((HALF, 2048), BF),
+            pltpu.VMEM((4, 32, 64, 512), BF),
+            pltpu.SemaphoreType.DMA((8,)),
+        ],
+        compiler_params=pltpu.CompilerParams(vmem_limit_bytes=32 * 2**20),
         name="up",
-        cost_estimate=pl.CostEstimate(flops=3 * 10**9, bytes_accessed=10**7, transcendentals=0),
-    )(at_x, p0, p1, p2, p3, weights)
+    )(at_x, near(p0), near(p1), near(p2), near(p3), off(weights))
 
     def down(k):
-        return pl.pallas_call(
-            down_body,
-            grid_spec=pltpu.PrefetchScalarGridSpec(
-                num_scalar_prefetch=1,
-                grid=(2,),
-                in_specs=[
-                    pl.BlockSpec((HALF, 1024), lambda s, _: (0, s)),
-                    pl.BlockSpec((8, 1, 64, 1024), lambda s, at: ((at[0] + k) % 4, s, 0, 1)),
-                ],
-                out_specs=pl.BlockSpec((HALF, 512), lambda s, _: (0, 0)),
-                scratch_shapes=[pltpu.VMEM((HALF, 512), F32)],
-            ),
-            out_shape=jax.ShapeDtypeStruct((HALF, 512), BF),
-            name="down",
-            cost_estimate=pl.CostEstimate(flops=8 * 10**8, bytes_accessed=3 * 10**6, transcendentals=0),
-        )(at_x, hidden, weights)
+        return call(partial(down_body, k), 3, [((HALF, 512), BF)], scalars=1)(at_x, hidden, down_weights)[0]
 
     d2, d1, d3, d0 = down(2), down(1), down(3), down(0)
     q2, q1, q3 = around(d2, 2), around(d1, 1), around(d3, 3)
-    second, stats = call(second_body, 5, [((HALF, 512), F32), ((8, HALF), F32)], name="second", flops=10**8)(
+    second, stats = call(second_body, 5, [((HALF, 512), F32), ((8, HALF), F32)])(
         resid, d0, q1, q2, q3
     )
     s1, s2, s3 = around(stats, 1), around(stats, 2), around(stats, 3)
-    keep, send = call(last_body, 8, [((HALF, 256), BF)] * 2, scalars=1, name="last", flops=10**8)(
+    full, send = call(last_body, 8, [((ROWS, 256), BF), ((HALF, 256), BF)], scalars=1, plain=(0,))(
         at_c, second, stats, s1, s2, s3, gains, gains_other
     )
     got = lax.ppermute(send, "c", swap)
-    lower = core == 0
-    return jnp.concatenate([jnp.where(lower, keep, got), jnp.where(lower, got, keep)], axis=0)
+    return lax.dynamic_update_slice_in_dim(full, got, (1 - core) * HALF, 0)
 
 
 def solution(mesh):
     torus = Mesh(mesh.devices.reshape(8, 4, 4, 2), ("z", "y", "x", "c"))
     return jax.shard_map(
-        per_device,
+        layer,
         mesh=torus,
         in_specs=(
             P(SP, TP),

time: 193 us -> 164 us (0.85)
  Pallas kernels: 51.1 us -> 24.9 us
  waiting for transfers between devices: 51.6 us -> 61.5 us
  local copies, waits for them, and re-layouts: 10.7 us -> 3.93 us
    pallas_call x13, Pallas kernels: 51.1 us -> 24.9 us  [the longest x12 18.8 us: call(): run(*[off(b) if k in far else b if k < scalars else near(b) for k, b in e...]
    unnamed x58 -> x8, local copies, waits for them, and re-layouts: 8.57 us -> 1.77 us
    ppermute x12, waiting for transfers between devices: 47.3 us -> 52.7 us  [around(): return lax.ppermute(a, 'x', [(i, (i + by) % 4) for i in range(4)])]
    ppermute x6, waiting for transfers between devices: 0.57 us -> 4.47 us  [shift(): lax.ppermute(a, axis, [(i, i + by) for i in range(count) if 0 <= i + by <...]
  transfers between devices with their start and end apart: 24 -> 24, of which waited for: 13 -> 15; matrix products, arithmetic and copies ran while one was open for 3% -> 2% of each run, Pallas kernels for 14% -> 9%
where the time goes in v2:
time: 164 us
  waiting for transfers between devices  61.5 us (38%)
  starting transfers between devices  43.2 us (26%)
  Pallas kernels  24.9 us (15%)
  blocking collectives  15 us (9%)
  between operations  13.6 us (8%)
  local copies, waits for them, and re-layouts  3.93 us (2%)
  other arithmetic  1.76 us (1%)
    ppermute x12, waiting for transfers between devices, around(): return lax.ppermute(a, 'x', [(i, (i + by) % 4) for i in range(4)])  52.7 us
    pallas_call x12, Pallas kernels, call(): run(*[off(b) if k in far else b if k < scalars else near(b) for k, b in e...  18.8 us
    ppermute x12, starting transfers between devices, around(): return lax.ppermute(a, 'x', [(i, (i + by) % 4) for i in range(4)])  16.7 us
    all_gather x1, blocking collectives, layer(): rows = lax.all_gather(pay, 'y')  15 us
    ppermute x6, starting transfers between devices, shift(): lax.ppermute(a, axis, [(i, i + by) for i in range(count) if 0 <= i + by <...  14.4 us
    pallas_call x1, Pallas kernels, layer(): pl.pallas_call(up_body, in_specs=[sm()] + [vm()] * 4 + [pl.BlockSpec(memo...  6.11 us
    ppermute x1, starting transfers between devices, layer(): other = lax.ppermute(send, 'c', swap)  4.53 us
    ppermute x6, waiting for transfers between devices, shift(): lax.ppermute(a, axis, [(i, i + by) for i in range(count) if 0 <= i + by <...  4.47 us
  transfers between devices with their start and end apart: 24, of which 15 were waited for; matrix products, arithmetic and copies ran while one was open for 2% of the time, Pallas kernels for 9%

profile of v2, /device:TPU:1, one launch (start us, length us, event | category | flops | bytes accessed | tf_op | source)
XLA Modules:
  0.0 163.9 jit_solution(13052678458414816032)
XLA Ops:
  6.5 1.7 %pad_maximum_fusion = bf16[64,2048]{1,0:T(8,128)(2,1)} fusion(bf16[64,1024]{1,0:T(8,128)(2,1)} %param.37, bf16[64,1024]{1,0:T(8,128)(2,1)} %param.36), kind=kLoop, calls=%fused_computation | loop fusion | flops 524288 | bytes 524288 | tf_op jit(solution)/shard_map/concatenate | solution.py:375
  8.3 3.3 %collective-permute-start.7 = (bf16[256,2048]{1,0:T(8,128)(2,1)}, bf16[256,2048]{1,0:T(8,128)(2,1)S(1)}, u32[]{:S(2)}, u32[]{:S(2)}) collective-permute-start(bf16[256,2048]{1,0:T(8,128)(2,1)} %wa.1), channel_id=1, source_target_pairs={{0,1},{1,0},{2,3},{3,2},{4,5},{5,4},{6,7},{7,6},{8,9},{9,8},{10,11... | collective-permute-start | bytes 3145736 | tf_op jit(solution)/shard_map/ppermute | solution.py:378
  18.9 5.0 %shard_map.181 = (bf16[768,256]{1,0:T(8,128)(2,1)S(1)}, bf16[768,128]{1,0:T(8,128)(2,1)S(1)}, bf16[768,128]{1,0:T(8,128)(2,1)S(1)}, f32[8,768]{1,0:T(8,128)S(1)}...) custom-call(s32[1]{0:T(128)} %bitcast.2.sp, ...), custom_call_target="tpu_custom_call" | custom-call | tf_op jit(solution)/shard_map/pallas_call | solution.py:49
  23.9 15.0 %all-gather = bf16[576,512]{1,0:T(8,128)(2,1)S(1)} all-gather(bf16[144,512]{1,0:T(8,128)(2,1)S(1)} %get-tuple-element.40), channel_id=2, replica_groups=mesh['z'=8,'y'=4,'x'=4,'c'=2] {'y'}, dimensions={0}, use_global_device_ids=true | all-gather | bytes 737280 | tf_op jit(solution)/shard_map/all_gather | solution.py:398
  39.1 5.2 %collective-permute-start.3 = (bf16[144,256]{1,0:T(8,128)(2,1)S(1)}, bf16[144,256]{1,0:T(8,128)(2,1)S(1)}, u32[]{:S(2)}, u32[]{:S(2)}) collective-permute-start(bf16[144,256]{1,0:T(8,128)(2,1)S(1)} %get-tuple-element.42), channel_id=1, source_target_pairs={{0,64},{32,96},{64,128},{96,160},{128,192},{160,224},{1,65},{33,97... | collective-permute-start | bytes 221192 | tf_op jit(solution)/shard_map/ppermute | solution.py:365
  44.3 3.8 %collective-permute-start.2 = (bf16[144,256]{1,0:T(8,128)(2,1)S(1)}, bf16[144,256]{1,0:T(8,128)(2,1)S(1)}, u32[]{:S(2)}, u32[]{:S(2)}) collective-permute-start(bf16[144,256]{1,0:T(8,128)(2,1)S(1)} %get-tuple-element.42), channel_id=1, source_target_pairs={{0,32},{32,64},{64,96},{96,128},{128,160},{160,192},{192,224},{1,3... | collective-permute-start | bytes 221192 | tf_op jit(solution)/shard_map/ppermute | solution.py:365
  50.7 2.2 %shard_map.182.yl = f32[768,256]{1,0:T(8,128)S(1)} custom-call(bf16[768,256]{1,0:T(8,128)(2,1)S(1)} %get-tuple-element.31.x, bf16[768,128]{1,0:T(8,128)(2,1)S(1)} %get-tuple-element.32.b, bf16[768,128]{1,0:T(8,128)(2,1)S(1)} %get-tuple-element.33.c, f32[8,768]{1,0:T(8,128)S(1)} %get-tuple-element.34.cum, f32[8,768]{1,0:T(8,128)S(1)} %get-tuple-element.35.dt, ...), custom_call_target="tpu_custom_call" | custom-call | tf_op jit(solution)/shard_map/pallas_call | solution.py:49
  52.9 1.9 %collective-permute-done.5.b2 = bf16[144,256]{1,0:T(8,128)(2,1)S(1)} collective-permute-done((bf16[144,256]{1,0:T(8,128)(2,1)S(1)}, bf16[144,256]{1,0:T(8,128)(2,1)S(1)}, u32[]{:S(2)}, u32[]{:S(2)}) %collective-permute-start.5) | collective-permute-done | bytes 73760 | tf_op jit(solution)/shard_map/ppermute | solution.py:365
  56.2 2.8 %shard_map.184 = (bf16[384,256]{1,0:T(8,128)(2,1)S(1)}, bf16[384,256]{1,0:T(8,128)(2,1)S(1)}) custom-call(s32[1]{0:T(128)} %bitcast.core, f32[768,256]{1,0:T(8,128)S(1)} %shard_map.182.yl, bf16[768,128]{1,0:T(8,128)(2,1)S(1)} %get-tuple-element.33.c, f32[8,768]{1,0:T(8,128)S(1)} %get-tuple-element.39.dev, f32[136,512]{1,0:T(8,128)S(1)} %get-tuple-element.41.pre, ...), custom_call_target="tpu_custom_call" | custom-call | tf_op jit(solution)/shard_map/pallas_call | solution.py:49
  59.0 4.5 %collective-permute-start.6 = (bf16[384,256]{1,0:T(8,128)(2,1)S(1)}, bf16[384,256]{1,0:T(8,128)(2,1)S(1)}, u32[]{:S(2)}, u32[]{:S(2)}) collective-permute-start(bf16[384,256]{1,0:T(8,128)(2,1)S(1)} %get-tuple-element.45), channel_id=1, source_target_pairs={{0,1},{1,0},{2,3},{3,2},{4,5},{5,4},{6,7},{7,6},{8,9},{9,8},{10,11... | collective-permute-start | bytes 589832 | tf_op jit(solution)/shard_map/ppermute | solution.py:408
  64.6 2.5 %shard_map.185 = (bf16[384,512]{1,0:T(8,128)(2,1)S(1)}, bf16[384,512]{1,0:T(8,128)(2,1)S(1)}, bf16[384,512]{1,0:T(8,128)(2,1)S(1)}, bf16[384,512]{1,0:T(8,128)(2,1)S(1)}) custom-call(s32[1]{0:T(128)} %bitcast.1.where_x, bf16[384,256]{1,0:T(8,128)(2,1)S(1)} %get-tuple-element.44.a, bf16[384,256]{1,0:T(8,128)(2,1)S(1)} %collective-permute-done.6.b, ...), custom_call_target="tpu_custom_call" | custom-call | tf_op jit(solution)/shard_map/pallas_call | solution.py:49
  68.4 2.4 %collective-permute-start.10 = (bf16[384,512]{1,0:T(8,128)(2,1)S(1)}, bf16[384,512]{1,0:T(8,128)(2,1)S(1)}, u32[]{:S(2)}, u32[]{:S(2)}) collective-permute-start(bf16[384,512]{1,0:T(8,128)(2,1)S(1)} %get-tuple-element.48), channel_id=1, source_target_pairs={{0,4},{2,6},{4,0},{6,2},{1,5},{3,7},{5,1},{7,3},{8,12},{10,14},{12... | collective-permute-start | bytes 1179656 | tf_op jit(solution)/shard_map/ppermute | solution.py:368
  74.8 4.0 %collective-permute-done.9.r1 = bf16[384,512]{1,0:T(8,128)(2,1)S(1)} collective-permute-done((bf16[384,512]{1,0:T(8,128)(2,1)S(1)}, bf16[384,512]{1,0:T(8,128)(2,1)S(1)}, u32[]{:S(2)}, u32[]{:S(2)}) %collective-permute-start.9) | collective-permute-done | bytes 393248 | tf_op jit(solution)/shard_map/ppermute | solution.py:368
  78.8 9.3 %collective-permute-done.10.r2 = bf16[384,512]{1,0:T(8,128)(2,1)S(1)} collective-permute-done((bf16[384,512]{1,0:T(8,128)(2,1)S(1)}, bf16[384,512]{1,0:T(8,128)(2,1)S(1)}, u32[]{:S(2)}, u32[]{:S(2)}) %collective-permute-start.10) | collective-permute-done | bytes 393248 | tf_op jit(solution)/shard_map/ppermute | solution.py:368
  88.6 2.9 %collective-permute-start.15 = (bf16[400,512]{1,0:T(8,128)(2,1)S(1)}, bf16[400,512]{1,0:T(8,128)(2,1)S(1)}, u32[]{:S(2)}, u32[]{:S(2)}) collective-permute-start(bf16[400,512]{1,0:T(8,128)(2,1)S(1)} %shard_map.186.p0), channel_id=1, source_target_pairs={{0,6},{2,0},{4,2},{6,4},{1,7},{3,1},{5,3},{7,5},{8,14},{10,8},{12,... | collective-permute-start | bytes 1228808 | tf_op jit(solution)/shard_map/ppermute | solution.py:368
  92.1 16.4 %collective-permute-done.15.p3 = bf16[400,512]{1,0:T(8,128)(2,1)S(1)} collective-permute-done((bf16[400,512]{1,0:T(8,128)(2,1)S(1)}, bf16[400,512]{1,0:T(8,128)(2,1)S(1)}, u32[]{:S(2)}, u32[]{:S(2)}) %collective-permute-start.15) | collective-permute-done | bytes 409632 | tf_op jit(solution)/shard_map/ppermute | solution.py:368
  108.5 4.4 %collective-permute-done.13.p1 = bf16[400,512]{1,0:T(8,128)(2,1)S(1)} collective-permute-done((bf16[400,512]{1,0:T(8,128)(2,1)S(1)}, bf16[400,512]{1,0:T(8,128)(2,1)S(1)}, u32[]{:S(2)}, u32[]{:S(2)}) %collective-permute-start.13) | collective-permute-done | bytes 409632 | tf_op jit(solution)/shard_map/ppermute | solution.py:368
  113.8 6.1 %up.1 = (bf16[384,2048]{1,0:T(8,128)(2,1)S(1)}, bf16[384,512]{1,0:T(8,128)(2,1)S(1)}, bf16[32,2,64,1024]{3,2,1,0:T(8,128)(2,1)S(1)}) custom-call(s32[1]{0:T(128)} %bitcast.1.where_x, bf16[400,512]{1,0:T(8,128)(2,1)S(1)} %shard_map.186.p0, bf16[400,512]{1,0:T(8,128)(2,1)S(1)} %collective-permute-done.13.p1, bf16[400,512]{1,0:T(8,128)(2,1)S(1)} %collective-permute-done.14.p2, ...), custom_call_target="tpu_custom_call" | custom-call | tf_op jit(solution)/shard_map/up/pallas_call | solution.py:421
  124.3 2.4 %collective-permute-start.17 = (bf16[384,512]{1,0:T(8,128)(2,1)S(1)}, bf16[384,512]{1,0:T(8,128)(2,1)S(1)}, u32[]{:S(2)}, u32[]{:S(2)}) collective-permute-start(bf16[384,512]{1,0:T(8,128)(2,1)S(1)} %shard_map.189), channel_id=1, source_target_pairs={{0,4},{2,6},{4,0},{6,2},{1,5},{3,7},{5,1},{7,3},{8,12},{10,14},{12... | collective-permute-start | bytes 1179656 | tf_op jit(solution)/shard_map/ppermute | solution.py:368
  128.9 5.8 %collective-permute-done.16.r1 = bf16[384,512]{1,0:T(8,128)(2,1)S(1)} collective-permute-done((bf16[384,512]{1,0:T(8,128)(2,1)S(1)}, bf16[384,512]{1,0:T(8,128)(2,1)S(1)}, u32[]{:S(2)}, u32[]{:S(2)}) %collective-permute-start.16) | collective-permute-done | bytes 393248 | tf_op jit(solution)/shard_map/ppermute | solution.py:368
  134.7 9.3 %collective-permute-done.17.r2 = bf16[384,512]{1,0:T(8,128)(2,1)S(1)} collective-permute-done((bf16[384,512]{1,0:T(8,128)(2,1)S(1)}, bf16[384,512]{1,0:T(8,128)(2,1)S(1)}, u32[]{:S(2)}, u32[]{:S(2)}) %collective-permute-start.17) | collective-permute-done | bytes 393248 | tf_op jit(solution)/shard_map/ppermute | solution.py:368
  144.6 2.7 %collective-permute-start.21 = (f32[8,384]{1,0:T(8,128)S(1)}, f32[8,384]{1,0:T(8,128)S(1)}, u32[]{:S(2)}, u32[]{:S(2)}) collective-permute-start(f32[8,384]{1,0:T(8,128)S(1)} %get-tuple-element.54.s0), channel_id=1, source_target_pairs={{0,6},{2,0},{4,2},{6,4},{1,7},{3,1},{5,3},{7,5},{8,14},{10,8},{12,... | collective-permute-start | bytes 36872 | tf_op jit(solution)/shard_map/ppermute | solution.py:368
  148.1 3.3 %collective-permute-done.20.s2 = f32[8,384]{1,0:T(8,128)S(1)} collective-permute-done((f32[8,384]{1,0:T(8,128)S(1)}, f32[8,384]{1,0:T(8,128)S(1)}, u32[]{:S(2)}, u32[]{:S(2)}) %collective-permute-start.20) | collective-permute-done | bytes 12320 | tf_op jit(solution)/shard_map/ppermute | solution.py:368
  152.6 2.7 %collective-permute-start.22 = (bf16[384,256]{1,0:T(8,128)(2,1)S(1)}, bf16[384,256]{1,0:T(8,128)(2,1)S(1)}, u32[]{:S(2)}, u32[]{:S(2)}) collective-permute-start(bf16[384,256]{1,0:T(8,128)(2,1)S(1)} %get-tuple-element.56), channel_id=1, source_target_pairs={{0,1},{1,0},{2,3},{3,2},{4,5},{5,4},{6,7},{7,6},{8,9},{9,8},{10,11... | collective-permute-start | bytes 589832 | tf_op jit(solution)/shard_map/ppermute | solution.py:451
  (55 shorter events, 30.4 us)
Async XLA Ops:
  6.5 107.3 %all-gather.3.cloned.1.call-start = ((), (), s32[]{:S(2)}) async-start(), calls=%async_computation | async-start | bytes 17039360 | tf_op jit(solution)/shard_map/all_gather | solution.py:376
  8.3 56.3 %collective-permute-start.7 = (bf16[256,2048]{1,0:T(8,128)(2,1)}, bf16[256,2048]{1,0:T(8,128)(2,1)S(1)}, u32[]{:S(2)}, u32[]{:S(2)}) collective-permute-start(bf16[256,2048]{1,0:T(8,128)(2,1)} %wa.1), channel_id=1, source_target_pairs={{0,1},{1,0},{2,3},{3,2},{4,5},{5,4},{6,7},{7,6},{8,9},{9,8},{10,11... | collective-permute-start | bytes 3145736 | tf_op jit(solution)/shard_map/ppermute | solution.py:378
  13.0 4.6 %collective-permute-start = (bf16[2,512]{1,0:T(2,128)(2,1)S(1)}, bf16[2,512]{1,0:T(2,128)(2,1)S(1)}, u32[]{:S(2)}, u32[]{:S(2)}) collective-permute-start(bf16[2,512]{1,0:T(2,128)(2,1)S(1)} %pad_maximum_fusion.1), channel_id=1, source_target_pairs={{0,8},{8,16},{16,24},{24,32},{32,40},{40,48},{48,56},{56,64},{64,7... | collective-permute-start | bytes 6152 | tf_op jit(solution)/shard_map/ppermute | solution.py:365
  14.6 4.3 %collective-permute-start.1 = (bf16[2,512]{1,0:T(2,128)(2,1)S(1)}, bf16[2,512]{1,0:T(2,128)(2,1)S(1)}, u32[]{:S(2)}, u32[]{:S(2)}) collective-permute-start(bf16[2,512]{1,0:T(2,128)(2,1)S(1)} %pad_maximum_fusion.2), channel_id=1, source_target_pairs={{8,0},{16,8},{24,16},{32,24},{40,32},{48,40},{56,48},{64,56},{72,6... | collective-permute-start | bytes 6152 | tf_op jit(solution)/shard_map/ppermute | solution.py:365
  39.1 13.8 %collective-permute-start.3 = (bf16[144,256]{1,0:T(8,128)(2,1)S(1)}, bf16[144,256]{1,0:T(8,128)(2,1)S(1)}, u32[]{:S(2)}, u32[]{:S(2)}) collective-permute-start(bf16[144,256]{1,0:T(8,128)(2,1)S(1)} %get-tuple-element.42), channel_id=1, source_target_pairs={{0,64},{32,96},{64,128},{96,160},{128,192},{160,224},{1,65},{33,97... | collective-permute-start | bytes 221192 | tf_op jit(solution)/shard_map/ppermute | solution.py:365
  44.3 8.6 %collective-permute-start.2 = (bf16[144,256]{1,0:T(8,128)(2,1)S(1)}, bf16[144,256]{1,0:T(8,128)(2,1)S(1)}, u32[]{:S(2)}, u32[]{:S(2)}) collective-permute-start(bf16[144,256]{1,0:T(8,128)(2,1)S(1)} %get-tuple-element.42), channel_id=1, source_target_pairs={{0,32},{32,64},{64,96},{96,128},{128,160},{160,192},{192,224},{1,3... | collective-permute-start | bytes 221192 | tf_op jit(solution)/shard_map/ppermute | solution.py:365
  48.1 6.7 %collective-permute-start.5 = (bf16[144,256]{1,0:T(8,128)(2,1)S(1)}, bf16[144,256]{1,0:T(8,128)(2,1)S(1)}, u32[]{:S(2)}, u32[]{:S(2)}) collective-permute-start(bf16[144,256]{1,0:T(8,128)(2,1)S(1)} %get-tuple-element.43), channel_id=1, source_target_pairs={{64,0},{96,32},{128,64},{160,96},{192,128},{224,160},{65,1},{97,33... | collective-permute-start | bytes 221192 | tf_op jit(solution)/shard_map/ppermute | solution.py:365
  49.4 6.7 %collective-permute-start.4 = (bf16[144,256]{1,0:T(8,128)(2,1)S(1)}, bf16[144,256]{1,0:T(8,128)(2,1)S(1)}, u32[]{:S(2)}, u32[]{:S(2)}) collective-permute-start(bf16[144,256]{1,0:T(8,128)(2,1)S(1)} %get-tuple-element.43), channel_id=1, source_target_pairs={{32,0},{64,32},{96,64},{128,96},{160,128},{192,160},{224,192},{33,... | collective-permute-start | bytes 221192 | tf_op jit(solution)/shard_map/ppermute | solution.py:365
  59.0 5.6 %collective-permute-start.6 = (bf16[384,256]{1,0:T(8,128)(2,1)S(1)}, bf16[384,256]{1,0:T(8,128)(2,1)S(1)}, u32[]{:S(2)}, u32[]{:S(2)}) collective-permute-start(bf16[384,256]{1,0:T(8,128)(2,1)S(1)} %get-tuple-element.45), channel_id=1, source_target_pairs={{0,1},{1,0},{2,3},{3,2},{4,5},{5,4},{6,7},{7,6},{8,9},{9,8},{10,11... | collective-permute-start | bytes 589832 | tf_op jit(solution)/shard_map/ppermute | solution.py:408
  67.1 11.7 %collective-permute-start.9 = (bf16[384,512]{1,0:T(8,128)(2,1)S(1)}, bf16[384,512]{1,0:T(8,128)(2,1)S(1)}, u32[]{:S(2)}, u32[]{:S(2)}) collective-permute-start(bf16[384,512]{1,0:T(8,128)(2,1)S(1)} %get-tuple-element.47), channel_id=1, source_target_pairs={{0,2},{2,4},{4,6},{6,0},{1,3},{3,5},{5,7},{7,1},{8,10},{10,12},{12... | collective-permute-start | bytes 1179656 | tf_op jit(solution)/shard_map/ppermute | solution.py:368
  68.4 19.7 %collective-permute-start.10 = (bf16[384,512]{1,0:T(8,128)(2,1)S(1)}, bf16[384,512]{1,0:T(8,128)(2,1)S(1)}, u32[]{:S(2)}, u32[]{:S(2)}) collective-permute-start(bf16[384,512]{1,0:T(8,128)(2,1)S(1)} %get-tuple-element.48), channel_id=1, source_target_pairs={{0,4},{2,6},{4,0},{6,2},{1,5},{3,7},{5,1},{7,3},{8,12},{10,14},{12... | collective-permute-start | bytes 1179656 | tf_op jit(solution)/shard_map/ppermute | solution.py:368
  70.9 17.3 %collective-permute-start.11 = (bf16[384,512]{1,0:T(8,128)(2,1)S(1)}, bf16[384,512]{1,0:T(8,128)(2,1)S(1)}, u32[]{:S(2)}, u32[]{:S(2)}) collective-permute-start(bf16[384,512]{1,0:T(8,128)(2,1)S(1)} %get-tuple-element.49), channel_id=1, source_target_pairs={{0,6},{2,0},{4,2},{6,4},{1,7},{3,1},{5,3},{7,5},{8,14},{10,8},{12,... | collective-permute-start | bytes 1179656 | tf_op jit(solution)/shard_map/ppermute | solution.py:368
  72.0 2.8 %collective-permute-start.8 = (bf16[384,256]{1,0:T(8,128)(2,1)S(1)}, bf16[384,256]{1,0:T(8,128)(2,1)S(1)}, u32[]{:S(2)}, u32[]{:S(2)}) collective-permute-start(bf16[384,256]{1,0:T(8,128)(2,1)S(1)} %get-tuple-element.57), channel_id=1, source_target_pairs={{0,1},{1,0},{2,3},{3,2},{4,5},{5,4},{6,7},{7,6},{8,9},{9,8},{10,11... | collective-permute-start | bytes 589832 | tf_op jit(solution)/shard_map/ppermute | solution.py:380
  73.5 1.3 collective-permute-start.12
  88.6 19.9 %collective-permute-start.15 = (bf16[400,512]{1,0:T(8,128)(2,1)S(1)}, bf16[400,512]{1,0:T(8,128)(2,1)S(1)}, u32[]{:S(2)}, u32[]{:S(2)}) collective-permute-start(bf16[400,512]{1,0:T(8,128)(2,1)S(1)} %shard_map.186.p0), channel_id=1, source_target_pairs={{0,6},{2,0},{4,2},{6,4},{1,7},{3,1},{5,3},{7,5},{8,14},{10,8},{12,... | collective-permute-start | bytes 1228808 | tf_op jit(solution)/shard_map/ppermute | solution.py:368
  91.4 17.1 %collective-permute-start.14 = (bf16[400,512]{1,0:T(8,128)(2,1)S(1)}, bf16[400,512]{1,0:T(8,128)(2,1)S(1)}, u32[]{:S(2)}, u32[]{:S(2)}) collective-permute-start(bf16[400,512]{1,0:T(8,128)(2,1)S(1)} %shard_map.186.p0), channel_id=1, source_target_pairs={{0,4},{2,6},{4,0},{6,2},{1,5},{3,7},{5,1},{7,3},{8,12},{10,14},{12... | collective-permute-start | bytes 1228808 | tf_op jit(solution)/shard_map/ppermute | solution.py:368
  91.6 21.3 %collective-permute-start.13 = (bf16[400,512]{1,0:T(8,128)(2,1)S(1)}, bf16[400,512]{1,0:T(8,128)(2,1)S(1)}, u32[]{:S(2)}, u32[]{:S(2)}) collective-permute-start(bf16[400,512]{1,0:T(8,128)(2,1)S(1)} %shard_map.186.p0), channel_id=1, source_target_pairs={{0,2},{2,4},{4,6},{6,0},{1,3},{3,5},{5,7},{7,1},{8,10},{10,12},{12... | collective-permute-start | bytes 1228808 | tf_op jit(solution)/shard_map/ppermute | solution.py:368
  123.0 11.7 %collective-permute-start.16 = (bf16[384,512]{1,0:T(8,128)(2,1)S(1)}, bf16[384,512]{1,0:T(8,128)(2,1)S(1)}, u32[]{:S(2)}, u32[]{:S(2)}) collective-permute-start(bf16[384,512]{1,0:T(8,128)(2,1)S(1)} %shard_map.188), channel_id=1, source_target_pairs={{0,2},{2,4},{4,6},{6,0},{1,3},{3,5},{5,7},{7,1},{8,10},{10,12},{12... | collective-permute-start | bytes 1179656 | tf_op jit(solution)/shard_map/ppermute | solution.py:368
  124.3 19.8 %collective-permute-start.17 = (bf16[384,512]{1,0:T(8,128)(2,1)S(1)}, bf16[384,512]{1,0:T(8,128)(2,1)S(1)}, u32[]{:S(2)}, u32[]{:S(2)}) collective-permute-start(bf16[384,512]{1,0:T(8,128)(2,1)S(1)} %shard_map.189), channel_id=1, source_target_pairs={{0,4},{2,6},{4,0},{6,2},{1,5},{3,7},{5,1},{7,3},{8,12},{10,14},{12... | collective-permute-start | bytes 1179656 | tf_op jit(solution)/shard_map/ppermute | solution.py:368
  126.7 17.4 %collective-permute-start.18 = (bf16[384,512]{1,0:T(8,128)(2,1)S(1)}, bf16[384,512]{1,0:T(8,128)(2,1)S(1)}, u32[]{:S(2)}, u32[]{:S(2)}) collective-permute-start(bf16[384,512]{1,0:T(8,128)(2,1)S(1)} %shard_map.190), channel_id=1, source_target_pairs={{0,6},{2,0},{4,2},{6,4},{1,7},{3,1},{5,3},{7,5},{8,14},{10,8},{12,... | collective-permute-start | bytes 1179656 | tf_op jit(solution)/shard_map/ppermute | solution.py:368
  144.6 3.6 %collective-permute-start.21 = (f32[8,384]{1,0:T(8,128)S(1)}, f32[8,384]{1,0:T(8,128)S(1)}, u32[]{:S(2)}, u32[]{:S(2)}) collective-permute-start(f32[8,384]{1,0:T(8,128)S(1)} %get-tuple-element.54.s0), channel_id=1, source_target_pairs={{0,6},{2,0},{4,2},{6,4},{1,7},{3,1},{5,3},{7,5},{8,14},{10,8},{12,... | collective-permute-start | bytes 36872 | tf_op jit(solution)/shard_map/ppermute | solution.py:368
  147.3 4.1 %collective-permute-start.20 = (f32[8,384]{1,0:T(8,128)S(1)}, f32[8,384]{1,0:T(8,128)S(1)}, u32[]{:S(2)}, u32[]{:S(2)}) collective-permute-start(f32[8,384]{1,0:T(8,128)S(1)} %get-tuple-element.54.s0), channel_id=1, source_target_pairs={{0,4},{2,6},{4,0},{6,2},{1,5},{3,7},{5,1},{7,3},{8,12},{10,14},{12... | collective-permute-start | bytes 36872 | tf_op jit(solution)/shard_map/ppermute | solution.py:368
  147.5 3.9 %collective-permute-start.19 = (f32[8,384]{1,0:T(8,128)S(1)}, f32[8,384]{1,0:T(8,128)S(1)}, u32[]{:S(2)}, u32[]{:S(2)}) collective-permute-start(f32[8,384]{1,0:T(8,128)S(1)} %get-tuple-element.54.s0), channel_id=1, source_target_pairs={{0,2},{2,4},{4,6},{6,0},{1,3},{3,5},{5,7},{7,1},{8,10},{10,12},{12... | collective-permute-start | bytes 36872 | tf_op jit(solution)/shard_map/ppermute | solution.py:368
  152.6 3.8 %collective-permute-start.22 = (bf16[384,256]{1,0:T(8,128)(2,1)S(1)}, bf16[384,256]{1,0:T(8,128)(2,1)S(1)}, u32[]{:S(2)}, u32[]{:S(2)}) collective-permute-start(bf16[384,256]{1,0:T(8,128)(2,1)S(1)} %get-tuple-element.56), channel_id=1, source_target_pairs={{0,1},{1,0},{2,3},{3,2},{4,5},{5,4},{6,7},{7,6},{8,9},{9,8},{10,11... | collective-permute-start | bytes 589832 | tf_op jit(solution)/shard_map/ppermute | solution.py:451
  (3 other events, 199.4 us)
Sparse Core Ops, SparseCore 0:
  10.1 103.6 all-gather.2

commit v3 on v2

--- a/solution.py
+++ b/solution.py
@@ -14,6 +14,7 @@
 TP = ("x", "c")
 ROWS = 768
 HALF = 384
+QUARTER = 192
 TILE = 256
 TILES = ROWS // TILE
 HI = lax.Precision.HIGHEST
@@ -305,15 +306,23 @@
         loads[k].wait()
 
 
-def down_body(block, where_x, h, w, out):
+def down_body(block, where_x, h, w, top, bottom):
     rows = pl.ds(((where_x[0] + block) % 4) * 8, 8)
     got = dot(h[:, 0:1024], w[rows, 0].reshape(512, 1024), 1, 1)
-    out[...] = (got + dot(h[:, 1024:2048], w[rows, 1].reshape(512, 1024), 1, 1)).astype(BF)
-
-
-def second_body(resid, own, r1, r2, r3, second, stats):
-    total = own[...].astype(F32) + r1[...].astype(F32) + r2[...].astype(F32) + r3[...].astype(F32)
-    total = RES * resid[...].astype(F32) + total
+    got = (got + dot(h[:, 1024:2048], w[rows, 1].reshape(512, 1024), 1, 1)).astype(BF)
+    top[...] = got[0:QUARTER]
+    bottom[...] = got[QUARTER:]
+
+
+def join_body(a, b, c, d, left, right):
+    left[...] = (a[...].astype(F32) + b[...].astype(F32)).astype(BF)
+    right[...] = (c[...].astype(F32) + d[...].astype(F32)).astype(BF)
+
+
+def second_body(resid, own_top, own_bottom, top1, bottom1, top3, bottom3, second, stats):
+    top = own_top[...].astype(F32) + top1[...].astype(F32) + top3[...].astype(F32)
+    bottom = own_bottom[...].astype(F32) + bottom1[...].astype(F32) + bottom3[...].astype(F32)
+    total = RES * resid[...].astype(F32) + jnp.concatenate([top, bottom], axis=0)
     second[...] = total
     s1 = jnp.transpose(jnp.broadcast_to(jnp.sum(total, axis=1, keepdims=True), (HALF, 128)))[0:8, :]
     s2 = jnp.transpose(jnp.broadcast_to(jnp.sum(total * total, axis=1, keepdims=True), (HALF, 128)))[0:8, :]
@@ -437,12 +446,19 @@
     )(at_x, near(p0), near(p1), near(p2), near(p3), off(weights))
 
     def down(k):
-        return call(partial(down_body, k), 3, [((HALF, 512), BF)], scalars=1)(at_x, hidden, down_weights)[0]
-
-    d2, d1, d3, d0 = down(2), down(1), down(3), down(0)
-    q2, q1, q3 = around(d2, 2), around(d1, 1), around(d3, 3)
-    second, stats = call(second_body, 5, [((HALF, 512), F32), ((8, HALF), F32)])(
-        resid, d0, q1, q2, q3
+        return call(partial(down_body, k), 3, [((QUARTER, 512), BF)] * 2, scalars=1)(at_x, hidden, down_weights)
+
+    far_top, far_bottom = down(2)
+    far_top, far_bottom = around(far_top, 1), around(far_bottom, 3)
+    next_top, next_bottom = down(1)
+    next_bottom = around(next_bottom, 1)
+    back_top, back_bottom = down(3)
+    back_top = around(back_top, 3)
+    own_top, own_bottom = down(0)
+    next_top, back_bottom = call(join_body, 4, [((QUARTER, 512), BF)] * 2)(next_top, far_top, back_bottom, far_bottom)
+    next_top, back_bottom = around(next_top, 1), around(back_bottom, 3)
+    second, stats = call(second_body, 7, [((HALF, 512), F32), ((8, HALF), F32)])(
+        resid, own_top, own_bottom, next_top, next_bottom, back_top, back_bottom
     )
     s1, s2, s3 = around(stats, 1), around(stats, 2), around(stats, 3)
     full, send = call(last_body, 8, [((ROWS, 256), BF), ((HALF, 256), BF)], scalars=1, plain=(0,))(

time: 164 us -> 157 us (0.957)
  waiting for transfers between devices: 61.5 us -> 52.7 us
    ppermute x12 -> x15, waiting for transfers between devices: 52.7 us -> 44 us  [around(): return lax.ppermute(a, 'x', [(i, (i + by) % 4) for i in range(4)])]
    ppermute x12 -> x15, starting transfers between devices: 16.7 us -> 17.2 us  [around(): return lax.ppermute(a, 'x', [(i, (i + by) % 4) for i in range(4)])]
    pallas_call x12 -> x13, Pallas kernels: 18.8 us -> 18.9 us  [call(): run(*[off(b) if k in far else b if k < scalars else near(b) for k, b in e...]
  transfers between devices with their start and end apart: 24 -> 27, of which waited for: 15 -> 18; matrix products, arithmetic and copies ran while one was open for 2% -> 2% of each run, Pallas kernels for 9% -> 10%
where the time goes in v3:
time: 157 us
  waiting for transfers between devices  52.7 us (34%)
  starting transfers between devices  44.7 us (28%)
  Pallas kernels  25 us (16%)
  blocking collectives  15 us (10%)
  between operations  13.6 us (9%)
  local copies, waits for them, and re-layouts  3.93 us (3%)
  other arithmetic  1.76 us (1%)
    ppermute x15, waiting for transfers between devices, around(): return lax.ppermute(a, 'x', [(i, (i + by) % 4) for i in range(4)])  44 us
    pallas_call x13, Pallas kernels, call(): run(*[off(b) if k in far else b if k < scalars else near(b) for k, b in e...  18.9 us
    ppermute x15, starting transfers between devices, around(): return lax.ppermute(a, 'x', [(i, (i + by) % 4) for i in range(4)])  17.2 us
    all_gather x1, blocking collectives, layer(): rows = lax.all_gather(pay, 'y')  15 us
    ppermute x6, starting transfers between devices, shift(): lax.ppermute(a, axis, [(i, i + by) for i in range(count) if 0 <= i + by <...  14.4 us
    pallas_call x1, Pallas kernels, layer(): pl.pallas_call(up_body, in_specs=[sm()] + [vm()] * 4 + [pl.BlockSpec(memo...  6.11 us
    ppermute x1, starting transfers between devices, layer(): other = lax.ppermute(send, 'c', swap)  4.53 us
    ppermute x6, waiting for transfers between devices, shift(): lax.ppermute(a, axis, [(i, i + by) for i in range(count) if 0 <= i + by <...  4.47 us
  transfers between devices with their start and end apart: 27, of which 18 were waited for; matrix products, arithmetic and copies ran while one was open for 2% of the time, Pallas kernels for 10%

profile of v3, /device:TPU:1, one launch (start us, length us, event | category | flops | bytes accessed | tf_op | source)
XLA Modules:
  0.0 156.7 jit_solution(3182020768022305737)
XLA Ops:
  6.5 1.7 %pad_maximum_fusion = bf16[64,2048]{1,0:T(8,128)(2,1)} fusion(bf16[64,1024]{1,0:T(8,128)(2,1)} %param.37, bf16[64,1024]{1,0:T(8,128)(2,1)} %param.36), kind=kLoop, calls=%fused_computation | loop fusion | flops 524288 | bytes 524288 | tf_op jit(solution)/shard_map/concatenate | solution.py:384
  8.3 3.3 %collective-permute-start.7 = (bf16[256,2048]{1,0:T(8,128)(2,1)}, bf16[256,2048]{1,0:T(8,128)(2,1)S(1)}, u32[]{:S(2)}, u32[]{:S(2)}) collective-permute-start(bf16[256,2048]{1,0:T(8,128)(2,1)} %wa.1), channel_id=1, source_target_pairs={{0,1},{1,0},{2,3},{3,2},{4,5},{5,4},{6,7},{7,6},{8,9},{9,8},{10,11... | collective-permute-start | bytes 3145736 | tf_op jit(solution)/shard_map/ppermute | solution.py:387
  13.0 1.5 collective-permute-start
  18.9 5.0 %shard_map.181 = (bf16[768,256]{1,0:T(8,128)(2,1)S(1)}, bf16[768,128]{1,0:T(8,128)(2,1)S(1)}, bf16[768,128]{1,0:T(8,128)(2,1)S(1)}, f32[8,768]{1,0:T(8,128)S(1)}...) custom-call(s32[1]{0:T(128)} %bitcast.2.sp, ...), custom_call_target="tpu_custom_call" | custom-call | tf_op jit(solution)/shard_map/pallas_call | solution.py:50
  23.9 15.0 %all-gather = bf16[576,512]{1,0:T(8,128)(2,1)S(1)} all-gather(bf16[144,512]{1,0:T(8,128)(2,1)S(1)} %get-tuple-element.50), channel_id=2, replica_groups=mesh['z'=8,'y'=4,'x'=4,'c'=2] {'y'}, dimensions={0}, use_global_device_ids=true | all-gather | bytes 737280 | tf_op jit(solution)/shard_map/all_gather | solution.py:407
  39.1 5.2 %collective-permute-start.3 = (bf16[144,256]{1,0:T(8,128)(2,1)S(1)}, bf16[144,256]{1,0:T(8,128)(2,1)S(1)}, u32[]{:S(2)}, u32[]{:S(2)}) collective-permute-start(bf16[144,256]{1,0:T(8,128)(2,1)S(1)} %get-tuple-element.52), channel_id=1, source_target_pairs={{0,64},{32,96},{64,128},{96,160},{128,192},{160,224},{1,65},{33,97... | collective-permute-start | bytes 221192 | tf_op jit(solution)/shard_map/ppermute | solution.py:374
  44.3 3.8 %collective-permute-start.2 = (bf16[144,256]{1,0:T(8,128)(2,1)S(1)}, bf16[144,256]{1,0:T(8,128)(2,1)S(1)}, u32[]{:S(2)}, u32[]{:S(2)}) collective-permute-start(bf16[144,256]{1,0:T(8,128)(2,1)S(1)} %get-tuple-element.52), channel_id=1, source_target_pairs={{0,32},{32,64},{64,96},{96,128},{128,160},{160,192},{192,224},{1,3... | collective-permute-start | bytes 221192 | tf_op jit(solution)/shard_map/ppermute | solution.py:374
  50.7 2.2 %shard_map.182.yl = f32[768,256]{1,0:T(8,128)S(1)} custom-call(bf16[768,256]{1,0:T(8,128)(2,1)S(1)} %get-tuple-element.41.x, bf16[768,128]{1,0:T(8,128)(2,1)S(1)} %get-tuple-element.42.b, bf16[768,128]{1,0:T(8,128)(2,1)S(1)} %get-tuple-element.43.c, f32[8,768]{1,0:T(8,128)S(1)} %get-tuple-element.44.cum, f32[8,768]{1,0:T(8,128)S(1)} %get-tuple-element.45.dt, ...), custom_call_target="tpu_custom_call" | custom-call | tf_op jit(solution)/shard_map/pallas_call | solution.py:50
  52.9 1.9 %collective-permute-done.5.b2 = bf16[144,256]{1,0:T(8,128)(2,1)S(1)} collective-permute-done((bf16[144,256]{1,0:T(8,128)(2,1)S(1)}, bf16[144,256]{1,0:T(8,128)(2,1)S(1)}, u32[]{:S(2)}, u32[]{:S(2)}) %collective-permute-start.5) | collective-permute-done | bytes 73760 | tf_op jit(solution)/shard_map/ppermute | solution.py:374
  56.2 2.8 %shard_map.184 = (bf16[384,256]{1,0:T(8,128)(2,1)S(1)}, bf16[384,256]{1,0:T(8,128)(2,1)S(1)}) custom-call(s32[1]{0:T(128)} %bitcast.core, f32[768,256]{1,0:T(8,128)S(1)} %shard_map.182.yl, bf16[768,128]{1,0:T(8,128)(2,1)S(1)} %get-tuple-element.43.c, f32[8,768]{1,0:T(8,128)S(1)} %get-tuple-element.49.dev, f32[136,512]{1,0:T(8,128)S(1)} %get-tuple-element.51.pre, ...), custom_call_target="tpu_custom_call" | custom-call | tf_op jit(solution)/shard_map/pallas_call | solution.py:50
  59.0 4.5 %collective-permute-start.6 = (bf16[384,256]{1,0:T(8,128)(2,1)S(1)}, bf16[384,256]{1,0:T(8,128)(2,1)S(1)}, u32[]{:S(2)}, u32[]{:S(2)}) collective-permute-start(bf16[384,256]{1,0:T(8,128)(2,1)S(1)} %get-tuple-element.55), channel_id=1, source_target_pairs={{0,1},{1,0},{2,3},{3,2},{4,5},{5,4},{6,7},{7,6},{8,9},{9,8},{10,11... | collective-permute-start | bytes 589832 | tf_op jit(solution)/shard_map/ppermute | solution.py:417
  64.6 2.5 %shard_map.185 = (bf16[384,512]{1,0:T(8,128)(2,1)S(1)}, bf16[384,512]{1,0:T(8,128)(2,1)S(1)}, bf16[384,512]{1,0:T(8,128)(2,1)S(1)}, bf16[384,512]{1,0:T(8,128)(2,1)S(1)}) custom-call(s32[1]{0:T(128)} %bitcast.1.where_x, bf16[384,256]{1,0:T(8,128)(2,1)S(1)} %get-tuple-element.54.a, bf16[384,256]{1,0:T(8,128)(2,1)S(1)} %collective-permute-done.6.b, ...), custom_call_target="tpu_custom_call" | custom-call | tf_op jit(solution)/shard_map/pallas_call | solution.py:50
  68.4 2.4 %collective-permute-start.10 = (bf16[384,512]{1,0:T(8,128)(2,1)S(1)}, bf16[384,512]{1,0:T(8,128)(2,1)S(1)}, u32[]{:S(2)}, u32[]{:S(2)}) collective-permute-start(bf16[384,512]{1,0:T(8,128)(2,1)S(1)} %get-tuple-element.58), channel_id=1, source_target_pairs={{0,4},{2,6},{4,0},{6,2},{1,5},{3,7},{5,1},{7,3},{8,12},{10,14},{12... | collective-permute-start | bytes 1179656 | tf_op jit(solution)/shard_map/ppermute | solution.py:377
  74.8 4.0 %collective-permute-done.9.r1 = bf16[384,512]{1,0:T(8,128)(2,1)S(1)} collective-permute-done((bf16[384,512]{1,0:T(8,128)(2,1)S(1)}, bf16[384,512]{1,0:T(8,128)(2,1)S(1)}, u32[]{:S(2)}, u32[]{:S(2)}) %collective-permute-start.9) | collective-permute-done | bytes 393248 | tf_op jit(solution)/shard_map/ppermute | solution.py:377
  78.8 9.3 %collective-permute-done.10.r2 = bf16[384,512]{1,0:T(8,128)(2,1)S(1)} collective-permute-done((bf16[384,512]{1,0:T(8,128)(2,1)S(1)}, bf16[384,512]{1,0:T(8,128)(2,1)S(1)}, u32[]{:S(2)}, u32[]{:S(2)}) %collective-permute-start.10) | collective-permute-done | bytes 393248 | tf_op jit(solution)/shard_map/ppermute | solution.py:377
  88.6 2.9 %collective-permute-start.15 = (bf16[400,512]{1,0:T(8,128)(2,1)S(1)}, bf16[400,512]{1,0:T(8,128)(2,1)S(1)}, u32[]{:S(2)}, u32[]{:S(2)}) collective-permute-start(bf16[400,512]{1,0:T(8,128)(2,1)S(1)} %shard_map.186.p0), channel_id=1, source_target_pairs={{0,6},{2,0},{4,2},{6,4},{1,7},{3,1},{5,3},{7,5},{8,14},{10,8},{12,... | collective-permute-start | bytes 1228808 | tf_op jit(solution)/shard_map/ppermute | solution.py:377
  92.1 16.4 %collective-permute-done.15.p3 = bf16[400,512]{1,0:T(8,128)(2,1)S(1)} collective-permute-done((bf16[400,512]{1,0:T(8,128)(2,1)S(1)}, bf16[400,512]{1,0:T(8,128)(2,1)S(1)}, u32[]{:S(2)}, u32[]{:S(2)}) %collective-permute-start.15) | collective-permute-done | bytes 409632 | tf_op jit(solution)/shard_map/ppermute | solution.py:377
  108.5 4.4 %collective-permute-done.13.p1 = bf16[400,512]{1,0:T(8,128)(2,1)S(1)} collective-permute-done((bf16[400,512]{1,0:T(8,128)(2,1)S(1)}, bf16[400,512]{1,0:T(8,128)(2,1)S(1)}, u32[]{:S(2)}, u32[]{:S(2)}) %collective-permute-start.13) | collective-permute-done | bytes 409632 | tf_op jit(solution)/shard_map/ppermute | solution.py:377
  113.8 6.1 %up.1 = (bf16[384,2048]{1,0:T(8,128)(2,1)S(1)}, bf16[384,512]{1,0:T(8,128)(2,1)S(1)}, bf16[32,2,64,1024]{3,2,1,0:T(8,128)(2,1)S(1)}) custom-call(s32[1]{0:T(128)} %bitcast.1.where_x, bf16[400,512]{1,0:T(8,128)(2,1)S(1)} %shard_map.186.p0, bf16[400,512]{1,0:T(8,128)(2,1)S(1)} %collective-permute-done.13.p1, bf16[400,512]{1,0:T(8,128)(2,1)S(1)} %collective-permute-done.14.p2, ...), custom_call_target="tpu_custom_call" | custom-call | tf_op jit(solution)/shard_map/up/pallas_call | solution.py:430
  122.3 1.5 collective-permute-start.17
  129.8 1.8 %collective-permute-start.21 = (bf16[192,512]{1,0:T(8,128)(2,1)S(1)}, bf16[192,512]{1,0:T(8,128)(2,1)S(1)}, u32[]{:S(2)}, u32[]{:S(2)}) collective-permute-start(bf16[192,512]{1,0:T(8,128)(2,1)S(1)} %get-tuple-element.72), channel_id=1, source_target_pairs={{0,6},{2,0},{4,2},{6,4},{1,7},{3,1},{5,3},{7,5},{8,14},{10,8},{12,... | collective-permute-start | bytes 589832 | tf_op jit(solution)/shard_map/ppermute | solution.py:377
  133.6 4.2 %collective-permute-done.18.top1 = bf16[192,512]{1,0:T(8,128)(2,1)S(1)} collective-permute-done((bf16[192,512]{1,0:T(8,128)(2,1)S(1)}, bf16[192,512]{1,0:T(8,128)(2,1)S(1)}, u32[]{:S(2)}, u32[]{:S(2)}) %collective-permute-start.18) | collective-permute-done | bytes 196640 | tf_op jit(solution)/shard_map/ppermute | solution.py:377
  140.9 2.0 %collective-permute-done.23.s2 = f32[8,384]{1,0:T(8,128)S(1)} collective-permute-done((f32[8,384]{1,0:T(8,128)S(1)}, f32[8,384]{1,0:T(8,128)S(1)}, u32[]{:S(2)}, u32[]{:S(2)}) %collective-permute-start.23) | collective-permute-done | bytes 12320 | tf_op jit(solution)/shard_map/ppermute | solution.py:377
  144.4 3.6 %collective-permute-start.25 = (bf16[384,256]{1,0:T(8,128)(2,1)S(1)}, bf16[384,256]{1,0:T(8,128)(2,1)S(1)}, u32[]{:S(2)}, u32[]{:S(2)}) collective-permute-start(bf16[384,256]{1,0:T(8,128)(2,1)S(1)} %get-tuple-element.76), channel_id=1, source_target_pairs={{0,1},{1,0},{2,3},{3,2},{4,5},{5,4},{6,7},{7,6},{8,9},{9,8},{10,11... | collective-permute-start | bytes 589832 | tf_op jit(solution)/shard_map/ppermute | solution.py:467
  (62 shorter events, 34.9 us)
Async XLA Ops:
  6.5 107.3 %all-gather.3.cloned.1.call-start = ((), (), s32[]{:S(2)}) async-start(), calls=%async_computation | async-start | bytes 17039360 | tf_op jit(solution)/shard_map/all_gather | solution.py:385
  8.3 56.3 %collective-permute-start.7 = (bf16[256,2048]{1,0:T(8,128)(2,1)}, bf16[256,2048]{1,0:T(8,128)(2,1)S(1)}, u32[]{:S(2)}, u32[]{:S(2)}) collective-permute-start(bf16[256,2048]{1,0:T(8,128)(2,1)} %wa.1), channel_id=1, source_target_pairs={{0,1},{1,0},{2,3},{3,2},{4,5},{5,4},{6,7},{7,6},{8,9},{9,8},{10,11... | collective-permute-start | bytes 3145736 | tf_op jit(solution)/shard_map/ppermute | solution.py:387
  13.0 4.6 %collective-permute-start = (bf16[2,512]{1,0:T(2,128)(2,1)S(1)}, bf16[2,512]{1,0:T(2,128)(2,1)S(1)}, u32[]{:S(2)}, u32[]{:S(2)}) collective-permute-start(bf16[2,512]{1,0:T(2,128)(2,1)S(1)} %pad_maximum_fusion.1), channel_id=1, source_target_pairs={{0,8},{8,16},{16,24},{24,32},{32,40},{40,48},{48,56},{56,64},{64,7... | collective-permute-start | bytes 6152 | tf_op jit(solution)/shard_map/ppermute | solution.py:374
  14.6 4.3 %collective-permute-start.1 = (bf16[2,512]{1,0:T(2,128)(2,1)S(1)}, bf16[2,512]{1,0:T(2,128)(2,1)S(1)}, u32[]{:S(2)}, u32[]{:S(2)}) collective-permute-start(bf16[2,512]{1,0:T(2,128)(2,1)S(1)} %pad_maximum_fusion.2), channel_id=1, source_target_pairs={{8,0},{16,8},{24,16},{32,24},{40,32},{48,40},{56,48},{64,56},{72,6... | collective-permute-start | bytes 6152 | tf_op jit(solution)/shard_map/ppermute | solution.py:374
  39.1 13.8 %collective-permute-start.3 = (bf16[144,256]{1,0:T(8,128)(2,1)S(1)}, bf16[144,256]{1,0:T(8,128)(2,1)S(1)}, u32[]{:S(2)}, u32[]{:S(2)}) collective-permute-start(bf16[144,256]{1,0:T(8,128)(2,1)S(1)} %get-tuple-element.52), channel_id=1, source_target_pairs={{0,64},{32,96},{64,128},{96,160},{128,192},{160,224},{1,65},{33,97... | collective-permute-start | bytes 221192 | tf_op jit(solution)/shard_map/ppermute | solution.py:374
  44.3 8.6 %collective-permute-start.2 = (bf16[144,256]{1,0:T(8,128)(2,1)S(1)}, bf16[144,256]{1,0:T(8,128)(2,1)S(1)}, u32[]{:S(2)}, u32[]{:S(2)}) collective-permute-start(bf16[144,256]{1,0:T(8,128)(2,1)S(1)} %get-tuple-element.52), channel_id=1, source_target_pairs={{0,32},{32,64},{64,96},{96,128},{128,160},{160,192},{192,224},{1,3... | collective-permute-start | bytes 221192 | tf_op jit(solution)/shard_map/ppermute | solution.py:374
  48.1 6.7 %collective-permute-start.5 = (bf16[144,256]{1,0:T(8,128)(2,1)S(1)}, bf16[144,256]{1,0:T(8,128)(2,1)S(1)}, u32[]{:S(2)}, u32[]{:S(2)}) collective-permute-start(bf16[144,256]{1,0:T(8,128)(2,1)S(1)} %get-tuple-element.53), channel_id=1, source_target_pairs={{64,0},{96,32},{128,64},{160,96},{192,128},{224,160},{65,1},{97,33... | collective-permute-start | bytes 221192 | tf_op jit(solution)/shard_map/ppermute | solution.py:374
  49.4 6.7 %collective-permute-start.4 = (bf16[144,256]{1,0:T(8,128)(2,1)S(1)}, bf16[144,256]{1,0:T(8,128)(2,1)S(1)}, u32[]{:S(2)}, u32[]{:S(2)}) collective-permute-start(bf16[144,256]{1,0:T(8,128)(2,1)S(1)} %get-tuple-element.53), channel_id=1, source_target_pairs={{32,0},{64,32},{96,64},{128,96},{160,128},{192,160},{224,192},{33,... | collective-permute-start | bytes 221192 | tf_op jit(solution)/shard_map/ppermute | solution.py:374
  59.0 5.6 %collective-permute-start.6 = (bf16[384,256]{1,0:T(8,128)(2,1)S(1)}, bf16[384,256]{1,0:T(8,128)(2,1)S(1)}, u32[]{:S(2)}, u32[]{:S(2)}) collective-permute-start(bf16[384,256]{1,0:T(8,128)(2,1)S(1)} %get-tuple-element.55), channel_id=1, source_target_pairs={{0,1},{1,0},{2,3},{3,2},{4,5},{5,4},{6,7},{7,6},{8,9},{9,8},{10,11... | collective-permute-start | bytes 589832 | tf_op jit(solution)/shard_map/ppermute | solution.py:417
  67.1 11.7 %collective-permute-start.9 = (bf16[384,512]{1,0:T(8,128)(2,1)S(1)}, bf16[384,512]{1,0:T(8,128)(2,1)S(1)}, u32[]{:S(2)}, u32[]{:S(2)}) collective-permute-start(bf16[384,512]{1,0:T(8,128)(2,1)S(1)} %get-tuple-element.57), channel_id=1, source_target_pairs={{0,2},{2,4},{4,6},{6,0},{1,3},{3,5},{5,7},{7,1},{8,10},{10,12},{12... | collective-permute-start | bytes 1179656 | tf_op jit(solution)/shard_map/ppermute | solution.py:377
  68.4 19.7 %collective-permute-start.10 = (bf16[384,512]{1,0:T(8,128)(2,1)S(1)}, bf16[384,512]{1,0:T(8,128)(2,1)S(1)}, u32[]{:S(2)}, u32[]{:S(2)}) collective-permute-start(bf16[384,512]{1,0:T(8,128)(2,1)S(1)} %get-tuple-element.58), channel_id=1, source_target_pairs={{0,4},{2,6},{4,0},{6,2},{1,5},{3,7},{5,1},{7,3},{8,12},{10,14},{12... | collective-permute-start | bytes 1179656 | tf_op jit(solution)/shard_map/ppermute | solution.py:377
  70.9 17.3 %collective-permute-start.11 = (bf16[384,512]{1,0:T(8,128)(2,1)S(1)}, bf16[384,512]{1,0:T(8,128)(2,1)S(1)}, u32[]{:S(2)}, u32[]{:S(2)}) collective-permute-start(bf16[384,512]{1,0:T(8,128)(2,1)S(1)} %get-tuple-element.59), channel_id=1, source_target_pairs={{0,6},{2,0},{4,2},{6,4},{1,7},{3,1},{5,3},{7,5},{8,14},{10,8},{12,... | collective-permute-start | bytes 1179656 | tf_op jit(solution)/shard_map/ppermute | solution.py:377
  88.6 19.9 %collective-permute-start.15 = (bf16[400,512]{1,0:T(8,128)(2,1)S(1)}, bf16[400,512]{1,0:T(8,128)(2,1)S(1)}, u32[]{:S(2)}, u32[]{:S(2)}) collective-permute-start(bf16[400,512]{1,0:T(8,128)(2,1)S(1)} %shard_map.186.p0), channel_id=1, source_target_pairs={{0,6},{2,0},{4,2},{6,4},{1,7},{3,1},{5,3},{7,5},{8,14},{10,8},{12,... | collective-permute-start | bytes 1228808 | tf_op jit(solution)/shard_map/ppermute | solution.py:377
  91.4 17.1 %collective-permute-start.14 = (bf16[400,512]{1,0:T(8,128)(2,1)S(1)}, bf16[400,512]{1,0:T(8,128)(2,1)S(1)}, u32[]{:S(2)}, u32[]{:S(2)}) collective-permute-start(bf16[400,512]{1,0:T(8,128)(2,1)S(1)} %shard_map.186.p0), channel_id=1, source_target_pairs={{0,4},{2,6},{4,0},{6,2},{1,5},{3,7},{5,1},{7,3},{8,12},{10,14},{12... | collective-permute-start | bytes 1228808 | tf_op jit(solution)/shard_map/ppermute | solution.py:377
  91.6 21.3 %collective-permute-start.13 = (bf16[400,512]{1,0:T(8,128)(2,1)S(1)}, bf16[400,512]{1,0:T(8,128)(2,1)S(1)}, u32[]{:S(2)}, u32[]{:S(2)}) collective-permute-start(bf16[400,512]{1,0:T(8,128)(2,1)S(1)} %shard_map.186.p0), channel_id=1, source_target_pairs={{0,2},{2,4},{4,6},{6,0},{1,3},{3,5},{5,7},{7,1},{8,10},{10,12},{12... | collective-permute-start | bytes 1228808 | tf_op jit(solution)/shard_map/ppermute | solution.py:377
  121.0 7.5 %collective-permute-start.16 = (bf16[192,512]{1,0:T(8,128)(2,1)S(1)}, bf16[192,512]{1,0:T(8,128)(2,1)S(1)}, u32[]{:S(2)}, u32[]{:S(2)}) collective-permute-start(bf16[192,512]{1,0:T(8,128)(2,1)S(1)} %get-tuple-element.66), channel_id=1, source_target_pairs={{0,2},{2,4},{4,6},{6,0},{1,3},{3,5},{5,7},{7,1},{8,10},{10,12},{12... | collective-permute-start | bytes 589832 | tf_op jit(solution)/shard_map/ppermute | solution.py:377
  122.3 6.2 %collective-permute-start.17 = (bf16[192,512]{1,0:T(8,128)(2,1)S(1)}, bf16[192,512]{1,0:T(8,128)(2,1)S(1)}, u32[]{:S(2)}, u32[]{:S(2)}) collective-permute-start(bf16[192,512]{1,0:T(8,128)(2,1)S(1)} %get-tuple-element.68), channel_id=1, source_target_pairs={{0,6},{2,0},{4,2},{6,4},{1,7},{3,1},{5,3},{7,5},{8,14},{10,8},{12,... | collective-permute-start | bytes 589832 | tf_op jit(solution)/shard_map/ppermute | solution.py:377
  125.8 6.9 %collective-permute-start.20 = (bf16[192,512]{1,0:T(8,128)(2,1)S(1)}, bf16[192,512]{1,0:T(8,128)(2,1)S(1)}, u32[]{:S(2)}, u32[]{:S(2)}) collective-permute-start(bf16[192,512]{1,0:T(8,128)(2,1)S(1)} %get-tuple-element.71), channel_id=1, source_target_pairs={{0,6},{2,0},{4,2},{6,4},{1,7},{3,1},{5,3},{7,5},{8,14},{10,8},{12,... | collective-permute-start | bytes 589832 | tf_op jit(solution)/shard_map/ppermute | solution.py:377
  127.1 6.6 %collective-permute-start.19 = (bf16[192,512]{1,0:T(8,128)(2,1)S(1)}, bf16[192,512]{1,0:T(8,128)(2,1)S(1)}, u32[]{:S(2)}, u32[]{:S(2)}) collective-permute-start(bf16[192,512]{1,0:T(8,128)(2,1)S(1)} %get-tuple-element.70), channel_id=1, source_target_pairs={{0,2},{2,4},{4,6},{6,0},{1,3},{3,5},{5,7},{7,1},{8,10},{10,12},{12... | collective-permute-start | bytes 589832 | tf_op jit(solution)/shard_map/ppermute | solution.py:377
  128.6 9.3 %collective-permute-start.18 = (bf16[192,512]{1,0:T(8,128)(2,1)S(1)}, bf16[192,512]{1,0:T(8,128)(2,1)S(1)}, u32[]{:S(2)}, u32[]{:S(2)}) collective-permute-start(bf16[192,512]{1,0:T(8,128)(2,1)S(1)} %get-tuple-element.69), channel_id=1, source_target_pairs={{0,2},{2,4},{4,6},{6,0},{1,3},{3,5},{5,7},{7,1},{8,10},{10,12},{12... | collective-permute-start | bytes 589832 | tf_op jit(solution)/shard_map/ppermute | solution.py:377
  129.8 8.1 %collective-permute-start.21 = (bf16[192,512]{1,0:T(8,128)(2,1)S(1)}, bf16[192,512]{1,0:T(8,128)(2,1)S(1)}, u32[]{:S(2)}, u32[]{:S(2)}) collective-permute-start(bf16[192,512]{1,0:T(8,128)(2,1)S(1)} %get-tuple-element.72), channel_id=1, source_target_pairs={{0,6},{2,0},{4,2},{6,4},{1,7},{3,1},{5,3},{7,5},{8,14},{10,8},{12,... | collective-permute-start | bytes 589832 | tf_op jit(solution)/shard_map/ppermute | solution.py:377
  138.9 4.0 %collective-permute-start.23 = (f32[8,384]{1,0:T(8,128)S(1)}, f32[8,384]{1,0:T(8,128)S(1)}, u32[]{:S(2)}, u32[]{:S(2)}) collective-permute-start(f32[8,384]{1,0:T(8,128)S(1)} %get-tuple-element.74.s0), channel_id=1, source_target_pairs={{0,4},{2,6},{4,0},{6,2},{1,5},{3,7},{5,1},{7,3},{8,12},{10,14},{12... | collective-permute-start | bytes 36872 | tf_op jit(solution)/shard_map/ppermute | solution.py:377
  139.2 4.1 %collective-permute-start.22 = (f32[8,384]{1,0:T(8,128)S(1)}, f32[8,384]{1,0:T(8,128)S(1)}, u32[]{:S(2)}, u32[]{:S(2)}) collective-permute-start(f32[8,384]{1,0:T(8,128)S(1)} %get-tuple-element.74.s0), channel_id=1, source_target_pairs={{0,2},{2,4},{4,6},{6,0},{1,3},{3,5},{5,7},{7,1},{8,10},{10,12},{12... | collective-permute-start | bytes 36872 | tf_op jit(solution)/shard_map/ppermute | solution.py:377
  144.4 4.7 %collective-permute-start.25 = (bf16[384,256]{1,0:T(8,128)(2,1)S(1)}, bf16[384,256]{1,0:T(8,128)(2,1)S(1)}, u32[]{:S(2)}, u32[]{:S(2)}) collective-permute-start(bf16[384,256]{1,0:T(8,128)(2,1)S(1)} %get-tuple-element.76), channel_id=1, source_target_pairs={{0,1},{1,0},{2,3},{3,2},{4,5},{5,4},{6,7},{7,6},{8,9},{9,8},{10,11... | collective-permute-start | bytes 589832 | tf_op jit(solution)/shard_map/ppermute | solution.py:467
  (6 other events, 206.1 us)
Sparse Core Ops, SparseCore 0:
  10.1 103.6 all-gather.2

commit v4 on v3

--- a/solution.py
+++ b/solution.py
@@ -1,5 +1,3 @@
-from functools import partial
-
 import jax
 import jax.numpy as jnp
 from jax import lax
@@ -152,10 +150,12 @@
     pg = [q[:, 256:512] for q in passing]
     f2 = f[1] + pf[1] * f[0]
     g0 = g[1] + pg[1] * g[2]
-    si_out[0] = f[0].astype(BF)
-    si_out[1] = f2.astype(BF)
-    si_out[2] = g0.astype(BF)
-    si_out[3] = g[2].astype(BF)
+    si_out[0] = jnp.zeros((128, 256), BF)
+    si_out[1] = f[0].astype(BF)
+    si_out[2] = f2.astype(BF)
+    si_out[3] = g0.astype(BF)
+    si_out[4] = g[2].astype(BF)
+    si_out[5] = jnp.zeros((128, 256), BF)
     pay_out[0:128, 0:256] = (f[2] + pf[2] * f2).astype(BF)
     pay_out[0:128, 256:512] = (g[0] + pg[0] * g0).astype(BF)
     whole = passing[0] * passing[1] * passing[2]
@@ -167,8 +167,10 @@
     lower = iota((TILE, TILE), 0) > iota((TILE, TILE), 1)
     upper = iota((TILE, TILE), 0) < iota((TILE, TILE), 1)
     side = iota((TILE, 128), 1) < 64
-    for i in range(TILES):
-        cols = slice(i * TILE, (i + 1) * TILE)
+
+    @pl.loop(0, TILES)
+    def _(i):
+        cols = pl.ds(pl.multiple_of(i * TILE, TILE), TILE)
         cc = c[cols, :]
         score = dot(cc, b[cols, :], 1, 1)
         cum_row = cum[:, cols]
@@ -192,10 +194,8 @@
             part = jnp.where(side, got[0], got[1])
             lanes = slice(pair * 128, pair * 128 + 128)
             wide = slice(256 + pair * 128, 384 + pair * 128)
-            if i > 0:
-                part = part + dot(cc, si[i - 1][:, lanes], 1, 0) * carried[:, lanes]
-            if i < TILES - 1:
-                part = part + dot(cc, si[i + 2][:, lanes], 1, 0) * carried[:, wide]
+            part = part + dot(cc, si[i, :, lanes], 1, 0) * carried[:, lanes]
+            part = part + dot(cc, si[i + 3, :, lanes], 1, 0) * carried[:, wide]
             y_out[cols, lanes] = part
 
 
@@ -224,8 +224,10 @@
         more = near[128:144, :].astype(F32)[0:1, :] * far[0:128, :].astype(F32)
         come = near[0:128, :].astype(F32) + more
         states.append((pre[0:128, lanes] + pre[128:129, lanes] * come).astype(BF))
-    for i in range(TILES):
-        cols = slice(i * TILE, (i + 1) * TILE)
+
+    @pl.loop(0, TILES)
+    def _(i):
+        cols = pl.ds(pl.multiple_of(i * TILE, TILE), TILE)
         wide = dot(dev[:, cols], spread, 0, 0, HI)
         y = yl[cols, :]
         y = y + dot(c[cols, :], states[0], 1, 0) * wide[:, 0:256]
@@ -234,6 +236,7 @@
         y = y * (z * jax.nn.sigmoid(z))
         y = y * lax.rsqrt(jnp.mean(y * y, axis=1, keepdims=True) + EPS)
         normed[cols, :] = (y * gain[...]).astype(BF)
+
     mine = pl.multiple_of(core[0] * HALF, HALF)
     other = pl.multiple_of(HALF - core[0] * HALF, HALF)
     keep[...] = normed[pl.ds(mine, HALF), :]
@@ -248,7 +251,7 @@
         out[...] = got.astype(BF)
 
 
-def first_body(core, own, stream_a, stream_b, r1, r2, r3, gain_a, gain_b, out, total, gain):
+def first_body(core, own, stream_a, stream_b, r1, r2, r3, gain_a, gain_b, top, bottom, total, gain):
     lane_a = pl.multiple_of(core[0] * 256, 256)
     lane_b = pl.multiple_of(256 - core[0] * 256, 256)
     total[:, pl.ds(lane_a, 256)] = stream_a[...].astype(F32)
@@ -258,7 +261,9 @@
     mix = own[...].astype(F32) + r1[...].astype(F32) + r2[...].astype(F32) + r3[...].astype(F32)
     first = RES * total[...] + mix
     mean = jnp.mean(first, axis=1, keepdims=True).astype(BF).astype(F32)
-    out[0:HALF, :] = (first - mean).astype(BF)
+    centred = (first - mean).astype(BF)
+    top[...] = centred[0:QUARTER]
+    bottom[0:QUARTER, :] = centred[QUARTER:]
     means = jnp.transpose(jnp.broadcast_to(mean, (HALF, 128)))[0:1, :]
     means = jnp.concatenate([means, jnp.zeros((1, 128), F32)], axis=1)
     g = gain[0:1, :]
@@ -267,26 +272,18 @@
     g2 = g - g0 - g1
     row = iota((16, 512), 0)
     tail = jnp.where(row == 0, means, jnp.where(row == 1, g0, jnp.where(row == 2, g1, jnp.where(row == 3, g2, 0.0))))
-    out[HALF : HALF + 16, :] = tail.astype(BF)
-
-
-def up_body(where_x, p0, p1, p2, p3, w, hidden, resid, down, xn, up, sems):
-    loads = []
-    for core in range(2):
-        for part in range(2):
-            lanes = slice(part * 512, part * 512 + 512)
-            loads.append((w.at[:, core, :, lanes], up.at[2 * core + part]))
-    for block in range(4):
-        rows = slice(block * 8, block * 8 + 8)
-        loads.append((w.at[rows, :, :, 1024:2048], down.at[rows]))
-    loads = [pltpu.make_async_copy(src, dst, sems.at[k]) for k, (src, dst) in enumerate(loads)]
-    for load in loads:
-        load.start()
-    blocks = (p0, p1, p2, p3)
-    tails = [p[HALF : HALF + 16, :].astype(F32) for p in blocks]
+    bottom[QUARTER : QUARTER + 16, :] = tail.astype(BF)
+
+
+def rows_body(where_x, t0, b0, t1, b1, t2, b2, t3, b3, xn, resid):
+    blocks = ((t0, b0), (t1, b1), (t2, b2), (t3, b3))
+    tails = [b[QUARTER : QUARTER + 16, :].astype(F32) for _, b in blocks]
     means = jnp.concatenate([t[0:1, 0:HALF] for t in tails] + [jnp.zeros((4, HALF), F32)], axis=0)
     mean_cols = jnp.transpose(means)
-    full = [p[0:HALF, :].astype(F32) + mean_cols[:, k : k + 1] for k, p in enumerate(blocks)]
+    full = [
+        jnp.concatenate([t[...], b[0:QUARTER, :]], axis=0).astype(F32) + mean_cols[:, k : k + 1]
+        for k, (t, b) in enumerate(blocks)
+    ]
     m = sum(jnp.sum(q, axis=1, keepdims=True) for q in full) / 2048.0
     full = [q - m for q in full]
     v = sum(jnp.sum(q * q, axis=1, keepdims=True) for q in full) / 2048.0
@@ -298,18 +295,51 @@
         xn[:, pl.ds(block, 512)] = done
         if k == 0:
             resid[...] = done
-    for k in range(4):
-        loads[k].wait()
+
+
+CHUNKS = 4
+
+
+def rows_of(w, where_x, block, to, sems):
+    loads = []
+    for k in range(2):
+        rows = pl.ds(((where_x[0] + block) % 4) * 8 + 4 * k, 4)
+        loads.append(pltpu.make_async_copy(w.at[rows, :, :, pl.ds(1024, 1024)], to.at[pl.ds(4 * k, 4)], sems[k]))
+    return loads
+
+
+def up_body(where_x, xn, w, hidden, far, after, back, up, sems):
+    loads = []
+    for k in range(CHUNKS):
+        src = w.at[:, k // 2, :, pl.ds((k % 2) * 512, 512)]
+        loads.append(pltpu.make_async_copy(src, up.at[k], sems.at[k]))
+    for j, (block, to) in enumerate(((2, far), (1, after), (3, back))):
+        loads += rows_of(w, where_x, block, to, [sems.at[CHUNKS + 2 * j], sems.at[CHUNKS + 2 * j + 1]])
+    for load in loads:
+        load.start()
+
+    @pl.loop(0, CHUNKS)
+    def _(k):
+        pltpu.make_async_copy(up.at[k], up.at[k], sems.at[k]).wait()
         got = jnp.maximum(dot(xn[...], up[k].reshape(2048, 512), 1, 0), 0.0)
-        hidden[:, k * 512 : k * 512 + 512] = (got * got).astype(BF)
-    for k in range(4, 8):
-        loads[k].wait()
-
-
-def down_body(block, where_x, h, w, top, bottom):
-    rows = pl.ds(((where_x[0] + block) % 4) * 8, 8)
-    got = dot(h[:, 0:1024], w[rows, 0].reshape(512, 1024), 1, 1)
-    got = (got + dot(h[:, 1024:2048], w[rows, 1].reshape(512, 1024), 1, 1)).astype(BF)
+        hidden[:, pl.ds(pl.multiple_of(k * 512, 512), 512)] = (got * got).astype(BF)
+
+    for load in loads[CHUNKS:]:
+        load.wait()
+
+
+def own_body(where_x, h, source, top, bottom, w, sems):
+    loads = rows_of(source, where_x, 0, w, [sems.at[0], sems.at[1]])
+    for load in loads:
+        load.start()
+    for load in loads:
+        load.wait()
+    down_body(h, w, top, bottom)
+
+
+def down_body(h, w, top, bottom):
+    got = dot(h[:, 0:1024], w[:, 0].reshape(512, 1024), 1, 1)
+    got = (got + dot(h[:, 1024:2048], w[:, 1].reshape(512, 1024), 1, 1)).astype(BF)
     top[...] = got[0:QUARTER]
     bottom[...] = got[QUARTER:]
 
@@ -395,7 +425,7 @@
         14,
         [((ROWS, 256), BF), ((ROWS, 128), BF), ((ROWS, 128), BF)]
         + [((8, ROWS), F32)] * 5
-        + [((4, 128, 256), BF), ((144, 512), BF)],
+        + [((6, 128, 256), BF), ((144, 512), BF)],
         scratch=[pltpu.VMEM((784, 512), F32)],
         scalars=3,
         far=(1, 2, 3, 4, 5, 8, 9, 10, 13),
@@ -419,42 +449,50 @@
         at_x, keep, other, mixer_output_weight, weight_other
     )
     r2, r1, r3 = around(o2, 2), around(o1, 1), around(o3, 3)
-    p0 = call(
+    top, bottom = call(
         first_body,
         9,
-        [((HALF + 16, 512), BF)],
+        [((QUARTER, 512), BF), ((QUARTER + 16, 512), BF)],
         scratch=[pltpu.VMEM((HALF, 512), F32), pltpu.VMEM((8, 512), F32)],
         scalars=1,
-    )(at_c, o0, stream_mine, stream_other, r1, r2, r3, gains, gains_other)[0]
-    p2, p1, p3 = around(p0, 2), around(p0, 1), around(p0, 3)
-    hidden, resid, down_weights = pl.pallas_call(
+    )(at_c, o0, stream_mine, stream_other, r1, r2, r3, gains, gains_other)
+    top1, bottom3 = around(top, 1), around(bottom, 3)
+    top3, bottom1 = around(top, 3), around(bottom, 1)
+    top2, bottom2 = around(top1, 1), around(bottom3, 3)
+    rows, resid = call(rows_body, 9, [((HALF, 2048), BF), ((HALF, 512), BF)], scalars=1)(
+        at_x, top, bottom, top1, bottom1, top2, bottom2, top3, bottom3
+    )
+    hidden, part2, part1, part3 = pl.pallas_call(
         up_body,
-        in_specs=[sm()] + [vm()] * 4 + [pl.BlockSpec(memory_space=pltpu.HBM)],
-        out_specs=[vm()] * 3,
-        out_shape=[
-            pltpu.VMEM((HALF, 2048), BF),
-            pltpu.VMEM((HALF, 512), BF),
-            pltpu.VMEM((32, 2, 64, 1024), BF),
-        ],
+        in_specs=[sm(), vm(), pl.BlockSpec(memory_space=pltpu.HBM)],
+        out_specs=[vm()] * 4,
+        out_shape=[pltpu.VMEM((HALF, 2048), BF)] + [pltpu.VMEM((8, 2, 64, 1024), BF)] * 3,
         scratch_shapes=[
-            pltpu.VMEM((HALF, 2048), BF),
-            pltpu.VMEM((4, 32, 64, 512), BF),
-            pltpu.SemaphoreType.DMA((8,)),
+            pltpu.VMEM((CHUNKS, 32, 64, 2048 // CHUNKS), BF),
+            pltpu.SemaphoreType.DMA((CHUNKS + 6,)),
         ],
         compiler_params=pltpu.CompilerParams(vmem_limit_bytes=32 * 2**20),
         name="up",
-    )(at_x, near(p0), near(p1), near(p2), near(p3), off(weights))
-
-    def down(k):
-        return call(partial(down_body, k), 3, [((QUARTER, 512), BF)] * 2, scalars=1)(at_x, hidden, down_weights)
-
-    far_top, far_bottom = down(2)
+    )(at_x, near(rows), off(weights))
+
+    def down(part):
+        return call(down_body, 2, [((QUARTER, 512), BF)] * 2)(hidden, part)
+
+    far_top, far_bottom = down(part2)
     far_top, far_bottom = around(far_top, 1), around(far_bottom, 3)
-    next_top, next_bottom = down(1)
+    next_top, next_bottom = down(part1)
     next_bottom = around(next_bottom, 1)
-    back_top, back_bottom = down(3)
+    back_top, back_bottom = down(part3)
     back_top = around(back_top, 3)
-    own_top, own_bottom = down(0)
+    own_top, own_bottom = pl.pallas_call(
+        own_body,
+        in_specs=[sm(), vm(), pl.BlockSpec(memory_space=pltpu.HBM)],
+        out_specs=[vm()] * 2,
+        out_shape=[pltpu.VMEM((QUARTER, 512), BF)] * 2,
+        scratch_shapes=[pltpu.VMEM((8, 2, 64, 1024), BF), pltpu.SemaphoreType.DMA((2,))],
+        compiler_params=pltpu.CompilerParams(vmem_limit_bytes=24 * 2**20),
+        name="down0",
+    )(at_x, near(hidden), off(weights))
     next_top, back_bottom = call(join_body, 4, [((QUARTER, 512), BF)] * 2)(next_top, far_top, back_bottom, far_bottom)
     next_top, back_bottom = around(next_top, 1), around(back_bottom, 3)
     second, stats = call(second_body, 7, [((HALF, 512), F32), ((8, HALF), F32)])(

time: 157 us -> 157 us (level)
  waiting for transfers between devices: 52.7 us -> 41.8 us
  starting transfers between devices: 44.7 us -> 52.1 us
  Pallas kernels: 25 us -> 28.6 us
    ppermute x15 -> x18, waiting for transfers between devices: 44 us -> 30 us  [around(): return lax.ppermute(a, 'x', [(i, (i + by) % 4) for i in range(4)])]
    ppermute x15 -> x18, starting transfers between devices: 17.2 us -> 25.2 us  [around(): return lax.ppermute(a, 'x', [(i, (i + by) % 4) for i in range(4)])]
    all_gather x1, waiting for transfers between devices: 0.95 us -> 4.54 us  [layer(): lax.all_gather(weights, ('z', 'y', 'c'), axis=0, tiled=True)]
    pallas_call x1 -> x2, Pallas kernels: 6.11 us -> 8.22 us  [the longest x1 5.64 us: layer(): pl.pallas_call(up_body, in_specs=[sm(), vm(), pl.BlockSpec(memory_space=p...]
  transfers between devices with their start and end apart: 27 -> 30, of which waited for: 18 -> 15; matrix products, arithmetic and copies ran while one was open for 2% -> 2% of each run, Pallas kernels for 10% -> 13%
where the time goes in v4:
time: 157 us
  starting transfers between devices  52.1 us (33%)
  waiting for transfers between devices  41.8 us (27%)
  Pallas kernels  28.6 us (18%)
  blocking collectives  14.8 us (9%)
  between operations  13.7 us (9%)
  local copies, waits for them, and re-layouts  3.94 us (3%)
  other arithmetic  1.71 us (1%)
    ppermute x18, waiting for transfers between devices, around(): return lax.ppermute(a, 'x', [(i, (i + by) % 4) for i in range(4)])  30 us
    ppermute x18, starting transfers between devices, around(): return lax.ppermute(a, 'x', [(i, (i + by) % 4) for i in range(4)])  25.2 us
    pallas_call x13, Pallas kernels, call(): run(*[off(b) if k in far else b if k < scalars else near(b) for k, b in e...  20.3 us
    all_gather x1, blocking collectives, layer(): rows = lax.all_gather(pay, 'y')  14.8 us
    ppermute x6, starting transfers between devices, shift(): lax.ppermute(a, axis, [(i, i + by) for i in range(count) if 0 <= i + by <...  14.6 us
    pallas_call x1, Pallas kernels, layer(): pl.pallas_call(up_body, in_specs=[sm(), vm(), pl.BlockSpec(memory_space=p...  5.64 us
    all_gather x1, waiting for transfers between devices, layer(): lax.all_gather(weights, ('z', 'y', 'c'), axis=0, tiled=True)  4.54 us
    ppermute x1, starting transfers between devices, layer(): other = lax.ppermute(send, 'c', swap)  4.41 us
  transfers between devices with their start and end apart: 30, of which 15 were waited for; matrix products, arithmetic and copies ran while one was open for 2% of the time, Pallas kernels for 13%

profile of v4, /device:TPU:1, one launch (start us, length us, event | category | flops | bytes accessed | tf_op | source)
XLA Modules:
  0.0 156.6 jit_solution(1164065393911605303)
XLA Ops:
  8.2 3.3 %collective-permute-start.7 = (bf16[256,2048]{1,0:T(8,128)(2,1)}, bf16[256,2048]{1,0:T(8,128)(2,1)S(1)}, u32[]{:S(2)}, u32[]{:S(2)}) collective-permute-start(bf16[256,2048]{1,0:T(8,128)(2,1)} %wa.1), channel_id=1, source_target_pairs={{0,1},{1,0},{2,3},{3,2},{4,5},{5,4},{6,7},{7,6},{8,9},{9,8},{10,11... | collective-permute-start | bytes 3145736 | tf_op jit(solution)/shard_map/ppermute | solution.py:417
  18.8 5.0 %shard_map.181 = (bf16[768,256]{1,0:T(8,128)(2,1)S(1)}, bf16[768,128]{1,0:T(8,128)(2,1)S(1)}, bf16[768,128]{1,0:T(8,128)(2,1)S(1)}, f32[8,768]{1,0:T(8,128)S(1)}...) custom-call(s32[1]{0:T(128)} %bitcast.2.sp, ...), custom_call_target="tpu_custom_call" | custom-call | tf_op jit(solution)/shard_map/pallas_call | solution.py:48
  23.9 14.8 %all-gather = bf16[576,512]{1,0:T(8,128)(2,1)S(1)} all-gather(bf16[144,512]{1,0:T(8,128)(2,1)S(1)} %get-tuple-element.55), channel_id=2, replica_groups=mesh['z'=8,'y'=4,'x'=4,'c'=2] {'y'}, dimensions={0}, use_global_device_ids=true | all-gather | bytes 737280 | tf_op jit(solution)/shard_map/all_gather | solution.py:437
  38.9 5.0 %collective-permute-start.3 = (bf16[144,256]{1,0:T(8,128)(2,1)S(1)}, bf16[144,256]{1,0:T(8,128)(2,1)S(1)}, u32[]{:S(2)}, u32[]{:S(2)}) collective-permute-start(bf16[144,256]{1,0:T(8,128)(2,1)S(1)} %get-tuple-element.57), channel_id=1, source_target_pairs={{0,64},{32,96},{64,128},{96,160},{128,192},{160,224},{1,65},{33,97... | collective-permute-start | bytes 221192 | tf_op jit(solution)/shard_map/ppermute | solution.py:404
  43.9 4.2 %collective-permute-start.2 = (bf16[144,256]{1,0:T(8,128)(2,1)S(1)}, bf16[144,256]{1,0:T(8,128)(2,1)S(1)}, u32[]{:S(2)}, u32[]{:S(2)}) collective-permute-start(bf16[144,256]{1,0:T(8,128)(2,1)S(1)} %get-tuple-element.57), channel_id=1, source_target_pairs={{0,32},{32,64},{64,96},{96,128},{128,160},{160,192},{192,224},{1,3... | collective-permute-start | bytes 221192 | tf_op jit(solution)/shard_map/ppermute | solution.py:404
  50.7 2.9 %shard_map.182.yl = f32[768,256]{1,0:T(8,128)S(1)} custom-call(bf16[768,256]{1,0:T(8,128)(2,1)S(1)} %get-tuple-element.46.x, bf16[768,128]{1,0:T(8,128)(2,1)S(1)} %get-tuple-element.47.b, bf16[768,128]{1,0:T(8,128)(2,1)S(1)} %get-tuple-element.48.c, f32[8,768]{1,0:T(8,128)S(1)} %get-tuple-element.49.cum, f32[8,768]{1,0:T(8,128)S(1)} %get-tuple-element.50.dt, ...), custom_call_target="tpu_custom_call" | custom-call | tf_op jit(solution)/shard_map/pallas_call | solution.py:48
  56.1 3.5 %shard_map.184 = (bf16[384,256]{1,0:T(8,128)(2,1)S(1)}, bf16[384,256]{1,0:T(8,128)(2,1)S(1)}) custom-call(s32[1]{0:T(128)} %bitcast.core, f32[768,256]{1,0:T(8,128)S(1)} %shard_map.182.yl, bf16[768,128]{1,0:T(8,128)(2,1)S(1)} %get-tuple-element.48.c, f32[8,768]{1,0:T(8,128)S(1)} %get-tuple-element.54.dev, f32[136,512]{1,0:T(8,128)S(1)} %get-tuple-element.56.pre, ...), custom_call_target="tpu_custom_call" | custom-call | tf_op jit(solution)/shard_map/pallas_call | solution.py:48
  59.7 4.4 %collective-permute-start.6 = (bf16[384,256]{1,0:T(8,128)(2,1)S(1)}, bf16[384,256]{1,0:T(8,128)(2,1)S(1)}, u32[]{:S(2)}, u32[]{:S(2)}) collective-permute-start(bf16[384,256]{1,0:T(8,128)(2,1)S(1)} %get-tuple-element.60), channel_id=1, source_target_pairs={{0,1},{1,0},{2,3},{3,2},{4,5},{5,4},{6,7},{7,6},{8,9},{9,8},{10,11... | collective-permute-start | bytes 589832 | tf_op jit(solution)/shard_map/ppermute | solution.py:447
  65.4 2.2 %shard_map.185 = (bf16[384,512]{1,0:T(8,128)(2,1)S(1)}, bf16[384,512]{1,0:T(8,128)(2,1)S(1)}, bf16[384,512]{1,0:T(8,128)(2,1)S(1)}, bf16[384,512]{1,0:T(8,128)(2,1)S(1)}) custom-call(s32[1]{0:T(128)} %bitcast.1.where_x, bf16[384,256]{1,0:T(8,128)(2,1)S(1)} %get-tuple-element.59.a, bf16[384,256]{1,0:T(8,128)(2,1)S(1)} %collective-permute-done.6.b, ...), custom_call_target="tpu_custom_call" | custom-call | tf_op jit(solution)/shard_map/pallas_call | solution.py:48
  69.0 2.6 %collective-permute-start.10 = (bf16[384,512]{1,0:T(8,128)(2,1)S(1)}, bf16[384,512]{1,0:T(8,128)(2,1)S(1)}, u32[]{:S(2)}, u32[]{:S(2)}) collective-permute-start(bf16[384,512]{1,0:T(8,128)(2,1)S(1)} %get-tuple-element.63), channel_id=1, source_target_pairs={{0,4},{2,6},{4,0},{6,2},{1,5},{3,7},{5,1},{7,3},{8,12},{10,14},{12... | collective-permute-start | bytes 1179656 | tf_op jit(solution)/shard_map/ppermute | solution.py:407
  75.3 4.0 %collective-permute-done.9.r1 = bf16[384,512]{1,0:T(8,128)(2,1)S(1)} collective-permute-done((bf16[384,512]{1,0:T(8,128)(2,1)S(1)}, bf16[384,512]{1,0:T(8,128)(2,1)S(1)}, u32[]{:S(2)}, u32[]{:S(2)}) %collective-permute-start.9) | collective-permute-done | bytes 393248 | tf_op jit(solution)/shard_map/ppermute | solution.py:407
  79.3 9.5 %collective-permute-done.10.r2 = bf16[384,512]{1,0:T(8,128)(2,1)S(1)} collective-permute-done((bf16[384,512]{1,0:T(8,128)(2,1)S(1)}, bf16[384,512]{1,0:T(8,128)(2,1)S(1)}, u32[]{:S(2)}, u32[]{:S(2)}) %collective-permute-start.10) | collective-permute-done | bytes 393248 | tf_op jit(solution)/shard_map/ppermute | solution.py:407
  89.3 3.0 %collective-permute-start.16 = (bf16[208,512]{1,0:T(8,128)(2,1)S(1)}, bf16[208,512]{1,0:T(8,128)(2,1)S(1)}, u32[]{:S(2)}, u32[]{:S(2)}) collective-permute-start(bf16[208,512]{1,0:T(8,128)(2,1)S(1)} %get-tuple-element.66.b0), channel_id=1, source_target_pairs={{0,6},{2,0},{4,2},{6,4},{1,7},{3,1},{5,3},{7,5},{8,14},{10,8},{12,... | collective-permute-start | bytes 638984 | tf_op jit(solution)/shard_map/ppermute | solution.py:407
  92.2 4.2 %collective-permute-done.16.b3 = bf16[208,512]{1,0:T(8,128)(2,1)S(1)} collective-permute-done((bf16[208,512]{1,0:T(8,128)(2,1)S(1)}, bf16[208,512]{1,0:T(8,128)(2,1)S(1)}, u32[]{:S(2)}, u32[]{:S(2)}) %collective-permute-start.16) | collective-permute-done | bytes 213024 | tf_op jit(solution)/shard_map/ppermute | solution.py:407
  96.4 3.5 %collective-permute-start.17 = (bf16[208,512]{1,0:T(8,128)(2,1)S(1)}, bf16[208,512]{1,0:T(8,128)(2,1)S(1)}, u32[]{:S(2)}, u32[]{:S(2)}) collective-permute-start(bf16[208,512]{1,0:T(8,128)(2,1)S(1)} %collective-permute-done.16.b3), channel_id=1, source_target_pairs={{0,6},{2,0},{4,2},{6,4},{1,7},{3,1},{5,3},{7,5},{8,14},{10,8},{12,... | collective-permute-start | bytes 638984 | tf_op jit(solution)/shard_map/ppermute | solution.py:407
  101.4 6.2 %collective-permute-done.18.t3 = bf16[192,512]{1,0:T(8,128)(2,1)S(1)} collective-permute-done((bf16[192,512]{1,0:T(8,128)(2,1)S(1)}, bf16[192,512]{1,0:T(8,128)(2,1)S(1)}, u32[]{:S(2)}, u32[]{:S(2)}) %collective-permute-start.18) | collective-permute-done | bytes 196640 | tf_op jit(solution)/shard_map/ppermute | solution.py:407
  109.3 4.5 %all-gather.3.cloned.1.call-done = bf16[4096,2048]{1,0:T(8,128)(2,1)} async-done(((bf16[64,2048]{1,0:T(8,128)(2,1)}), bf16[4096,2048]{1,0:T(8,128)(2,1)}) %all-gather.3.cloned.1.call-update) | async-done | bytes 16777232 | tf_op jit(solution)/shard_map/all_gather | solution.py:415
  113.8 5.6 %up.1 = (bf16[384,2048]{1,0:T(8,128)(2,1)S(1)}, bf16[8,2,64,1024]{3,2,1,0:T(8,128)(2,1)S(1)}, bf16[8,2,64,1024]{3,2,1,0:T(8,128)(2,1)S(1)}, bf16[8,2,64,1024]{3,2,1,0:T(8,128)(2,1)S(1)}) custom-call(s32[1]{0:T(128)} %bitcast.1.where_x, bf16[384,2048]{1,0:T(8,128)(2,1)S(1)} %get-tuple-element.68.xn, bf16[32,2,64,2048]{3,2,1,0:T(8,128)(2,1)} %bitcast.11), custom_call_target="tpu_custom_call" | custom-call | tf_op jit(solution)/shard_map/up/pallas_call | solution.py:465
  125.4 2.7 %collective-permute-start.23 = (bf16[192,512]{1,0:T(8,128)(2,1)S(1)}, bf16[192,512]{1,0:T(8,128)(2,1)S(1)}, u32[]{:S(2)}, u32[]{:S(2)}) collective-permute-start(bf16[192,512]{1,0:T(8,128)(2,1)S(1)} %get-tuple-element.81), channel_id=1, source_target_pairs={{0,6},{2,0},{4,2},{6,4},{1,7},{3,1},{5,3},{7,5},{8,14},{10,8},{12,... | collective-permute-start | bytes 589832 | tf_op jit(solution)/shard_map/ppermute | solution.py:407
  131.0 2.6 %down0.1 = (bf16[192,512]{1,0:T(8,128)(2,1)S(1)}, bf16[192,512]{1,0:T(8,128)(2,1)S(1)}) custom-call(s32[1]{0:T(128)} %bitcast.1.where_x, bf16[384,2048]{1,0:T(8,128)(2,1)S(1)} %get-tuple-element.69.h, bf16[32,2,64,2048]{3,2,1,0:T(8,128)(2,1)} %bitcast.12), custom_call_target="tpu_custom_call" | custom-call | tf_op jit(solution)/shard_map/down0/pallas_call | solution.py:487
  133.6 2.3 %collective-permute-done.21.top1 = bf16[192,512]{1,0:T(8,128)(2,1)S(1)} collective-permute-done((bf16[192,512]{1,0:T(8,128)(2,1)S(1)}, bf16[192,512]{1,0:T(8,128)(2,1)S(1)}, u32[]{:S(2)}, u32[]{:S(2)}) %collective-permute-start.21) | collective-permute-done | bytes 196640 | tf_op jit(solution)/shard_map/ppermute | solution.py:407
  136.3 3.3 %collective-permute-start.27 = (f32[8,384]{1,0:T(8,128)S(1)}, f32[8,384]{1,0:T(8,128)S(1)}, u32[]{:S(2)}, u32[]{:S(2)}) collective-permute-start(f32[8,384]{1,0:T(8,128)S(1)} %get-tuple-element.84.s0), channel_id=1, source_target_pairs={{0,6},{2,0},{4,2},{6,4},{1,7},{3,1},{5,3},{7,5},{8,14},{10,8},{12,... | collective-permute-start | bytes 36872 | tf_op jit(solution)/shard_map/ppermute | solution.py:407
  140.4 3.2 %collective-permute-done.26.s2 = f32[8,384]{1,0:T(8,128)S(1)} collective-permute-done((f32[8,384]{1,0:T(8,128)S(1)}, f32[8,384]{1,0:T(8,128)S(1)}, u32[]{:S(2)}, u32[]{:S(2)}) %collective-permute-start.26) | collective-permute-done | bytes 12320 | tf_op jit(solution)/shard_map/ppermute | solution.py:407
  144.8 3.2 %collective-permute-start.28 = (bf16[384,256]{1,0:T(8,128)(2,1)S(1)}, bf16[384,256]{1,0:T(8,128)(2,1)S(1)}, u32[]{:S(2)}, u32[]{:S(2)}) collective-permute-start(bf16[384,256]{1,0:T(8,128)(2,1)S(1)} %get-tuple-element.86), channel_id=1, source_target_pairs={{0,1},{1,0},{2,3},{3,2},{4,5},{5,4},{6,7},{7,6},{8,9},{9,8},{10,11... | collective-permute-start | bytes 589832 | tf_op jit(solution)/shard_map/ppermute | solution.py:505
  (69 shorter events, 37.0 us)
Async XLA Ops:
  6.5 107.3 %all-gather.3.cloned.1.call-start = ((), (), s32[]{:S(2)}) async-start(), calls=%async_computation | async-start | bytes 17039360 | tf_op jit(solution)/shard_map/all_gather | solution.py:415
  8.2 57.2 %collective-permute-start.7 = (bf16[256,2048]{1,0:T(8,128)(2,1)}, bf16[256,2048]{1,0:T(8,128)(2,1)S(1)}, u32[]{:S(2)}, u32[]{:S(2)}) collective-permute-start(bf16[256,2048]{1,0:T(8,128)(2,1)} %wa.1), channel_id=1, source_target_pairs={{0,1},{1,0},{2,3},{3,2},{4,5},{5,4},{6,7},{7,6},{8,9},{9,8},{10,11... | collective-permute-start | bytes 3145736 | tf_op jit(solution)/shard_map/ppermute | solution.py:417
  13.0 4.6 %collective-permute-start = (bf16[2,512]{1,0:T(2,128)(2,1)S(1)}, bf16[2,512]{1,0:T(2,128)(2,1)S(1)}, u32[]{:S(2)}, u32[]{:S(2)}) collective-permute-start(bf16[2,512]{1,0:T(2,128)(2,1)S(1)} %pad_maximum_fusion.1), channel_id=1, source_target_pairs={{0,8},{8,16},{16,24},{24,32},{32,40},{40,48},{48,56},{56,64},{64,7... | collective-permute-start | bytes 6152 | tf_op jit(solution)/shard_map/ppermute | solution.py:404
  14.5 4.3 %collective-permute-start.1 = (bf16[2,512]{1,0:T(2,128)(2,1)S(1)}, bf16[2,512]{1,0:T(2,128)(2,1)S(1)}, u32[]{:S(2)}, u32[]{:S(2)}) collective-permute-start(bf16[2,512]{1,0:T(2,128)(2,1)S(1)} %pad_maximum_fusion.2), channel_id=1, source_target_pairs={{8,0},{16,8},{24,16},{32,24},{40,32},{48,40},{56,48},{64,56},{72,6... | collective-permute-start | bytes 6152 | tf_op jit(solution)/shard_map/ppermute | solution.py:404
  38.9 14.7 %collective-permute-start.3 = (bf16[144,256]{1,0:T(8,128)(2,1)S(1)}, bf16[144,256]{1,0:T(8,128)(2,1)S(1)}, u32[]{:S(2)}, u32[]{:S(2)}) collective-permute-start(bf16[144,256]{1,0:T(8,128)(2,1)S(1)} %get-tuple-element.57), channel_id=1, source_target_pairs={{0,64},{32,96},{64,128},{96,160},{128,192},{160,224},{1,65},{33,97... | collective-permute-start | bytes 221192 | tf_op jit(solution)/shard_map/ppermute | solution.py:404
  43.9 9.7 %collective-permute-start.2 = (bf16[144,256]{1,0:T(8,128)(2,1)S(1)}, bf16[144,256]{1,0:T(8,128)(2,1)S(1)}, u32[]{:S(2)}, u32[]{:S(2)}) collective-permute-start(bf16[144,256]{1,0:T(8,128)(2,1)S(1)} %get-tuple-element.57), channel_id=1, source_target_pairs={{0,32},{32,64},{64,96},{96,128},{128,160},{160,192},{192,224},{1,3... | collective-permute-start | bytes 221192 | tf_op jit(solution)/shard_map/ppermute | solution.py:404
  48.1 6.7 %collective-permute-start.5 = (bf16[144,256]{1,0:T(8,128)(2,1)S(1)}, bf16[144,256]{1,0:T(8,128)(2,1)S(1)}, u32[]{:S(2)}, u32[]{:S(2)}) collective-permute-start(bf16[144,256]{1,0:T(8,128)(2,1)S(1)} %get-tuple-element.58), channel_id=1, source_target_pairs={{64,0},{96,32},{128,64},{160,96},{192,128},{224,160},{65,1},{97,33... | collective-permute-start | bytes 221192 | tf_op jit(solution)/shard_map/ppermute | solution.py:404
  49.4 6.7 %collective-permute-start.4 = (bf16[144,256]{1,0:T(8,128)(2,1)S(1)}, bf16[144,256]{1,0:T(8,128)(2,1)S(1)}, u32[]{:S(2)}, u32[]{:S(2)}) collective-permute-start(bf16[144,256]{1,0:T(8,128)(2,1)S(1)} %get-tuple-element.58), channel_id=1, source_target_pairs={{32,0},{64,32},{96,64},{128,96},{160,128},{192,160},{224,192},{33,... | collective-permute-start | bytes 221192 | tf_op jit(solution)/shard_map/ppermute | solution.py:404
  59.7 5.7 %collective-permute-start.6 = (bf16[384,256]{1,0:T(8,128)(2,1)S(1)}, bf16[384,256]{1,0:T(8,128)(2,1)S(1)}, u32[]{:S(2)}, u32[]{:S(2)}) collective-permute-start(bf16[384,256]{1,0:T(8,128)(2,1)S(1)} %get-tuple-element.60), channel_id=1, source_target_pairs={{0,1},{1,0},{2,3},{3,2},{4,5},{5,4},{6,7},{7,6},{8,9},{9,8},{10,11... | collective-permute-start | bytes 589832 | tf_op jit(solution)/shard_map/ppermute | solution.py:447
  67.7 11.6 %collective-permute-start.9 = (bf16[384,512]{1,0:T(8,128)(2,1)S(1)}, bf16[384,512]{1,0:T(8,128)(2,1)S(1)}, u32[]{:S(2)}, u32[]{:S(2)}) collective-permute-start(bf16[384,512]{1,0:T(8,128)(2,1)S(1)} %get-tuple-element.62), channel_id=1, source_target_pairs={{0,2},{2,4},{4,6},{6,0},{1,3},{3,5},{5,7},{7,1},{8,10},{10,12},{12... | collective-permute-start | bytes 1179656 | tf_op jit(solution)/shard_map/ppermute | solution.py:407
  69.0 19.8 %collective-permute-start.10 = (bf16[384,512]{1,0:T(8,128)(2,1)S(1)}, bf16[384,512]{1,0:T(8,128)(2,1)S(1)}, u32[]{:S(2)}, u32[]{:S(2)}) collective-permute-start(bf16[384,512]{1,0:T(8,128)(2,1)S(1)} %get-tuple-element.63), channel_id=1, source_target_pairs={{0,4},{2,6},{4,0},{6,2},{1,5},{3,7},{5,1},{7,3},{8,12},{10,14},{12... | collective-permute-start | bytes 1179656 | tf_op jit(solution)/shard_map/ppermute | solution.py:407
  71.6 17.3 %collective-permute-start.11 = (bf16[384,512]{1,0:T(8,128)(2,1)S(1)}, bf16[384,512]{1,0:T(8,128)(2,1)S(1)}, u32[]{:S(2)}, u32[]{:S(2)}) collective-permute-start(bf16[384,512]{1,0:T(8,128)(2,1)S(1)} %get-tuple-element.64), channel_id=1, source_target_pairs={{0,6},{2,0},{4,2},{6,4},{1,7},{3,1},{5,3},{7,5},{8,14},{10,8},{12,... | collective-permute-start | bytes 1179656 | tf_op jit(solution)/shard_map/ppermute | solution.py:407
  89.3 7.2 %collective-permute-start.16 = (bf16[208,512]{1,0:T(8,128)(2,1)S(1)}, bf16[208,512]{1,0:T(8,128)(2,1)S(1)}, u32[]{:S(2)}, u32[]{:S(2)}) collective-permute-start(bf16[208,512]{1,0:T(8,128)(2,1)S(1)} %get-tuple-element.66.b0), channel_id=1, source_target_pairs={{0,6},{2,0},{4,2},{6,4},{1,7},{3,1},{5,3},{7,5},{8,14},{10,8},{12,... | collective-permute-start | bytes 638984 | tf_op jit(solution)/shard_map/ppermute | solution.py:407
  92.2 7.8 %collective-permute-start.13 = (bf16[192,512]{1,0:T(8,128)(2,1)S(1)}, bf16[192,512]{1,0:T(8,128)(2,1)S(1)}, u32[]{:S(2)}, u32[]{:S(2)}) collective-permute-start(bf16[192,512]{1,0:T(8,128)(2,1)S(1)} %get-tuple-element.65.t0), channel_id=1, source_target_pairs={{0,2},{2,4},{4,6},{6,0},{1,3},{3,5},{5,7},{7,1},{8,10},{10,12},{12... | collective-permute-start | bytes 589832 | tf_op jit(solution)/shard_map/ppermute | solution.py:407
  92.2 15.4 %collective-permute-start.14 = (bf16[208,512]{1,0:T(8,128)(2,1)S(1)}, bf16[208,512]{1,0:T(8,128)(2,1)S(1)}, u32[]{:S(2)}, u32[]{:S(2)}) collective-permute-start(bf16[208,512]{1,0:T(8,128)(2,1)S(1)} %get-tuple-element.66.b0), channel_id=1, source_target_pairs={{0,2},{2,4},{4,6},{6,0},{1,3},{3,5},{5,7},{7,1},{8,10},{10,12},{12... | collective-permute-start | bytes 638984 | tf_op jit(solution)/shard_map/ppermute | solution.py:407
  96.4 11.5 %collective-permute-start.17 = (bf16[208,512]{1,0:T(8,128)(2,1)S(1)}, bf16[208,512]{1,0:T(8,128)(2,1)S(1)}, u32[]{:S(2)}, u32[]{:S(2)}) collective-permute-start(bf16[208,512]{1,0:T(8,128)(2,1)S(1)} %collective-permute-done.16.b3), channel_id=1, source_target_pairs={{0,6},{2,0},{4,2},{6,4},{1,7},{3,1},{5,3},{7,5},{8,14},{10,8},{12,... | collective-permute-start | bytes 638984 | tf_op jit(solution)/shard_map/ppermute | solution.py:407
  100.0 7.7 %collective-permute-start.18 = (bf16[192,512]{1,0:T(8,128)(2,1)S(1)}, bf16[192,512]{1,0:T(8,128)(2,1)S(1)}, u32[]{:S(2)}, u32[]{:S(2)}) collective-permute-start(bf16[192,512]{1,0:T(8,128)(2,1)S(1)} %get-tuple-element.65.t0), channel_id=1, source_target_pairs={{0,6},{2,0},{4,2},{6,4},{1,7},{3,1},{5,3},{7,5},{8,14},{10,8},{12,... | collective-permute-start | bytes 589832 | tf_op jit(solution)/shard_map/ppermute | solution.py:407
  100.0 7.9 %collective-permute-start.15 = (bf16[192,512]{1,0:T(8,128)(2,1)S(1)}, bf16[192,512]{1,0:T(8,128)(2,1)S(1)}, u32[]{:S(2)}, u32[]{:S(2)}) collective-permute-start(bf16[192,512]{1,0:T(8,128)(2,1)S(1)} %collective-permute-done.13.t1), channel_id=1, source_target_pairs={{0,2},{2,4},{4,6},{6,0},{1,3},{3,5},{5,7},{7,1},{8,10},{10,12},{12... | collective-permute-start | bytes 589832 | tf_op jit(solution)/shard_map/ppermute | solution.py:407
  120.5 7.6 %collective-permute-start.19 = (bf16[192,512]{1,0:T(8,128)(2,1)S(1)}, bf16[192,512]{1,0:T(8,128)(2,1)S(1)}, u32[]{:S(2)}, u32[]{:S(2)}) collective-permute-start(bf16[192,512]{1,0:T(8,128)(2,1)S(1)} %get-tuple-element.75), channel_id=1, source_target_pairs={{0,2},{2,4},{4,6},{6,0},{1,3},{3,5},{5,7},{7,1},{8,10},{10,12},{12... | collective-permute-start | bytes 589832 | tf_op jit(solution)/shard_map/ppermute | solution.py:407
  121.8 6.4 %collective-permute-start.20 = (bf16[192,512]{1,0:T(8,128)(2,1)S(1)}, bf16[192,512]{1,0:T(8,128)(2,1)S(1)}, u32[]{:S(2)}, u32[]{:S(2)}) collective-permute-start(bf16[192,512]{1,0:T(8,128)(2,1)S(1)} %get-tuple-element.78), channel_id=1, source_target_pairs={{0,6},{2,0},{4,2},{6,4},{1,7},{3,1},{5,3},{7,5},{8,14},{10,8},{12,... | collective-permute-start | bytes 589832 | tf_op jit(solution)/shard_map/ppermute | solution.py:407
  124.3 9.3 %collective-permute-start.22 = (bf16[192,512]{1,0:T(8,128)(2,1)S(1)}, bf16[192,512]{1,0:T(8,128)(2,1)S(1)}, u32[]{:S(2)}, u32[]{:S(2)}) collective-permute-start(bf16[192,512]{1,0:T(8,128)(2,1)S(1)} %get-tuple-element.80), channel_id=1, source_target_pairs={{0,2},{2,4},{4,6},{6,0},{1,3},{3,5},{5,7},{7,1},{8,10},{10,12},{12... | collective-permute-start | bytes 589832 | tf_op jit(solution)/shard_map/ppermute | solution.py:407
  125.4 8.2 %collective-permute-start.23 = (bf16[192,512]{1,0:T(8,128)(2,1)S(1)}, bf16[192,512]{1,0:T(8,128)(2,1)S(1)}, u32[]{:S(2)}, u32[]{:S(2)}) collective-permute-start(bf16[192,512]{1,0:T(8,128)(2,1)S(1)} %get-tuple-element.81), channel_id=1, source_target_pairs={{0,6},{2,0},{4,2},{6,4},{1,7},{3,1},{5,3},{7,5},{8,14},{10,8},{12,... | collective-permute-start | bytes 589832 | tf_op jit(solution)/shard_map/ppermute | solution.py:407
  128.2 7.7 %collective-permute-start.21 = (bf16[192,512]{1,0:T(8,128)(2,1)S(1)}, bf16[192,512]{1,0:T(8,128)(2,1)S(1)}, u32[]{:S(2)}, u32[]{:S(2)}) collective-permute-start(bf16[192,512]{1,0:T(8,128)(2,1)S(1)} %get-tuple-element.79), channel_id=1, source_target_pairs={{0,2},{2,4},{4,6},{6,0},{1,3},{3,5},{5,7},{7,1},{8,10},{10,12},{12... | collective-permute-start | bytes 589832 | tf_op jit(solution)/shard_map/ppermute | solution.py:407
  129.1 6.9 %collective-permute-start.24 = (bf16[192,512]{1,0:T(8,128)(2,1)S(1)}, bf16[192,512]{1,0:T(8,128)(2,1)S(1)}, u32[]{:S(2)}, u32[]{:S(2)}) collective-permute-start(bf16[192,512]{1,0:T(8,128)(2,1)S(1)} %get-tuple-element.82), channel_id=1, source_target_pairs={{0,6},{2,0},{4,2},{6,4},{1,7},{3,1},{5,3},{7,5},{8,14},{10,8},{12,... | collective-permute-start | bytes 589832 | tf_op jit(solution)/shard_map/ppermute | solution.py:407
  (9 other events, 65.4 us)
Sparse Core Ops, SparseCore 0:
  10.1 103.7 all-gather.2

commit v5 on v4

--- a/solution.py
+++ b/solution.py
@@ -308,7 +308,7 @@
     return loads
 
 
-def up_body(where_x, xn, w, hidden, far, after, back, up, sems):
+def up_body(where_x, xn, w, hidden, after, back, top, bottom, far, up, sems):
     loads = []
     for k in range(CHUNKS):
         src = w.at[:, k // 2, :, pl.ds((k % 2) * 512, 512)]
@@ -324,7 +324,10 @@
         got = jnp.maximum(dot(xn[...], up[k].reshape(2048, 512), 1, 0), 0.0)
         hidden[:, pl.ds(pl.multiple_of(k * 512, 512), 512)] = (got * got).astype(BF)
 
-    for load in loads[CHUNKS:]:
+    for load in loads[CHUNKS : CHUNKS + 2]:
+        load.wait()
+    down_body(hidden, far, top, bottom)
+    for load in loads[CHUNKS + 2 :]:
         load.wait()
 
 
@@ -462,12 +465,15 @@
     rows, resid = call(rows_body, 9, [((HALF, 2048), BF), ((HALF, 512), BF)], scalars=1)(
         at_x, top, bottom, top1, bottom1, top2, bottom2, top3, bottom3
     )
-    hidden, part2, part1, part3 = pl.pallas_call(
+    hidden, part1, part3, far_top, far_bottom = pl.pallas_call(
         up_body,
         in_specs=[sm(), vm(), pl.BlockSpec(memory_space=pltpu.HBM)],
-        out_specs=[vm()] * 4,
-        out_shape=[pltpu.VMEM((HALF, 2048), BF)] + [pltpu.VMEM((8, 2, 64, 1024), BF)] * 3,
+        out_specs=[vm()] * 5,
+        out_shape=[pltpu.VMEM((HALF, 2048), BF)]
+        + [pltpu.VMEM((8, 2, 64, 1024), BF)] * 2
+        + [pltpu.VMEM((QUARTER, 512), BF)] * 2,
         scratch_shapes=[
+            pltpu.VMEM((8, 2, 64, 1024), BF),
             pltpu.VMEM((CHUNKS, 32, 64, 2048 // CHUNKS), BF),
             pltpu.SemaphoreType.DMA((CHUNKS + 6,)),
         ],
@@ -478,7 +484,6 @@
     def down(part):
         return call(down_body, 2, [((QUARTER, 512), BF)] * 2)(hidden, part)
 
-    far_top, far_bottom = down(part2)
     far_top, far_bottom = around(far_top, 1), around(far_bottom, 3)
     next_top, next_bottom = down(part1)
     next_bottom = around(next_bottom, 1)

time: 157 us -> 157 us (level)
    pallas_call x13 -> x12, Pallas kernels: 20.3 us -> 19.3 us  [call(): run(*[off(b) if k in far else b if k < scalars else near(b) for k, b in e...]
where the time goes in v5:
time: 157 us
  starting transfers between devices  51.4 us (33%)
  waiting for transfers between devices  42.4 us (27%)
  Pallas kernels  28.6 us (18%)
  blocking collectives  14.8 us (9%)
  between operations  13.7 us (9%)
  local copies, waits for them, and re-layouts  3.94 us (3%)
  other arithmetic  1.71 us (1%)
    ppermute x18, waiting for transfers between devices, around(): return lax.ppermute(a, 'x', [(i, (i + by) % 4) for i in range(4)])  30.6 us
    ppermute x18, starting transfers between devices, around(): return lax.ppermute(a, 'x', [(i, (i + by) % 4) for i in range(4)])  24.5 us
    pallas_call x12, Pallas kernels, call(): run(*[off(b) if k in far else b if k < scalars else near(b) for k, b in e...  19.3 us
    all_gather x1, blocking collectives, layer(): rows = lax.all_gather(pay, 'y')  14.8 us
    ppermute x6, starting transfers between devices, shift(): lax.ppermute(a, axis, [(i, i + by) for i in range(count) if 0 <= i + by <...  14.6 us
    pallas_call x1, Pallas kernels, layer(): pl.pallas_call(up_body, in_specs=[sm(), vm(), pl.BlockSpec(memory_space=p...  6.67 us
    all_gather x1, waiting for transfers between devices, layer(): lax.all_gather(weights, ('z', 'y', 'c'), axis=0, tiled=True)  4.54 us
    ppermute x1, starting transfers between devices, layer(): other = lax.ppermute(send, 'c', swap)  4.41 us
  transfers between devices with their start and end apart: 30, of which 15 were waited for; matrix products, arithmetic and copies ran while one was open for 2% of the time, Pallas kernels for 13%

profile of v5, /device:TPU:1, one launch (start us, length us, event | category | flops | bytes accessed | tf_op | source)
XLA Modules:
  0.0 156.5 jit_solution(547480177018303221)
XLA Ops:
  8.2 3.3 %collective-permute-start.7 = (bf16[256,2048]{1,0:T(8,128)(2,1)}, bf16[256,2048]{1,0:T(8,128)(2,1)S(1)}, u32[]{:S(2)}, u32[]{:S(2)}) collective-permute-start(bf16[256,2048]{1,0:T(8,128)(2,1)} %wa.1), channel_id=1, source_target_pairs={{0,1},{1,0},{2,3},{3,2},{4,5},{5,4},{6,7},{7,6},{8,9},{9,8},{10,11... | collective-permute-start | bytes 3145736 | tf_op jit(solution)/shard_map/ppermute | solution.py:420
  18.8 5.0 %shard_map.181 = (bf16[768,256]{1,0:T(8,128)(2,1)S(1)}, bf16[768,128]{1,0:T(8,128)(2,1)S(1)}, bf16[768,128]{1,0:T(8,128)(2,1)S(1)}, f32[8,768]{1,0:T(8,128)S(1)}...) custom-call(s32[1]{0:T(128)} %bitcast.2.sp, ...), custom_call_target="tpu_custom_call" | custom-call | tf_op jit(solution)/shard_map/pallas_call | solution.py:48
  23.9 14.8 %all-gather = bf16[576,512]{1,0:T(8,128)(2,1)S(1)} all-gather(bf16[144,512]{1,0:T(8,128)(2,1)S(1)} %get-tuple-element.54), channel_id=2, replica_groups=mesh['z'=8,'y'=4,'x'=4,'c'=2] {'y'}, dimensions={0}, use_global_device_ids=true | all-gather | bytes 737280 | tf_op jit(solution)/shard_map/all_gather | solution.py:440
  38.9 5.0 %collective-permute-start.3 = (bf16[144,256]{1,0:T(8,128)(2,1)S(1)}, bf16[144,256]{1,0:T(8,128)(2,1)S(1)}, u32[]{:S(2)}, u32[]{:S(2)}) collective-permute-start(bf16[144,256]{1,0:T(8,128)(2,1)S(1)} %get-tuple-element.56), channel_id=1, source_target_pairs={{0,64},{32,96},{64,128},{96,160},{128,192},{160,224},{1,65},{33,97... | collective-permute-start | bytes 221192 | tf_op jit(solution)/shard_map/ppermute | solution.py:407
  43.9 4.2 %collective-permute-start.2 = (bf16[144,256]{1,0:T(8,128)(2,1)S(1)}, bf16[144,256]{1,0:T(8,128)(2,1)S(1)}, u32[]{:S(2)}, u32[]{:S(2)}) collective-permute-start(bf16[144,256]{1,0:T(8,128)(2,1)S(1)} %get-tuple-element.56), channel_id=1, source_target_pairs={{0,32},{32,64},{64,96},{96,128},{128,160},{160,192},{192,224},{1,3... | collective-permute-start | bytes 221192 | tf_op jit(solution)/shard_map/ppermute | solution.py:407
  50.7 2.9 %shard_map.182.yl = f32[768,256]{1,0:T(8,128)S(1)} custom-call(bf16[768,256]{1,0:T(8,128)(2,1)S(1)} %get-tuple-element.45.x, bf16[768,128]{1,0:T(8,128)(2,1)S(1)} %get-tuple-element.46.b, bf16[768,128]{1,0:T(8,128)(2,1)S(1)} %get-tuple-element.47.c, f32[8,768]{1,0:T(8,128)S(1)} %get-tuple-element.48.cum, f32[8,768]{1,0:T(8,128)S(1)} %get-tuple-element.49.dt, ...), custom_call_target="tpu_custom_call" | custom-call | tf_op jit(solution)/shard_map/pallas_call | solution.py:48
  56.1 3.5 %shard_map.184 = (bf16[384,256]{1,0:T(8,128)(2,1)S(1)}, bf16[384,256]{1,0:T(8,128)(2,1)S(1)}) custom-call(s32[1]{0:T(128)} %bitcast.core, f32[768,256]{1,0:T(8,128)S(1)} %shard_map.182.yl, bf16[768,128]{1,0:T(8,128)(2,1)S(1)} %get-tuple-element.47.c, f32[8,768]{1,0:T(8,128)S(1)} %get-tuple-element.53.dev, f32[136,512]{1,0:T(8,128)S(1)} %get-tuple-element.55.pre, ...), custom_call_target="tpu_custom_call" | custom-call | tf_op jit(solution)/shard_map/pallas_call | solution.py:48
  59.7 4.4 %collective-permute-start.6 = (bf16[384,256]{1,0:T(8,128)(2,1)S(1)}, bf16[384,256]{1,0:T(8,128)(2,1)S(1)}, u32[]{:S(2)}, u32[]{:S(2)}) collective-permute-start(bf16[384,256]{1,0:T(8,128)(2,1)S(1)} %get-tuple-element.59), channel_id=1, source_target_pairs={{0,1},{1,0},{2,3},{3,2},{4,5},{5,4},{6,7},{7,6},{8,9},{9,8},{10,11... | collective-permute-start | bytes 589832 | tf_op jit(solution)/shard_map/ppermute | solution.py:450
  65.4 2.2 %shard_map.185 = (bf16[384,512]{1,0:T(8,128)(2,1)S(1)}, bf16[384,512]{1,0:T(8,128)(2,1)S(1)}, bf16[384,512]{1,0:T(8,128)(2,1)S(1)}, bf16[384,512]{1,0:T(8,128)(2,1)S(1)}) custom-call(s32[1]{0:T(128)} %bitcast.1.where_x, bf16[384,256]{1,0:T(8,128)(2,1)S(1)} %get-tuple-element.58.a, bf16[384,256]{1,0:T(8,128)(2,1)S(1)} %collective-permute-done.6.b, ...), custom_call_target="tpu_custom_call" | custom-call | tf_op jit(solution)/shard_map/pallas_call | solution.py:48
  69.0 2.6 %collective-permute-start.10 = (bf16[384,512]{1,0:T(8,128)(2,1)S(1)}, bf16[384,512]{1,0:T(8,128)(2,1)S(1)}, u32[]{:S(2)}, u32[]{:S(2)}) collective-permute-start(bf16[384,512]{1,0:T(8,128)(2,1)S(1)} %get-tuple-element.62), channel_id=1, source_target_pairs={{0,4},{2,6},{4,0},{6,2},{1,5},{3,7},{5,1},{7,3},{8,12},{10,14},{12... | collective-permute-start | bytes 1179656 | tf_op jit(solution)/shard_map/ppermute | solution.py:410
  75.3 4.0 %collective-permute-done.9.r1 = bf16[384,512]{1,0:T(8,128)(2,1)S(1)} collective-permute-done((bf16[384,512]{1,0:T(8,128)(2,1)S(1)}, bf16[384,512]{1,0:T(8,128)(2,1)S(1)}, u32[]{:S(2)}, u32[]{:S(2)}) %collective-permute-start.9) | collective-permute-done | bytes 393248 | tf_op jit(solution)/shard_map/ppermute | solution.py:410
  79.3 9.5 %collective-permute-done.10.r2 = bf16[384,512]{1,0:T(8,128)(2,1)S(1)} collective-permute-done((bf16[384,512]{1,0:T(8,128)(2,1)S(1)}, bf16[384,512]{1,0:T(8,128)(2,1)S(1)}, u32[]{:S(2)}, u32[]{:S(2)}) %collective-permute-start.10) | collective-permute-done | bytes 393248 | tf_op jit(solution)/shard_map/ppermute | solution.py:410
  89.3 3.0 %collective-permute-start.16 = (bf16[208,512]{1,0:T(8,128)(2,1)S(1)}, bf16[208,512]{1,0:T(8,128)(2,1)S(1)}, u32[]{:S(2)}, u32[]{:S(2)}) collective-permute-start(bf16[208,512]{1,0:T(8,128)(2,1)S(1)} %get-tuple-element.65.b0), channel_id=1, source_target_pairs={{0,6},{2,0},{4,2},{6,4},{1,7},{3,1},{5,3},{7,5},{8,14},{10,8},{12,... | collective-permute-start | bytes 638984 | tf_op jit(solution)/shard_map/ppermute | solution.py:410
  92.2 4.2 %collective-permute-done.16.b3 = bf16[208,512]{1,0:T(8,128)(2,1)S(1)} collective-permute-done((bf16[208,512]{1,0:T(8,128)(2,1)S(1)}, bf16[208,512]{1,0:T(8,128)(2,1)S(1)}, u32[]{:S(2)}, u32[]{:S(2)}) %collective-permute-start.16) | collective-permute-done | bytes 213024 | tf_op jit(solution)/shard_map/ppermute | solution.py:410
  96.4 3.5 %collective-permute-start.17 = (bf16[208,512]{1,0:T(8,128)(2,1)S(1)}, bf16[208,512]{1,0:T(8,128)(2,1)S(1)}, u32[]{:S(2)}, u32[]{:S(2)}) collective-permute-start(bf16[208,512]{1,0:T(8,128)(2,1)S(1)} %collective-permute-done.16.b3), channel_id=1, source_target_pairs={{0,6},{2,0},{4,2},{6,4},{1,7},{3,1},{5,3},{7,5},{8,14},{10,8},{12,... | collective-permute-start | bytes 638984 | tf_op jit(solution)/shard_map/ppermute | solution.py:410
  101.4 6.2 %collective-permute-done.18.t3 = bf16[192,512]{1,0:T(8,128)(2,1)S(1)} collective-permute-done((bf16[192,512]{1,0:T(8,128)(2,1)S(1)}, bf16[192,512]{1,0:T(8,128)(2,1)S(1)}, u32[]{:S(2)}, u32[]{:S(2)}) %collective-permute-start.18) | collective-permute-done | bytes 196640 | tf_op jit(solution)/shard_map/ppermute | solution.py:410
  109.3 4.5 %all-gather.3.cloned.1.call-done = bf16[4096,2048]{1,0:T(8,128)(2,1)} async-done(((bf16[64,2048]{1,0:T(8,128)(2,1)}), bf16[4096,2048]{1,0:T(8,128)(2,1)}) %all-gather.3.cloned.1.call-update) | async-done | bytes 16777232 | tf_op jit(solution)/shard_map/all_gather | solution.py:418
  113.8 6.7 %up.1 = (bf16[384,2048]{1,0:T(8,128)(2,1)S(1)}, bf16[8,2,64,1024]{3,2,1,0:T(8,128)(2,1)S(1)}, bf16[8,2,64,1024]{3,2,1,0:T(8,128)(2,1)S(1)}, bf16[192,512]{1,0:T(8,128)(2,1)S(1)}, bf16[192,512]{1,0:T(8,128)(2,1)S(1)}) custom-call(s32[1]{0:T(128)} %bitcast.1.where_x, bf16[384,2048]{1,0:T(8,128)(2,1)S(1)} %get-tuple-element.67.xn, ...), custom_call_target="tpu_custom_call" | custom-call | tf_op jit(solution)/shard_map/up/pallas_call | solution.py:468
  125.4 2.7 %collective-permute-start.23 = (bf16[192,512]{1,0:T(8,128)(2,1)S(1)}, bf16[192,512]{1,0:T(8,128)(2,1)S(1)}, u32[]{:S(2)}, u32[]{:S(2)}) collective-permute-start(bf16[192,512]{1,0:T(8,128)(2,1)S(1)} %get-tuple-element.79), channel_id=1, source_target_pairs={{0,6},{2,0},{4,2},{6,4},{1,7},{3,1},{5,3},{7,5},{8,14},{10,8},{12,... | collective-permute-start | bytes 589832 | tf_op jit(solution)/shard_map/ppermute | solution.py:410
  130.9 2.6 %down0.1 = (bf16[192,512]{1,0:T(8,128)(2,1)S(1)}, bf16[192,512]{1,0:T(8,128)(2,1)S(1)}) custom-call(s32[1]{0:T(128)} %bitcast.1.where_x, bf16[384,2048]{1,0:T(8,128)(2,1)S(1)} %get-tuple-element.68.h, bf16[32,2,64,2048]{3,2,1,0:T(8,128)(2,1)} %bitcast.12), custom_call_target="tpu_custom_call" | custom-call | tf_op jit(solution)/shard_map/down0/pallas_call | solution.py:492
  133.5 2.9 %collective-permute-done.21.top1 = bf16[192,512]{1,0:T(8,128)(2,1)S(1)} collective-permute-done((bf16[192,512]{1,0:T(8,128)(2,1)S(1)}, bf16[192,512]{1,0:T(8,128)(2,1)S(1)}, u32[]{:S(2)}, u32[]{:S(2)}) %collective-permute-start.21) | collective-permute-done | bytes 196640 | tf_op jit(solution)/shard_map/ppermute | solution.py:410
  136.9 2.7 %collective-permute-start.27 = (f32[8,384]{1,0:T(8,128)S(1)}, f32[8,384]{1,0:T(8,128)S(1)}, u32[]{:S(2)}, u32[]{:S(2)}) collective-permute-start(f32[8,384]{1,0:T(8,128)S(1)} %get-tuple-element.82.s0), channel_id=1, source_target_pairs={{0,6},{2,0},{4,2},{6,4},{1,7},{3,1},{5,3},{7,5},{8,14},{10,8},{12,... | collective-permute-start | bytes 36872 | tf_op jit(solution)/shard_map/ppermute | solution.py:410
  140.4 3.2 %collective-permute-done.26.s2 = f32[8,384]{1,0:T(8,128)S(1)} collective-permute-done((f32[8,384]{1,0:T(8,128)S(1)}, f32[8,384]{1,0:T(8,128)S(1)}, u32[]{:S(2)}, u32[]{:S(2)}) %collective-permute-start.26) | collective-permute-done | bytes 12320 | tf_op jit(solution)/shard_map/ppermute | solution.py:410
  144.7 3.2 %collective-permute-start.28 = (bf16[384,256]{1,0:T(8,128)(2,1)S(1)}, bf16[384,256]{1,0:T(8,128)(2,1)S(1)}, u32[]{:S(2)}, u32[]{:S(2)}) collective-permute-start(bf16[384,256]{1,0:T(8,128)(2,1)S(1)} %get-tuple-element.84), channel_id=1, source_target_pairs={{0,1},{1,0},{2,3},{3,2},{4,5},{5,4},{6,7},{7,6},{8,9},{9,8},{10,11... | collective-permute-start | bytes 589832 | tf_op jit(solution)/shard_map/ppermute | solution.py:510
  (68 shorter events, 36.0 us)
Async XLA Ops:
  6.5 107.3 %all-gather.3.cloned.1.call-start = ((), (), s32[]{:S(2)}) async-start(), calls=%async_computation | async-start | bytes 17039360 | tf_op jit(solution)/shard_map/all_gather | solution.py:418
  8.2 57.2 %collective-permute-start.7 = (bf16[256,2048]{1,0:T(8,128)(2,1)}, bf16[256,2048]{1,0:T(8,128)(2,1)S(1)}, u32[]{:S(2)}, u32[]{:S(2)}) collective-permute-start(bf16[256,2048]{1,0:T(8,128)(2,1)} %wa.1), channel_id=1, source_target_pairs={{0,1},{1,0},{2,3},{3,2},{4,5},{5,4},{6,7},{7,6},{8,9},{9,8},{10,11... | collective-permute-start | bytes 3145736 | tf_op jit(solution)/shard_map/ppermute | solution.py:420
  13.0 4.6 %collective-permute-start = (bf16[2,512]{1,0:T(2,128)(2,1)S(1)}, bf16[2,512]{1,0:T(2,128)(2,1)S(1)}, u32[]{:S(2)}, u32[]{:S(2)}) collective-permute-start(bf16[2,512]{1,0:T(2,128)(2,1)S(1)} %pad_maximum_fusion.1), channel_id=1, source_target_pairs={{0,8},{8,16},{16,24},{24,32},{32,40},{40,48},{48,56},{56,64},{64,7... | collective-permute-start | bytes 6152 | tf_op jit(solution)/shard_map/ppermute | solution.py:407
  14.5 4.3 %collective-permute-start.1 = (bf16[2,512]{1,0:T(2,128)(2,1)S(1)}, bf16[2,512]{1,0:T(2,128)(2,1)S(1)}, u32[]{:S(2)}, u32[]{:S(2)}) collective-permute-start(bf16[2,512]{1,0:T(2,128)(2,1)S(1)} %pad_maximum_fusion.2), channel_id=1, source_target_pairs={{8,0},{16,8},{24,16},{32,24},{40,32},{48,40},{56,48},{64,56},{72,6... | collective-permute-start | bytes 6152 | tf_op jit(solution)/shard_map/ppermute | solution.py:407
  38.9 14.7 %collective-permute-start.3 = (bf16[144,256]{1,0:T(8,128)(2,1)S(1)}, bf16[144,256]{1,0:T(8,128)(2,1)S(1)}, u32[]{:S(2)}, u32[]{:S(2)}) collective-permute-start(bf16[144,256]{1,0:T(8,128)(2,1)S(1)} %get-tuple-element.56), channel_id=1, source_target_pairs={{0,64},{32,96},{64,128},{96,160},{128,192},{160,224},{1,65},{33,97... | collective-permute-start | bytes 221192 | tf_op jit(solution)/shard_map/ppermute | solution.py:407
  43.9 9.7 %collective-permute-start.2 = (bf16[144,256]{1,0:T(8,128)(2,1)S(1)}, bf16[144,256]{1,0:T(8,128)(2,1)S(1)}, u32[]{:S(2)}, u32[]{:S(2)}) collective-permute-start(bf16[144,256]{1,0:T(8,128)(2,1)S(1)} %get-tuple-element.56), channel_id=1, source_target_pairs={{0,32},{32,64},{64,96},{96,128},{128,160},{160,192},{192,224},{1,3... | collective-permute-start | bytes 221192 | tf_op jit(solution)/shard_map/ppermute | solution.py:407
  48.1 6.7 %collective-permute-start.5 = (bf16[144,256]{1,0:T(8,128)(2,1)S(1)}, bf16[144,256]{1,0:T(8,128)(2,1)S(1)}, u32[]{:S(2)}, u32[]{:S(2)}) collective-permute-start(bf16[144,256]{1,0:T(8,128)(2,1)S(1)} %get-tuple-element.57), channel_id=1, source_target_pairs={{64,0},{96,32},{128,64},{160,96},{192,128},{224,160},{65,1},{97,33... | collective-permute-start | bytes 221192 | tf_op jit(solution)/shard_map/ppermute | solution.py:407
  49.4 6.7 %collective-permute-start.4 = (bf16[144,256]{1,0:T(8,128)(2,1)S(1)}, bf16[144,256]{1,0:T(8,128)(2,1)S(1)}, u32[]{:S(2)}, u32[]{:S(2)}) collective-permute-start(bf16[144,256]{1,0:T(8,128)(2,1)S(1)} %get-tuple-element.57), channel_id=1, source_target_pairs={{32,0},{64,32},{96,64},{128,96},{160,128},{192,160},{224,192},{33,... | collective-permute-start | bytes 221192 | tf_op jit(solution)/shard_map/ppermute | solution.py:407
  59.7 5.7 %collective-permute-start.6 = (bf16[384,256]{1,0:T(8,128)(2,1)S(1)}, bf16[384,256]{1,0:T(8,128)(2,1)S(1)}, u32[]{:S(2)}, u32[]{:S(2)}) collective-permute-start(bf16[384,256]{1,0:T(8,128)(2,1)S(1)} %get-tuple-element.59), channel_id=1, source_target_pairs={{0,1},{1,0},{2,3},{3,2},{4,5},{5,4},{6,7},{7,6},{8,9},{9,8},{10,11... | collective-permute-start | bytes 589832 | tf_op jit(solution)/shard_map/ppermute | solution.py:450
  67.7 11.6 %collective-permute-start.9 = (bf16[384,512]{1,0:T(8,128)(2,1)S(1)}, bf16[384,512]{1,0:T(8,128)(2,1)S(1)}, u32[]{:S(2)}, u32[]{:S(2)}) collective-permute-start(bf16[384,512]{1,0:T(8,128)(2,1)S(1)} %get-tuple-element.61), channel_id=1, source_target_pairs={{0,2},{2,4},{4,6},{6,0},{1,3},{3,5},{5,7},{7,1},{8,10},{10,12},{12... | collective-permute-start | bytes 1179656 | tf_op jit(solution)/shard_map/ppermute | solution.py:410
  69.0 19.8 %collective-permute-start.10 = (bf16[384,512]{1,0:T(8,128)(2,1)S(1)}, bf16[384,512]{1,0:T(8,128)(2,1)S(1)}, u32[]{:S(2)}, u32[]{:S(2)}) collective-permute-start(bf16[384,512]{1,0:T(8,128)(2,1)S(1)} %get-tuple-element.62), channel_id=1, source_target_pairs={{0,4},{2,6},{4,0},{6,2},{1,5},{3,7},{5,1},{7,3},{8,12},{10,14},{12... | collective-permute-start | bytes 1179656 | tf_op jit(solution)/shard_map/ppermute | solution.py:410
  71.6 17.3 %collective-permute-start.11 = (bf16[384,512]{1,0:T(8,128)(2,1)S(1)}, bf16[384,512]{1,0:T(8,128)(2,1)S(1)}, u32[]{:S(2)}, u32[]{:S(2)}) collective-permute-start(bf16[384,512]{1,0:T(8,128)(2,1)S(1)} %get-tuple-element.63), channel_id=1, source_target_pairs={{0,6},{2,0},{4,2},{6,4},{1,7},{3,1},{5,3},{7,5},{8,14},{10,8},{12,... | collective-permute-start | bytes 1179656 | tf_op jit(solution)/shard_map/ppermute | solution.py:410
  89.3 7.2 %collective-permute-start.16 = (bf16[208,512]{1,0:T(8,128)(2,1)S(1)}, bf16[208,512]{1,0:T(8,128)(2,1)S(1)}, u32[]{:S(2)}, u32[]{:S(2)}) collective-permute-start(bf16[208,512]{1,0:T(8,128)(2,1)S(1)} %get-tuple-element.65.b0), channel_id=1, source_target_pairs={{0,6},{2,0},{4,2},{6,4},{1,7},{3,1},{5,3},{7,5},{8,14},{10,8},{12,... | collective-permute-start | bytes 638984 | tf_op jit(solution)/shard_map/ppermute | solution.py:410
  92.2 7.8 %collective-permute-start.13 = (bf16[192,512]{1,0:T(8,128)(2,1)S(1)}, bf16[192,512]{1,0:T(8,128)(2,1)S(1)}, u32[]{:S(2)}, u32[]{:S(2)}) collective-permute-start(bf16[192,512]{1,0:T(8,128)(2,1)S(1)} %get-tuple-element.64.t0), channel_id=1, source_target_pairs={{0,2},{2,4},{4,6},{6,0},{1,3},{3,5},{5,7},{7,1},{8,10},{10,12},{12... | collective-permute-start | bytes 589832 | tf_op jit(solution)/shard_map/ppermute | solution.py:410
  92.2 15.4 %collective-permute-start.14 = (bf16[208,512]{1,0:T(8,128)(2,1)S(1)}, bf16[208,512]{1,0:T(8,128)(2,1)S(1)}, u32[]{:S(2)}, u32[]{:S(2)}) collective-permute-start(bf16[208,512]{1,0:T(8,128)(2,1)S(1)} %get-tuple-element.65.b0), channel_id=1, source_target_pairs={{0,2},{2,4},{4,6},{6,0},{1,3},{3,5},{5,7},{7,1},{8,10},{10,12},{12... | collective-permute-start | bytes 638984 | tf_op jit(solution)/shard_map/ppermute | solution.py:410
  96.4 11.5 %collective-permute-start.17 = (bf16[208,512]{1,0:T(8,128)(2,1)S(1)}, bf16[208,512]{1,0:T(8,128)(2,1)S(1)}, u32[]{:S(2)}, u32[]{:S(2)}) collective-permute-start(bf16[208,512]{1,0:T(8,128)(2,1)S(1)} %collective-permute-done.16.b3), channel_id=1, source_target_pairs={{0,6},{2,0},{4,2},{6,4},{1,7},{3,1},{5,3},{7,5},{8,14},{10,8},{12,... | collective-permute-start | bytes 638984 | tf_op jit(solution)/shard_map/ppermute | solution.py:410
  100.0 7.7 %collective-permute-start.18 = (bf16[192,512]{1,0:T(8,128)(2,1)S(1)}, bf16[192,512]{1,0:T(8,128)(2,1)S(1)}, u32[]{:S(2)}, u32[]{:S(2)}) collective-permute-start(bf16[192,512]{1,0:T(8,128)(2,1)S(1)} %get-tuple-element.64.t0), channel_id=1, source_target_pairs={{0,6},{2,0},{4,2},{6,4},{1,7},{3,1},{5,3},{7,5},{8,14},{10,8},{12,... | collective-permute-start | bytes 589832 | tf_op jit(solution)/shard_map/ppermute | solution.py:410
  100.0 7.9 %collective-permute-start.15 = (bf16[192,512]{1,0:T(8,128)(2,1)S(1)}, bf16[192,512]{1,0:T(8,128)(2,1)S(1)}, u32[]{:S(2)}, u32[]{:S(2)}) collective-permute-start(bf16[192,512]{1,0:T(8,128)(2,1)S(1)} %collective-permute-done.13.t1), channel_id=1, source_target_pairs={{0,2},{2,4},{4,6},{6,0},{1,3},{3,5},{5,7},{7,1},{8,10},{10,12},{12... | collective-permute-start | bytes 589832 | tf_op jit(solution)/shard_map/ppermute | solution.py:410
  120.5 7.5 %collective-permute-start.19 = (bf16[192,512]{1,0:T(8,128)(2,1)S(1)}, bf16[192,512]{1,0:T(8,128)(2,1)S(1)}, u32[]{:S(2)}, u32[]{:S(2)}) collective-permute-start(bf16[192,512]{1,0:T(8,128)(2,1)S(1)} %get-tuple-element.73), channel_id=1, source_target_pairs={{0,2},{2,4},{4,6},{6,0},{1,3},{3,5},{5,7},{7,1},{8,10},{10,12},{12... | collective-permute-start | bytes 589832 | tf_op jit(solution)/shard_map/ppermute | solution.py:410
  121.8 6.3 %collective-permute-start.20 = (bf16[192,512]{1,0:T(8,128)(2,1)S(1)}, bf16[192,512]{1,0:T(8,128)(2,1)S(1)}, u32[]{:S(2)}, u32[]{:S(2)}) collective-permute-start(bf16[192,512]{1,0:T(8,128)(2,1)S(1)} %get-tuple-element.76), channel_id=1, source_target_pairs={{0,6},{2,0},{4,2},{6,4},{1,7},{3,1},{5,3},{7,5},{8,14},{10,8},{12,... | collective-permute-start | bytes 589832 | tf_op jit(solution)/shard_map/ppermute | solution.py:410
  125.3 8.2 %collective-permute-start.22 = (bf16[192,512]{1,0:T(8,128)(2,1)S(1)}, bf16[192,512]{1,0:T(8,128)(2,1)S(1)}, u32[]{:S(2)}, u32[]{:S(2)}) collective-permute-start(bf16[192,512]{1,0:T(8,128)(2,1)S(1)} %get-tuple-element.78), channel_id=1, source_target_pairs={{0,2},{2,4},{4,6},{6,0},{1,3},{3,5},{5,7},{7,1},{8,10},{10,12},{12... | collective-permute-start | bytes 589832 | tf_op jit(solution)/shard_map/ppermute | solution.py:410
  125.4 8.1 %collective-permute-start.23 = (bf16[192,512]{1,0:T(8,128)(2,1)S(1)}, bf16[192,512]{1,0:T(8,128)(2,1)S(1)}, u32[]{:S(2)}, u32[]{:S(2)}) collective-permute-start(bf16[192,512]{1,0:T(8,128)(2,1)S(1)} %get-tuple-element.79), channel_id=1, source_target_pairs={{0,6},{2,0},{4,2},{6,4},{1,7},{3,1},{5,3},{7,5},{8,14},{10,8},{12,... | collective-permute-start | bytes 589832 | tf_op jit(solution)/shard_map/ppermute | solution.py:410
  128.2 8.3 %collective-permute-start.21 = (bf16[192,512]{1,0:T(8,128)(2,1)S(1)}, bf16[192,512]{1,0:T(8,128)(2,1)S(1)}, u32[]{:S(2)}, u32[]{:S(2)}) collective-permute-start(bf16[192,512]{1,0:T(8,128)(2,1)S(1)} %get-tuple-element.77), channel_id=1, source_target_pairs={{0,2},{2,4},{4,6},{6,0},{1,3},{3,5},{5,7},{7,1},{8,10},{10,12},{12... | collective-permute-start | bytes 589832 | tf_op jit(solution)/shard_map/ppermute | solution.py:410
  129.1 7.4 %collective-permute-start.24 = (bf16[192,512]{1,0:T(8,128)(2,1)S(1)}, bf16[192,512]{1,0:T(8,128)(2,1)S(1)}, u32[]{:S(2)}, u32[]{:S(2)}) collective-permute-start(bf16[192,512]{1,0:T(8,128)(2,1)S(1)} %get-tuple-element.80), channel_id=1, source_target_pairs={{0,6},{2,0},{4,2},{6,4},{1,7},{3,1},{5,3},{7,5},{8,14},{10,8},{12,... | collective-permute-start | bytes 589832 | tf_op jit(solution)/shard_map/ppermute | solution.py:410
  (9 other events, 64.8 us)
Sparse Core Ops, SparseCore 0:
  10.1 103.7 all-gather.2
